TPU v7x, 32 devices: a whole 2x2x4 slice. The times are simulated.
32 devices in a mesh: sp: 8 (over z, x), tp: 4 (over y, core).
Axes of the slice: x: 2, y: 2, z: 4, core: 2. Of those that a mesh axis runs over, the one named last changes fastest.
Arguments:
- tokens: bfloat16 [8192, 2048], P('sp', 'tp'), may hold values from -6 to 6
- norm_gain: float32 [2048], replicated, may hold values from 0.1 to 1.9
- att_query: bfloat16 [2048, 1024], P(None, 'tp'), may hold values from -1 to 1
- att_key: bfloat16 [2048, 512], P(None, 'tp'), may hold values from -16 to 16
- att_value: bfloat16 [2048, 512], P(None, 'tp'), may hold values from -0.125 to 0.125
- ret_query: bfloat16 [2048, 512], P(None, 'tp'), may hold values from -0.125 to 0.125
- ret_key: bfloat16 [2048, 512], P(None, 'tp'), may hold values from -0.125 to 0.125
- ret_value: bfloat16 [2048, 1024], P(None, 'tp'), may hold values from -0.125 to 0.125
- ret_gate: bfloat16 [2048, 1024], P(None, 'tp'), may hold values from -0.125 to 0.125
- att_sink: float32 [16], P('tp'), may hold values from 4 to 7
- decay_log: float32 [8, 8192], P('tp', 'sp'), may hold values from -2 to 0, as said below
- init_state: float32 [2, 8, 64, 128], P(None, 'tp'), may hold values from -24 to 24
- out_att: bfloat16 [1024, 2048], P('tp'), may hold values from -0.125 to 0.125
- out_ret: bfloat16 [1024, 2048], P('tp'), may hold values from -0.125 to 0.125
Outputs:
- mixed: bfloat16 [8192, 2048], P('sp', 'tp')
Inputs may be any that keep to these rules, and one draw needn't show every extreme that they name: `decay_log`: log decays, negative.
All inputs are finite; a program needn't handle non-finite values.
Results may differ from a plain program's by a relative error of at most 0.02.
Values may be sent and summed in bfloat16 or wider, within the bound.
No kernel may reach another device: no remote copies, remote signals or barrier semaphores. Data moves between devices by JAX's collectives and lax.ppermute only.
A program may use at most 64 MiB of HBM per device.

v0:
```python
import jax
import jax.numpy as jnp
from jax import lax
from jax.sharding import PartitionSpec as P

HD = 64
RK = 64
RV = 128
WINDOW = 128
RET_BLOCK = 128


NORM_EPS = 1e-06
ROPE_BASE = 10000.0
HIGHEST = lax.Precision.HIGHEST


def padded_2(block, sides, width):
    for axis, dim in sides:
        count = lax.axis_size(axis)
        forward = [(i, i + 1) for i in range(count - 1)]
        backward = [(target, source) for source, target in forward]
        low = lax.ppermute(
            lax.slice_in_dim(block, block.shape[dim] - width, None, axis=dim), axis, forward
        )
        high = lax.ppermute(lax.slice_in_dim(block, 0, width, axis=dim), axis, backward)
        block = jnp.concatenate([low, block, high], axis=dim)
    return block


def passed_along(value, axis, by):
    length = lax.axis_size(axis)
    pairs = [(i, i + by) for i in range(length) if 0 <= i + by < length]
    return lax.ppermute(value, axis, pairs)


def rotated(values, positions):
    half_dim = values.shape[-1] // 2
    inverse = ROPE_BASE ** (-2.0 * jnp.arange(half_dim, dtype=jnp.float32) / values.shape[-1])
    angles = positions.astype(jnp.float32)[:, None] * inverse[None, :]
    cosine = jnp.cos(angles)[:, None, :]
    sine = jnp.sin(angles)[:, None, :]
    first_half = values[..., :half_dim]
    second_half = values[..., half_dim:]
    return jnp.concatenate(
        [first_half * cosine - second_half * sine, first_half * sine + second_half * cosine],
        axis=-1,
    )


def advance(state_now, item_pair):
    factor_now, term_now = item_pair
    return (factor_now[:, None, None] * state_now + term_now, state_now)


def body(
    tokens,
    norm_gain,
    att_query,
    att_key,
    att_value,
    ret_query,
    ret_key,
    ret_value,
    ret_gate,
    att_sink,
    decay_log,
    init_state,
    out_att,
    out_ret,
):
    tok_rows = tokens.shape[0]
    chan_local = tokens.shape[1]
    query_cols = att_query.shape[1]
    kv_cols = att_key.shape[1]
    rk_cols = ret_query.shape[1]
    rv_cols = ret_value.shape[1]
    heads_local = att_sink.shape[0]
    kv_local = kv_cols // HD
    groups = heads_local // kv_local
    ret_local = decay_log.shape[0]
    seq_offset = lax.axis_index("sp") * tok_rows
    seq_len = tok_rows * lax.axis_size("sp")
    joined = jnp.concatenate(
        [att_query, att_key, att_value, ret_query, ret_key, ret_value, ret_gate], axis=1
    )
    piece_f = lax.all_gather(tokens, "tp", axis=1, tiled=True).astype(jnp.float32)
    scaled = (piece_f * norm_gain[None, :]).astype(jnp.bfloat16)
    proj_sums = jnp.dot(scaled, joined, preferred_element_type=jnp.float32)
    squares = jnp.sum(piece_f * piece_f, axis=1)
    inv_rms = lax.rsqrt(squares / (chan_local * lax.axis_size("tp")) + NORM_EPS)
    projected = (proj_sums * inv_rms[:, None]).astype(jnp.bfloat16)
    off_rq = query_cols + 2 * kv_cols
    off_rk = off_rq + rk_cols
    off_rv = off_rk + rk_cols
    off_gate = off_rv + rv_cols
    key_vals = projected[:, query_cols:off_rq]
    padded = padded_2(key_vals, (("sp", 0),), WINDOW)
    block_rows = min(512, tok_rows)
    span_rows = block_rows + 2 * WINDOW
    queries = projected[:, :query_cols].reshape(tok_rows, kv_local, groups, HD)
    sink_col = att_sink.reshape(kv_local, groups, 1, 1)
    outputs = []
    for first_row in range(0, tok_rows, block_rows):
        query_block = queries[first_row : first_row + block_rows]
        span_block = padded[first_row : first_row + span_rows]
        key_block = span_block[:, :kv_cols].reshape(span_rows, kv_local, HD)
        value_block = span_block[:, kv_cols:].reshape(span_rows, kv_local, HD)
        scores = jnp.einsum(
            "qkgd,skd->kgqs", query_block, key_block, preferred_element_type=jnp.float32
        ) * HD ** (-0.5)
        query_pos = seq_offset + first_row + jnp.arange(block_rows, dtype=jnp.int32)
        key_pos = seq_offset + first_row - WINDOW + jnp.arange(span_rows, dtype=jnp.int32)
        allowed = (
            (jnp.abs(query_pos[:, None] - key_pos[None, :]) <= WINDOW)
            & (key_pos >= 0)[None, :]
            & (key_pos < seq_len)[None, :]
        )
        scores = jnp.where(allowed, scores, -jnp.inf)
        row_top = jnp.maximum(jnp.max(scores, axis=-1, keepdims=True), sink_col)
        raised = jnp.exp(scores - row_top)
        denominator = jnp.sum(raised, axis=-1, keepdims=True) + jnp.exp(sink_col - row_top)
        weights_bf = (raised / denominator).astype(jnp.bfloat16)
        block_out = jnp.einsum(
            "kgqs,skd->qkgd", weights_bf, value_block, preferred_element_type=jnp.float32
        )
        outputs.append(block_out.reshape(block_rows, query_cols).astype(jnp.bfloat16))
    attended = jnp.concatenate(outputs, axis=0)
    positions = seq_offset + jnp.arange(tok_rows, dtype=jnp.int32)
    query_rot = rotated(
        projected[:, off_rq:off_rk].astype(jnp.float32).reshape(tok_rows, ret_local, RK), positions
    )
    key_rot = rotated(
        projected[:, off_rk:off_rv].astype(jnp.float32).reshape(tok_rows, ret_local, RK), positions
    ) * RK ** (-0.5)
    value_f = projected[:, off_rv:off_gate].astype(jnp.float32).reshape(tok_rows, ret_local, RV)
    gate_f = projected[:, off_gate:].astype(jnp.float32)
    block_count = tok_rows // RET_BLOCK

    def heads_first(values, width):
        return jnp.transpose(values.reshape(block_count, RET_BLOCK, ret_local, width), (2, 0, 1, 3))

    query_h = heads_first(query_rot, RK)
    key_h = heads_first(key_rot, RK)
    value_h = heads_first(value_f, RV)
    block_logs = decay_log.reshape(ret_local, block_count, RET_BLOCK)
    cumul = jnp.cumsum(block_logs, axis=-1)
    block_log = cumul[..., -1]
    inner_w = jnp.einsum("hbnk,hbmk->hbnm", query_h, key_h, precision=HIGHEST) * jnp.exp(
        -jnp.abs(cumul[..., :, None] - cumul[..., None, :])
    )
    local_out = jnp.einsum("hbnm,hbmv->hbnv", inner_w, value_h, precision=HIGHEST)
    fwd_terms = jnp.einsum(
        "hbmk,hbmv->bhkv",
        key_h * jnp.exp(block_log[..., None] - cumul)[..., None],
        value_h,
        precision=HIGHEST,
    )
    bwd_terms = jnp.einsum(
        "hbmk,hbmv->bhkv", key_h * jnp.exp(cumul)[..., None], value_h, precision=HIGHEST
    )
    factors = jnp.exp(block_log).T
    zero_state = jnp.zeros((ret_local, RK, RV), jnp.float32)
    fwd_total, fwd_local = lax.scan(advance, zero_state, (factors, fwd_terms))
    bwd_total, bwd_local = lax.scan(advance, zero_state, (factors, bwd_terms), reverse=True)
    before_log = jnp.cumsum(block_log, axis=1) - block_log
    after_log = jnp.sum(block_log, axis=1, keepdims=True) - jnp.cumsum(block_log, axis=1)
    device_factor = jnp.exp(jnp.sum(block_log, axis=1))
    my_index = lax.axis_index("sp")
    axis_count = lax.axis_size("sp")

    def relay(turn_index, running):
        fwd_now, bwd_now = running
        sent_fwd = passed_along(
            (device_factor[:, None, None] * fwd_now + fwd_total).astype(jnp.bfloat16), "sp", 1
        ).astype(jnp.float32)
        sent_bwd = passed_along(
            (device_factor[:, None, None] * bwd_now + bwd_total).astype(jnp.bfloat16), "sp", -1
        ).astype(jnp.float32)
        return (
            jnp.where(my_index == 0, init_state[0], sent_fwd),
            jnp.where(my_index == axis_count - 1, init_state[1], sent_bwd),
        )

    fwd_start, bwd_start = lax.fori_loop(0, axis_count - 1, relay, (init_state[0], init_state[1]))
    fwd_in = fwd_local + jnp.exp(before_log).T[:, :, None, None] * fwd_start[None]
    bwd_in = bwd_local + jnp.exp(after_log).T[:, :, None, None] * bwd_start[None]
    cross_out = jnp.exp(cumul)[..., None] * jnp.einsum(
        "hbnk,bhkv->hbnv", query_h, fwd_in, precision=HIGHEST
    )
    cross_out = cross_out + jnp.exp(block_log[..., None] - cumul)[..., None] * jnp.einsum(
        "hbnk,bhkv->hbnv", query_h, bwd_in, precision=HIGHEST
    )
    combined = local_out + cross_out
    centered = combined - jnp.mean(combined, axis=-1, keepdims=True)
    normed = centered * lax.rsqrt(jnp.mean(centered * centered, axis=-1, keepdims=True) + NORM_EPS)
    retained = jnp.transpose(normed, (1, 2, 0, 3)).reshape(tok_rows, ret_local * RV)
    ret_out = (jax.nn.silu(gate_f) * retained).astype(jnp.bfloat16)
    contract_dims = (((0,), (1,)), ((), ()))
    att_part = lax.dot_general(out_att, attended, contract_dims, preferred_element_type=jnp.float32)
    summed = lax.psum_scatter(
        (
            att_part
            + lax.dot_general(out_ret, ret_out, contract_dims, preferred_element_type=jnp.float32)
        ).astype(jnp.bfloat16),
        "tp",
        scatter_dimension=0,
        tiled=True,
    ).astype(jnp.float32)
    return summed.T.astype(jnp.bfloat16)


def solution(mesh):
    in_specs = (
        P("sp", "tp"),
        P(),
        P(None, "tp"),
        P(None, "tp"),
        P(None, "tp"),
        P(None, "tp"),
        P(None, "tp"),
        P(None, "tp"),
        P(None, "tp"),
        P("tp"),
        P("tp", "sp"),
        P(None, "tp", None, None),
        P("tp", None),
        P("tp", None),
    )
    out_specs = P("sp", "tp")
    return jax.shard_map(body, mesh=mesh, in_specs=in_specs, out_specs=out_specs, check_vma=False)
```

profile of v0, /device:TPU:17, one launch (start us, length us, event | category | flops | bytes accessed | tf_op | source)
XLA Modules:
  0.0 273.7 jit_solution(15155859861386811351)
XLA Ops:
  19.3 2.5 constant_dynamic-update-slice_fusion.6
  21.8 2.0 constant_dynamic-update-slice_fusion.5
  29.9 15.0 %all-gather.2.cloned.1.call-done = bf16[1024,2048]{1,0:T(8,128)(2,1)} async-done(((bf16[1024,512]{1,0:T(8,128)(2,1)}), bf16[1024,2048]{1,0:T(8,128)(2,1)}) %all-gather.2.cloned.1.call-update) | async-done | bytes 4194320 | tf_op jit(solution)/shard_map/all_gather | solution.py:87
  44.9 3.1 %fusion.3 = f32[1024]{0:T(1024)S(1)} fusion(bf16[1024,2048]{1,0:T(8,128)(2,1)} %all-gather.2.cloned.1.call-done), kind=kLoop, calls=%fused_computation.15 | loop fusion | flops 6290432 | bytes 4198400 | tf_op jit(solution)/shard_map/reduce_sum | solution.py:90
  48.0 8.9 %multiply_convert_fusion = bf16[1024,1280]{1,0:T(8,128)(2,1)S(1)} fusion(bf16[2048,1280]{1,0:T(8,128)(2,1)} %constant_dynamic-update-slice_fusion, bf16[1024,2048]{1,0:T(8,128)(2,1)} %all-gather.2.cloned.1.call-done, f32[2048]{0:T(1024)S(1)} %copy-done.25, f32[1024]{0:T(1024)S(1)} %add_rsqrt_fusion), kind=kOutput, calls=%fused_computation.25 | convolution fusion | flops 5377622016 | bytes 12070912 | tf_op jit(solution)/shard_map/dot_general | solution.py:89
  60.4 3.1 %collective-permute-start.2 = (bf16[128,256]{1,0:T(8,128)(2,1)}, bf16[128,256]{1,0:T(8,128)(2,1)}, u32[]{:S(2)}, u32[]{:S(2)}) collective-permute-start(bf16[128,256]{1,0:T(8,128)(2,1)} %get-tuple-element.351), channel_id=1, source_target_pairs={{0,4},{4,8},{8,12},{12,16},{16,20},{20,24},{24,28},{1,5},{5,9},{9,... | collective-permute-start | bytes 196616 | tf_op jit(solution)/shard_map/ppermute | solution.py:23
  63.5 3.3 %collective-permute-start.3 = (bf16[128,256]{1,0:T(8,128)(2,1)}, bf16[128,256]{1,0:T(8,128)(2,1)}, u32[]{:S(2)}, u32[]{:S(2)}) collective-permute-start(bf16[128,256]{1,0:T(8,128)(2,1)} %get-tuple-element.352), channel_id=1, source_target_pairs={{4,0},{8,4},{12,8},{16,12},{20,16},{24,20},{28,24},{5,1},{9,5},{13... | collective-permute-start | bytes 196616 | tf_op jit(solution)/shard_map/ppermute | solution.py:26
  72.1 13.0 %while.46 = (s32[]{:T(128)}, f32[2,64,128]{2,1,0:T(8,128)S(1)}, f32[8,2,64,128]{3,2,1,0:T(8,128)S(1)}, f32[8,2]{1,0:T(8,128)}, f32[8,2,64,128]{3,2,1,0:T(8,128)}, /*index=5*/s32[]{:T(128)}, s32[]{:T(128)}, s32[]{:T(128)}) while((s32[]{:T(128)}, f32[2,64,128]{2,1,0:T(8,128)S(1)}, f32[8,2,64,128]{3,2,1,0:T(8,128)S(1)}, ...), condition=%wide.region_11.12_spmd.clone, body=%wide.region_10.11_spmd.clone.sunk | while | flops 65540 | bytes 327832 | solution.py:165
  87.1 13.0 %while.45 = (s32[]{:T(128)}, f32[2,64,128]{2,1,0:T(8,128)S(1)}, f32[8,2,64,128]{3,2,1,0:T(8,128)S(1)}, f32[8,2]{1,0:T(8,128)}, f32[8,2,64,128]{3,2,1,0:T(8,128)}, /*index=5*/s32[]{:T(128)}, s32[]{:T(128)}) while((s32[]{:T(128)}, f32[2,64,128]{2,1,0:T(8,128)S(1)}, f32[8,2,64,128]{3,2,1,0:T(8,128)S(1)}, f32[8,2]{1,0:T(8,128)}, ...), condition=%wide.region_7.8_spmd.clone, body=%wide.region_6.7_spmd.clone.sunk | while | flops 65539 | bytes 327812 | solution.py:164
  100.1 75.1 %while.44 = (s32[]{:T(128)}, f32[2,64,128]{2,1,0:T(8,128)S(1)}, f32[2,64,128]{2,1,0:T(8,128)S(1)}, pred[]{:T(512)}, f32[2,2,64,128]{3,2,1,0:T(8,128)S(1)}, /*ind...) while((s32[]{:T(128)}, f32[2,64,128]{2,1,0:T(8,128)S(1)}, ...), condition=%wide.region_13.14_spmd, body=%wide.region_12.13_spmd.sunk | while | flops 163842 | bytes 1179895 | solution.py:185
  101.5 2.2 collective-permute-start
  103.7 3.1 %collective-permute-start.1 = (bf16[2,64,128]{2,1,0:T(8,128)(2,1)}, bf16[2,64,128]{2,1,0:T(8,128)(2,1)S(1)}, u32[]{:S(2)}, u32[]{:S(2)}) collective-permute-start(bf16[2,64,128]{2,1,0:T(8,128)(2,1)} %get-tuple-element.505), channel_id=1, source_target_pairs={{0,4},{4,8},{8,12},{12,16},{16,20},{20,24},{24,28},{1,5},{5,9},{9,... | collective-permute-start | bytes 98312 | tf_op jit(solution)/shard_map/while/body/eval_jaxpr/ppermute | solution.py:34
  106.8 2.6 collective-permute-done.1
  112.3 2.2 collective-permute-start
  114.4 3.1 %collective-permute-start.1 = (bf16[2,64,128]{2,1,0:T(8,128)(2,1)}, bf16[2,64,128]{2,1,0:T(8,128)(2,1)S(1)}, u32[]{:S(2)}, u32[]{:S(2)}) collective-permute-start(bf16[2,64,128]{2,1,0:T(8,128)(2,1)} %get-tuple-element.505), channel_id=1, source_target_pairs={{0,4},{4,8},{8,12},{12,16},{16,20},{20,24},{24,28},{1,5},{5,9},{9,... | collective-permute-start | bytes 98312 | tf_op jit(solution)/shard_map/while/body/eval_jaxpr/ppermute | solution.py:34
  117.6 2.6 collective-permute-done.1
  123.0 3.0 %collective-permute-start = (bf16[2,64,128]{2,1,0:T(8,128)(2,1)}, bf16[2,64,128]{2,1,0:T(8,128)(2,1)S(1)}, u32[]{:S(2)}, u32[]{:S(2)}) collective-permute-start(bf16[2,64,128]{2,1,0:T(8,128)(2,1)} %get-tuple-element.504), channel_id=1, source_target_pairs={{4,0},{8,4},{12,8},{16,12},{20,16},{24,20},{28,24},{5,1},{9,5},{13... | collective-permute-start | bytes 98312 | tf_op jit(solution)/shard_map/while/body/eval_jaxpr/ppermute | solution.py:34
  126.1 2.2 collective-permute-start.1
  128.3 3.5 %collective-permute-done.1 = bf16[2,64,128]{2,1,0:T(8,128)(2,1)S(1)} collective-permute-done((bf16[2,64,128]{2,1,0:T(8,128)(2,1)}, bf16[2,64,128]{2,1,0:T(8,128)(2,1)S(1)}, u32[]{:S(2)}, u32[]{:S(2)}) %collective-permute-start.1) | collective-permute-done | bytes 32800 | tf_op jit(solution)/shard_map/while/body/eval_jaxpr/ppermute | solution.py:34
  136.6 3.4 %collective-permute-start.1 = (bf16[2,64,128]{2,1,0:T(8,128)(2,1)}, bf16[2,64,128]{2,1,0:T(8,128)(2,1)S(1)}, u32[]{:S(2)}, u32[]{:S(2)}) collective-permute-start(bf16[2,64,128]{2,1,0:T(8,128)(2,1)} %get-tuple-element.505), channel_id=1, source_target_pairs={{0,4},{4,8},{8,12},{12,16},{16,20},{20,24},{24,28},{1,5},{5,9},{9,... | collective-permute-start | bytes 98312 | tf_op jit(solution)/shard_map/while/body/eval_jaxpr/ppermute | solution.py:34
  140.0 2.4 collective-permute-done.1
  147.0 3.4 %collective-permute-start.1 = (bf16[2,64,128]{2,1,0:T(8,128)(2,1)}, bf16[2,64,128]{2,1,0:T(8,128)(2,1)S(1)}, u32[]{:S(2)}, u32[]{:S(2)}) collective-permute-start(bf16[2,64,128]{2,1,0:T(8,128)(2,1)} %get-tuple-element.505), channel_id=1, source_target_pairs={{0,4},{4,8},{8,12},{12,16},{16,20},{20,24},{24,28},{1,5},{5,9},{9,... | collective-permute-start | bytes 98312 | tf_op jit(solution)/shard_map/while/body/eval_jaxpr/ppermute | solution.py:34
  150.4 2.4 collective-permute-done.1
  157.5 3.4 %collective-permute-start.1 = (bf16[2,64,128]{2,1,0:T(8,128)(2,1)}, bf16[2,64,128]{2,1,0:T(8,128)(2,1)S(1)}, u32[]{:S(2)}, u32[]{:S(2)}) collective-permute-start(bf16[2,64,128]{2,1,0:T(8,128)(2,1)} %get-tuple-element.505), channel_id=1, source_target_pairs={{0,4},{4,8},{8,12},{12,16},{16,20},{20,24},{24,28},{1,5},{5,9},{9,... | collective-permute-start | bytes 98312 | tf_op jit(solution)/shard_map/while/body/eval_jaxpr/ppermute | solution.py:34
  160.9 2.4 collective-permute-done.1
  168.0 3.4 %collective-permute-start.1 = (bf16[2,64,128]{2,1,0:T(8,128)(2,1)}, bf16[2,64,128]{2,1,0:T(8,128)(2,1)S(1)}, u32[]{:S(2)}, u32[]{:S(2)}) collective-permute-start(bf16[2,64,128]{2,1,0:T(8,128)(2,1)} %get-tuple-element.505), channel_id=1, source_target_pairs={{0,4},{4,8},{8,12},{12,16},{16,20},{20,24},{24,28},{1,5},{5,9},{9,... | collective-permute-start | bytes 98312 | tf_op jit(solution)/shard_map/while/body/eval_jaxpr/ppermute | solution.py:34
  171.4 2.4 collective-permute-done.1
  179.8 2.0 convolution_multiply_fusion
  191.6 2.2 fusion.6
  200.1 4.9 %fusion.17 = bf16[2,64,2,512]{3,1,2,0:T(8,128)(2,1)S(1)} fusion(bf16[768,2,64,1]{0,2,3,1:T(8,128)(2,1)} %bitcast.206, f32[2,768,512,2]{2,1,3,0:T(8,128)} %copy-done.2, f32[2,2,512]{2,1,0:T(2,128)S(1)} %exponential_add_fusion, f32[2,2,512]{2,1,0:T(2,128)S(1)} %get-tuple-element.381, pred[512,768]{0,1:T(8,128)(4,1)} %fusion.16), kind=kOutput, calls=%fused_computation.41 | convolution fusion | flops 209321984 | bytes 7159808 | tf_op jit(solution)/shard_map/kgqs,skd->qkgd/dot_general | solution.py:124
  208.6 4.4 %fusion.10 = bf16[2048,1024]{0,1:T(8,128)(2,1)} fusion(f32[1024,2048]{1,0:T(8,128)S(1)} %fusion.32, bf16[256,2048]{1,0:T(8,128)(2,1)S(1)} %copy-done.14, f32[128,8,2,128]{3,2,1,0:T(2,128)S(1)} %bitcast.193, bf16[1024,1280]{1,0:T(8,128)(2,1)} %copy-done.5), kind=kOutput, calls=%fused_computation.29 | convolution fusion | flops 1079771136 | bytes 15204352 | tf_op jit(solution)/shard_map/dot_general | solution.py:204
  213.0 53.9 %reduce-scatter.2.cloned.1.call-done = bf16[512,1024]{0,1:T(8,128)(2,1)} async-done(((bf16[2048,1024]{0,1:T(8,128)(2,1)}), bf16[512,1024]{0,1:T(8,128)(2,1)}) %reduce-scatter.2.cloned.1.call-update) | async-done | bytes 1048592 | tf_op jit(solution)/shard_map/reduce_scatter | solution.py:201
  (234 shorter events, 106.5 us)
Async XLA Ops:
  6.5 200.5 %copy-start = (bf16[256,2048]{1,0:T(8,128)(2,1)S(1)}, bf16[256,2048]{1,0:T(8,128)(2,1)}, u32[]{:S(2)}) copy-start(bf16[256,2048]{1,0:T(8,128)(2,1)} %param.32) | copy-start | bytes 3145732
  6.5 21.1 %copy-start.12 = (bf16[2048,256]{1,0:T(8,128)(2,1)S(1)}, bf16[2048,256]{1,0:T(8,128)(2,1)}, u32[]{:S(2)}) copy-start(bf16[2048,256]{1,0:T(8,128)(2,1)} %param.27) | copy-start | bytes 3145732
  6.5 22.3 %copy-start.13 = (bf16[2048,256]{1,0:T(8,128)(2,1)S(1)}, bf16[2048,256]{1,0:T(8,128)(2,1)}, u32[]{:S(2)}) copy-start(bf16[2048,256]{1,0:T(8,128)(2,1)} %param.28) | copy-start | bytes 3145732
  6.5 38.4 %all-gather.2.cloned.1.call-start = ((), (), s32[]{:S(2)}) async-start(), calls=%async_computation.1 | async-start | bytes 5242880 | tf_op jit(solution)/shard_map/all_gather | solution.py:87
  7.3 259.6 %reduce-scatter.2.cloned.1.call-start = ((), (), s32[]{:S(2)}) async-start(), calls=%async_computation.2 | async-start | bytes 5242880 | tf_op jit(solution)/shard_map/reduce_scatter | solution.py:201
  13.0 12.7 %copy-start.17 = (bf16[2048,128]{1,0:T(8,128)(2,1)S(1)}, bf16[2048,128]{1,0:T(8,128)(2,1)}, u32[]{:S(2)}) copy-start(bf16[2048,128]{1,0:T(8,128)(2,1)} %param.25) | copy-start | bytes 1572868
  13.0 13.7 %copy-start.18 = (bf16[2048,128]{1,0:T(8,128)(2,1)S(1)}, bf16[2048,128]{1,0:T(8,128)(2,1)}, u32[]{:S(2)}) copy-start(bf16[2048,128]{1,0:T(8,128)(2,1)} %param.26) | copy-start | bytes 1572868
  25.7 22.3 %copy-start.25 = (f32[2048]{0:T(1024)S(1)}, f32[2048]{0:T(1024)}, u32[]{:S(2)}) copy-start(f32[2048]{0:T(1024)} %param.21) | copy-start | bytes 24580
  60.4 129.1 %collective-permute-start.2 = (bf16[128,256]{1,0:T(8,128)(2,1)}, bf16[128,256]{1,0:T(8,128)(2,1)}, u32[]{:S(2)}, u32[]{:S(2)}) collective-permute-start(bf16[128,256]{1,0:T(8,128)(2,1)} %get-tuple-element.351), channel_id=1, source_target_pairs={{0,4},{4,8},{8,12},{12,16},{16,20},{20,24},{24,28},{1,5},{5,9},{9,... | collective-permute-start | bytes 196616 | tf_op jit(solution)/shard_map/ppermute | solution.py:23
  63.5 126.0 %collective-permute-start.3 = (bf16[128,256]{1,0:T(8,128)(2,1)}, bf16[128,256]{1,0:T(8,128)(2,1)}, u32[]{:S(2)}, u32[]{:S(2)}) collective-permute-start(bf16[128,256]{1,0:T(8,128)(2,1)} %get-tuple-element.352), channel_id=1, source_target_pairs={{4,0},{8,4},{12,8},{16,12},{20,16},{24,20},{28,24},{5,1},{9,5},{13... | collective-permute-start | bytes 196616 | tf_op jit(solution)/shard_map/ppermute | solution.py:26
  68.5 31.6 %copy-start.3 = (f32[2,2,64,128]{3,2,1,0:T(8,128)S(1)}, f32[2,2,64,128]{3,2,1,0:T(8,128)}, u32[]{:S(2)}) copy-start(f32[2,2,64,128]{3,2,1,0:T(8,128)} %param.31) | copy-start | bytes 393220
  100.1 79.7 %copy-start.6 = (f32[2,8,128,64]{2,1,3,0:T(8,128)S(1)}, f32[2,8,128,64]{2,1,3,0:T(8,128)}, u32[]{:S(2)}) copy-start(f32[2,8,128,64]{2,1,3,0:T(8,128)} %fusion.36) | copy-start | bytes 1572868
  101.5 5.3 %collective-permute-start = (bf16[2,64,128]{2,1,0:T(8,128)(2,1)}, bf16[2,64,128]{2,1,0:T(8,128)(2,1)S(1)}, u32[]{:S(2)}, u32[]{:S(2)}) collective-permute-start(bf16[2,64,128]{2,1,0:T(8,128)(2,1)} %get-tuple-element.504), channel_id=1, source_target_pairs={{4,0},{8,4},{12,8},{16,12},{20,16},{24,20},{28,24},{5,1},{9,5},{13... | collective-permute-start | bytes 98312 | tf_op jit(solution)/shard_map/while/body/eval_jaxpr/ppermute | solution.py:34
  103.7 5.8 %collective-permute-start.1 = (bf16[2,64,128]{2,1,0:T(8,128)(2,1)}, bf16[2,64,128]{2,1,0:T(8,128)(2,1)S(1)}, u32[]{:S(2)}, u32[]{:S(2)}) collective-permute-start(bf16[2,64,128]{2,1,0:T(8,128)(2,1)} %get-tuple-element.505), channel_id=1, source_target_pairs={{0,4},{4,8},{8,12},{12,16},{16,20},{20,24},{24,28},{1,5},{5,9},{9,... | collective-permute-start | bytes 98312 | tf_op jit(solution)/shard_map/while/body/eval_jaxpr/ppermute | solution.py:34
  112.3 5.3 %collective-permute-start = (bf16[2,64,128]{2,1,0:T(8,128)(2,1)}, bf16[2,64,128]{2,1,0:T(8,128)(2,1)S(1)}, u32[]{:S(2)}, u32[]{:S(2)}) collective-permute-start(bf16[2,64,128]{2,1,0:T(8,128)(2,1)} %get-tuple-element.504), channel_id=1, source_target_pairs={{4,0},{8,4},{12,8},{16,12},{20,16},{24,20},{28,24},{5,1},{9,5},{13... | collective-permute-start | bytes 98312 | tf_op jit(solution)/shard_map/while/body/eval_jaxpr/ppermute | solution.py:34
  114.4 5.8 %collective-permute-start.1 = (bf16[2,64,128]{2,1,0:T(8,128)(2,1)}, bf16[2,64,128]{2,1,0:T(8,128)(2,1)S(1)}, u32[]{:S(2)}, u32[]{:S(2)}) collective-permute-start(bf16[2,64,128]{2,1,0:T(8,128)(2,1)} %get-tuple-element.505), channel_id=1, source_target_pairs={{0,4},{4,8},{8,12},{12,16},{16,20},{20,24},{24,28},{1,5},{5,9},{9,... | collective-permute-start | bytes 98312 | tf_op jit(solution)/shard_map/while/body/eval_jaxpr/ppermute | solution.py:34
  123.0 5.3 %collective-permute-start = (bf16[2,64,128]{2,1,0:T(8,128)(2,1)}, bf16[2,64,128]{2,1,0:T(8,128)(2,1)S(1)}, u32[]{:S(2)}, u32[]{:S(2)}) collective-permute-start(bf16[2,64,128]{2,1,0:T(8,128)(2,1)} %get-tuple-element.504), channel_id=1, source_target_pairs={{4,0},{8,4},{12,8},{16,12},{20,16},{24,20},{28,24},{5,1},{9,5},{13... | collective-permute-start | bytes 98312 | tf_op jit(solution)/shard_map/while/body/eval_jaxpr/ppermute | solution.py:34
  126.1 5.8 %collective-permute-start.1 = (bf16[2,64,128]{2,1,0:T(8,128)(2,1)}, bf16[2,64,128]{2,1,0:T(8,128)(2,1)S(1)}, u32[]{:S(2)}, u32[]{:S(2)}) collective-permute-start(bf16[2,64,128]{2,1,0:T(8,128)(2,1)} %get-tuple-element.505), channel_id=1, source_target_pairs={{0,4},{4,8},{8,12},{12,16},{16,20},{20,24},{24,28},{1,5},{5,9},{9,... | collective-permute-start | bytes 98312 | tf_op jit(solution)/shard_map/while/body/eval_jaxpr/ppermute | solution.py:34
  134.6 5.3 %collective-permute-start = (bf16[2,64,128]{2,1,0:T(8,128)(2,1)}, bf16[2,64,128]{2,1,0:T(8,128)(2,1)S(1)}, u32[]{:S(2)}, u32[]{:S(2)}) collective-permute-start(bf16[2,64,128]{2,1,0:T(8,128)(2,1)} %get-tuple-element.504), channel_id=1, source_target_pairs={{4,0},{8,4},{12,8},{16,12},{20,16},{24,20},{28,24},{5,1},{9,5},{13... | collective-permute-start | bytes 98312 | tf_op jit(solution)/shard_map/while/body/eval_jaxpr/ppermute | solution.py:34
  136.6 5.8 %collective-permute-start.1 = (bf16[2,64,128]{2,1,0:T(8,128)(2,1)}, bf16[2,64,128]{2,1,0:T(8,128)(2,1)S(1)}, u32[]{:S(2)}, u32[]{:S(2)}) collective-permute-start(bf16[2,64,128]{2,1,0:T(8,128)(2,1)} %get-tuple-element.505), channel_id=1, source_target_pairs={{0,4},{4,8},{8,12},{12,16},{16,20},{20,24},{24,28},{1,5},{5,9},{9,... | collective-permute-start | bytes 98312 | tf_op jit(solution)/shard_map/while/body/eval_jaxpr/ppermute | solution.py:34
  145.1 5.3 %collective-permute-start = (bf16[2,64,128]{2,1,0:T(8,128)(2,1)}, bf16[2,64,128]{2,1,0:T(8,128)(2,1)S(1)}, u32[]{:S(2)}, u32[]{:S(2)}) collective-permute-start(bf16[2,64,128]{2,1,0:T(8,128)(2,1)} %get-tuple-element.504), channel_id=1, source_target_pairs={{4,0},{8,4},{12,8},{16,12},{20,16},{24,20},{28,24},{5,1},{9,5},{13... | collective-permute-start | bytes 98312 | tf_op jit(solution)/shard_map/while/body/eval_jaxpr/ppermute | solution.py:34
  147.0 5.8 %collective-permute-start.1 = (bf16[2,64,128]{2,1,0:T(8,128)(2,1)}, bf16[2,64,128]{2,1,0:T(8,128)(2,1)S(1)}, u32[]{:S(2)}, u32[]{:S(2)}) collective-permute-start(bf16[2,64,128]{2,1,0:T(8,128)(2,1)} %get-tuple-element.505), channel_id=1, source_target_pairs={{0,4},{4,8},{8,12},{12,16},{16,20},{20,24},{24,28},{1,5},{5,9},{9,... | collective-permute-start | bytes 98312 | tf_op jit(solution)/shard_map/while/body/eval_jaxpr/ppermute | solution.py:34
  155.6 5.3 %collective-permute-start = (bf16[2,64,128]{2,1,0:T(8,128)(2,1)}, bf16[2,64,128]{2,1,0:T(8,128)(2,1)S(1)}, u32[]{:S(2)}, u32[]{:S(2)}) collective-permute-start(bf16[2,64,128]{2,1,0:T(8,128)(2,1)} %get-tuple-element.504), channel_id=1, source_target_pairs={{4,0},{8,4},{12,8},{16,12},{20,16},{24,20},{28,24},{5,1},{9,5},{13... | collective-permute-start | bytes 98312 | tf_op jit(solution)/shard_map/while/body/eval_jaxpr/ppermute | solution.py:34
  157.5 5.8 %collective-permute-start.1 = (bf16[2,64,128]{2,1,0:T(8,128)(2,1)}, bf16[2,64,128]{2,1,0:T(8,128)(2,1)S(1)}, u32[]{:S(2)}, u32[]{:S(2)}) collective-permute-start(bf16[2,64,128]{2,1,0:T(8,128)(2,1)} %get-tuple-element.505), channel_id=1, source_target_pairs={{0,4},{4,8},{8,12},{12,16},{16,20},{20,24},{24,28},{1,5},{5,9},{9,... | collective-permute-start | bytes 98312 | tf_op jit(solution)/shard_map/while/body/eval_jaxpr/ppermute | solution.py:34
  166.1 5.3 %collective-permute-start = (bf16[2,64,128]{2,1,0:T(8,128)(2,1)}, bf16[2,64,128]{2,1,0:T(8,128)(2,1)S(1)}, u32[]{:S(2)}, u32[]{:S(2)}) collective-permute-start(bf16[2,64,128]{2,1,0:T(8,128)(2,1)} %get-tuple-element.504), channel_id=1, source_target_pairs={{4,0},{8,4},{12,8},{16,12},{20,16},{24,20},{28,24},{5,1},{9,5},{13... | collective-permute-start | bytes 98312 | tf_op jit(solution)/shard_map/while/body/eval_jaxpr/ppermute | solution.py:34
  168.0 5.8 %collective-permute-start.1 = (bf16[2,64,128]{2,1,0:T(8,128)(2,1)}, bf16[2,64,128]{2,1,0:T(8,128)(2,1)S(1)}, u32[]{:S(2)}, u32[]{:S(2)}) collective-permute-start(bf16[2,64,128]{2,1,0:T(8,128)(2,1)} %get-tuple-element.505), channel_id=1, source_target_pairs={{0,4},{4,8},{8,12},{12,16},{16,20},{20,24},{24,28},{1,5},{5,9},{9,... | collective-permute-start | bytes 98312 | tf_op jit(solution)/shard_map/while/body/eval_jaxpr/ppermute | solution.py:34
  175.2 6.6 %copy-start.8 = (bf16[8,128,2,128]{1,3,0,2:T(8,128)(2,1)S(1)}, bf16[8,128,2,128]{1,3,0,2:T(8,128)(2,1)}, u32[]{:S(2)}) copy-start(bf16[8,128,2,128]{1,3,0,2:T(8,128)(2,1)} %copy.46) | copy-start | bytes 1572868
  175.2 6.6 %copy-start.21 = (f32[2,8,128]{2,1,0:T(8,128)S(1)}, f32[2,8,128]{2,1,0:T(8,128)}, u32[]{:S(2)}) copy-start(f32[2,8,128]{2,1,0:T(8,128)} %get-tuple-element.374) | copy-start | bytes 24580
  177.9 5.4 %copy-start.22 = (f32[8,128,2]{1,0,2:T(8,128)S(1)}, f32[8,128,2]{1,0,2:T(8,128)}, u32[]{:S(2)}) copy-start(f32[8,128,2]{1,0,2:T(8,128)} %get-tuple-element.369) | copy-start | bytes 24580
  183.2 6.4 %copy-start.7 = (bf16[1024,256]{1,0:T(8,128)(2,1)S(1)}, bf16[1024,256]{1,0:T(8,128)(2,1)}, u32[]{:S(2)}) copy-start(bf16[1024,256]{1,0:T(8,128)(2,1)} %get-tuple-element.348) | copy-start | bytes 1572868
  183.3 8.2 %copy-start.9 = (pred[512,768]{0,1:T(8,128)(4,1)S(1)}, pred[512,768]{0,1:T(8,128)(4,1)}, u32[]{:S(2)}) copy-start(pred[512,768]{0,1:T(8,128)(4,1)} %fusion.14) | copy-start | bytes 1179652
  199.3 5.8 %slice-start = ((s8[6291456]{0:T(1024)(128)(4,1)}), s8[2097152]{0:T(1024)(128)(4,1)S(1)}, s32[]{:S(2)}) async-start(s8[6291456]{0:T(1024)(128)(4,1)} %bitcast.191), calls=%async_computation.3 | async-start | bytes 4194304
  (26 other events, 60.4 us)
Sparse Core Ops, SparseCore 0:
  8.9 35.9 all-gather.1
  213.1 53.7 reduce-scatter.1
where the time goes:
time: 278 us; the launch traced here: 274 us
  waiting for transfers between devices  87.9 us (32%)
  other arithmetic  47.7 us (17%)
  local copies, waits for them, and re-layouts  44.6 us (16%)
  starting transfers between devices  43.3 us (16%)
  matrix products  35.8 us (13%)
  between operations  14 us (5%)
    reduce_scatter x1, waiting for transfers between devices, body(): lax.psum_scatter((att_part + lax.dot_general(out_ret, ret_out, contract_d...  53.9 us
    ppermute x14, starting transfers between devices, passed_along(): return lax.ppermute(value, axis, pairs)  36.9 us
    ppermute x14, waiting for transfers between devices, passed_along(): return lax.ppermute(value, axis, pairs)  18.3 us
    all_gather x1, waiting for transfers between devices, body(): lax.all_gather(tokens, 'tp', axis=1, tiled=True).astype(jnp.float32)  15 us
    add x16, other arithmetic, advance(): return (factor_now[:, None, None] * state_now + term_now, state_now)  14.6 us
    unnamed x62, local copies, waits for them, and re-layouts  12.4 us
    mul x16, local copies, waits for them, and re-layouts, advance(): return (factor_now[:, None, None] * state_now + term_now, state_now)  11.1 us
    convert_element_type x7, other arithmetic, relay(): (device_factor[:, None, None] * bwd_now + bwd_total).astype(jnp.bfloat16)  9.74 us
  transfers between devices with their start and end apart: 18, of which 9 were waited for; matrix products, arithmetic and copies ran while one was open for 31% of the time, Pallas kernels for 0%

commit v1 on v0

v1 whole, which is shorter than its diff:
```python
import functools

import jax
import jax.numpy as jnp
import numpy as np
from jax import lax
from jax.experimental import pallas as pl
from jax.experimental.pallas import tpu as pltpu
from jax.sharding import PartitionSpec as P

HD = 64
RK = 64
RV = 128
WINDOW = 128
NORM_EPS = 1e-06
ROPE_BASE = 10000.0
NEG = -1e30
EXTRA = 16
CHUNKS = 4
F32 = jnp.float32
BF16 = jnp.bfloat16

VMEM = pl.BlockSpec(memory_space=pltpu.VMEM)
SMEM = pl.BlockSpec(memory_space=pltpu.SMEM)
ANY = pl.BlockSpec(memory_space=pl.ANY)


def cost(flops, nbytes):
    return pl.CostEstimate(flops=int(flops), bytes_accessed=int(nbytes), transcendentals=0)


def dot(a, b):
    return jnp.dot(a, b, preferred_element_type=F32)


def dot_t(a, b):
    return lax.dot_general(a, b, (((1,), (1,)), ((), ())), preferred_element_type=F32)


def t_dot(a, b):
    return lax.dot_general(a, b, (((0,), (0,)), ((), ())), preferred_element_type=F32)


def project_kernel(n_blocks, n_w, parts, *refs):
    idx_ref, gain_ref = refs[:2]
    blocks = refs[2 : 2 + n_blocks]
    cos_ref, sin_ref, perm_ref = refs[2 + n_blocks : 5 + n_blocks]
    w_refs = refs[5 + n_blocks : 5 + n_blocks + n_w]
    out_ref = refs[5 + n_blocks + n_w]
    xn, wbuf, sems = refs[-3:]
    width = blocks[0].shape[1]
    copies = []
    for w_ref, (group, low) in zip(w_refs, parts):
        dst = wbuf.at[group]
        if w_ref.shape[1] != wbuf.shape[2]:
            dst = wbuf.at[group, :, pl.ds(low, w_ref.shape[1])]
        copy = pltpu.make_async_copy(w_ref, dst, sems.at[group])
        copy.start()
        copies.append(copy)
    rows = xn.shape[0]
    squares = jnp.zeros((rows, 1), F32)
    for i, block in enumerate(blocks):
        start = pl.multiple_of(idx_ref[i] * width, width)
        values = block[...].astype(F32)
        squares = squares + jnp.sum(values * values, axis=1, keepdims=True)
        xn[:, pl.ds(start, width)] = (values * gain_ref[:, pl.ds(start, width)]).astype(BF16)
    inv = lax.rsqrt(squares / (width * n_blocks) + NORM_EPS)

    def group_step(group, carry):
        pltpu.make_async_copy(wbuf.at[group], wbuf.at[group], sems.at[group]).wait()
        scale = jnp.where(group == 0, HD ** (-0.5), 1.0).astype(F32)
        out_ref[group] = (dot(xn[...], wbuf[group]) * inv).astype(BF16) * scale.astype(BF16)
        return carry

    lax.fori_loop(0, out_ref.shape[0], group_step, 0)
    raw = out_ref[2]
    turned = raw.astype(F32) * cos_ref[...] + dot(raw, perm_ref[...]) * sin_ref[...]
    out_ref[2] = turned.astype(BF16)


def project(idx, gain, blocks, cos, sin, perm, weights, parts, chunk, rows, interpret_width):
    group_width = interpret_width
    depth = gain.shape[1]
    in_specs = [SMEM, VMEM]
    for block in blocks:
        pick = chunk if block.shape[0] != rows else 0
        in_specs.append(pl.BlockSpec((rows, block.shape[1]), lambda i, pick=pick: (pick, 0)))
    for _ in range(2):
        in_specs.append(pl.BlockSpec((rows, group_width), lambda i: (chunk, 0)))
    in_specs.append(VMEM)
    in_specs += [ANY] * len(weights)
    return pl.pallas_call(
        functools.partial(project_kernel, len(blocks), len(weights), parts),
        grid=(1,),
        out_shape=jax.ShapeDtypeStruct((5, rows, group_width), BF16),
        in_specs=in_specs,
        out_specs=pl.BlockSpec((5, rows, group_width), lambda i: (0, 0, 0)),
        scratch_shapes=[
            pltpu.VMEM((rows, depth), BF16),
            pltpu.VMEM((5, depth, group_width), BF16),
            pltpu.SemaphoreType.DMA((5,)),
        ],
        cost_estimate=cost(2 * rows * depth * 5 * group_width // 4, 7 << 20),
        name="project",
    )(idx, gain, *blocks, cos, sin, perm, *weights)


def attend_kernel(n_chunks, kv_local, groups, seq_len, *refs):
    offset_ref, sink_ref = refs[:2]
    q_refs = refs[2 : 2 + n_chunks]
    kv_refs = refs[2 + n_chunks : 2 + 2 * n_chunks]
    low_ref, high_ref, out_ref = refs[2 + 2 * n_chunks : 5 + 2 * n_chunks]
    qbuf, kvbuf = refs[-2:]
    rows = q_refs[0].shape[1]
    total = rows * n_chunks
    kv_cols = kv_local * HD
    kvbuf[0:WINDOW] = low_ref[...]
    for c in range(n_chunks):
        kvbuf[pl.ds(WINDOW + c * rows, rows)] = kv_refs[c][0]
        qbuf[pl.ds(c * rows, rows)] = q_refs[c][0]
    kvbuf[pl.ds(WINDOW + total, WINDOW)] = high_ref[...]
    block = WINDOW
    span = block + 2 * WINDOW
    row = lax.broadcasted_iota(jnp.int32, (block, span), 0)
    col = lax.broadcasted_iota(jnp.int32, (block, span), 1)
    band = (col >= row) & (col <= row + 2 * WINDOW)

    def step(i, carry):
        first = pl.multiple_of(i * block, block)
        q = qbuf[pl.ds(first, block)]
        kv = kvbuf[pl.ds(first, span)]
        pos = col + (offset_ref[0] + first - WINDOW)
        allowed = band & (pos >= 0) & (pos < seq_len)
        outs = []
        for g in range(kv_local):
            k = kv[:, g * HD : (g + 1) * HD]
            v = kv[:, kv_cols + g * HD : kv_cols + (g + 1) * HD]
            vo = jnp.concatenate([v, jnp.ones((span, 128 - HD), BF16)], axis=1)
            for j in range(groups):
                h = g * groups + j
                s = jnp.where(allowed, dot_t(q[:, h * HD : (h + 1) * HD], k), NEG)
                sink = sink_ref[h]
                top = jnp.maximum(jnp.max(s, axis=1, keepdims=True), sink)
                p = jnp.exp(s - top).astype(BF16)
                o = dot(p, vo)
                den = o[:, HD : HD + 1] + jnp.exp(sink - top)
                outs.append(o[:, :HD] / den)
        out_ref[pl.ds(first, block)] = jnp.concatenate(outs, axis=1).astype(BF16)
        return carry

    lax.fori_loop(0, total // block, step, 0)


def group_spec(group, rows, width):
    return pl.BlockSpec((1, rows, width), lambda i: (group, 0, 0))


def attend(offset, sink, proj, low, high, kv_local, groups, seq_len):
    n = len(proj)
    _, rows, width = proj[0].shape
    total = rows * n
    return pl.pallas_call(
        functools.partial(attend_kernel, n, kv_local, groups, seq_len),
        grid=(1,),
        out_shape=jax.ShapeDtypeStruct((total, width), BF16),
        in_specs=[SMEM, SMEM]
        + [group_spec(0, rows, width)] * n
        + [group_spec(1, rows, width)] * n
        + [VMEM, VMEM],
        out_specs=pl.BlockSpec((total, width), lambda i: (0, 0)),
        scratch_shapes=[
            pltpu.VMEM((total, width), BF16),
            pltpu.VMEM((total + 2 * WINDOW, width), BF16),
        ],
        cost_estimate=cost(1.5e9, 3 << 20),
        name="attend",
    )(offset, sink, *proj, *proj, low, high)


def totals_kernel(n_chunks, ret_local, n_sp, *refs):
    me_ref, ccol_ref, end_ref = refs[:3]
    r_refs = refs[3 : 3 + n_chunks]
    v_refs = refs[3 + n_chunks : 3 + 2 * n_chunks]
    out_ref = refs[-1]
    rows = r_refs[0].shape[1]
    sums = [jnp.zeros((RK, 2 * RV), F32) for _ in range(ret_local)]
    for c in range(n_chunks):
        k_all = r_refs[c][0]
        v_all = v_refs[c][0]
        for h in range(ret_local):
            col = ccol_ref[pl.ds(c * rows, rows), h : h + 1]
            v = v_all[:, h * RV : (h + 1) * RV].astype(F32)
            both = jnp.concatenate(
                [v * jnp.exp(end_ref[h] - col), v * jnp.exp(col)], axis=1
            ).astype(BF16)
            k = k_all[:, (ret_local + h) * RK : (ret_local + h + 1) * RK]
            sums[h] = sums[h] + t_dot(k, both)
    me = me_ref[0]
    line = lax.broadcasted_iota(jnp.int32, (EXTRA, RV), 0)
    for h in range(ret_local):
        end = jnp.full((EXTRA, RV), end_ref[h], F32)
        d0 = end.astype(BF16).astype(F32)
        d1 = (end - d0).astype(BF16).astype(F32)
        d2 = end - d0 - d1
        extra = jnp.where(line == 0, d0, jnp.where(line == 1, d1, jnp.where(line == 2, d2, 0.0)))
        fwd = jnp.concatenate([sums[h][:, :RV], extra], axis=0).astype(BF16)
        bwd = jnp.concatenate([sums[h][:, RV:], extra], axis=0).astype(BF16)
        for j in range(n_sp):
            out_ref[j, h] = jnp.where(j > me, fwd, bwd)


def totals(me, ccol, end, proj, ret_local, n_sp):
    n = len(proj)
    _, rows, width = proj[0].shape
    return pl.pallas_call(
        functools.partial(totals_kernel, n, ret_local, n_sp),
        grid=(1,),
        out_shape=jax.ShapeDtypeStruct((n_sp, ret_local, RK + EXTRA, RV), BF16),
        in_specs=[SMEM, VMEM, SMEM]
        + [group_spec(2, rows, width)] * n
        + [group_spec(3, rows, width)] * n,
        out_specs=pl.BlockSpec((n_sp, ret_local, RK + EXTRA, RV), lambda i: (0, 0, 0, 0)),
        cost_estimate=cost(0.3e9, 2 << 20),
        name="totals",
    )(me, ccol, end, *proj, *proj)


def local_kernel(n_chunks, ret_local, *refs):
    ccol_ref, crow_ref = refs[:2]
    r_refs = refs[2 : 2 + n_chunks]
    v_refs = refs[2 + n_chunks : 2 + 2 * n_chunks]
    out_ref = refs[2 + 2 * n_chunks]
    rbuf, vbuf = refs[-2:]
    rows = r_refs[0].shape[1]
    total = rows * n_chunks
    for c in range(n_chunks):
        rbuf[pl.ds(c * rows, rows)] = r_refs[c][0]
        vbuf[pl.ds(c * rows, rows)] = v_refs[c][0]
    block = min(128, rows)

    def step(i, carry):
        first = pl.multiple_of(i * block, block)
        for h in range(ret_local):
            q = rbuf[pl.ds(first, block), h * RK : (h + 1) * RK]
            k = rbuf[:, (ret_local + h) * RK : (ret_local + h + 1) * RK]
            gap = ccol_ref[pl.ds(first, block), h : h + 1] - crow_ref[h : h + 1, :]
            w = (dot_t(q, k) * jnp.exp(-jnp.abs(gap))).astype(BF16)
            out_ref[pl.ds(first, block), h * RV : (h + 1) * RV] = dot(
                w, vbuf[:, h * RV : (h + 1) * RV]
            )
        return carry

    lax.fori_loop(0, total // block, step, 0)


def local(ccol, crow, proj, ret_local):
    n = len(proj)
    _, rows, width = proj[0].shape
    total = rows * n
    return pl.pallas_call(
        functools.partial(local_kernel, n, ret_local),
        grid=(1,),
        out_shape=jax.ShapeDtypeStruct((total, width), F32),
        in_specs=[VMEM, VMEM]
        + [group_spec(2, rows, width)] * n
        + [group_spec(3, rows, width)] * n,
        out_specs=pl.BlockSpec((total, width), lambda i: (0, 0)),
        scratch_shapes=[pltpu.VMEM((total, width), BF16), pltpu.VMEM((total, width), BF16)],
        cost_estimate=cost(1e9, 3 << 20),
        name="local",
    )(ccol, crow, *proj, *proj)


def cross_kernel(n_chunks, ret_local, n_sp, *refs):
    me_ref, end_ref, ccol_ref, got_ref, init_ref, loc_ref = refs[:6]
    r_refs = refs[6 : 6 + n_chunks]
    g_refs = refs[6 + n_chunks : 6 + 2 * n_chunks]
    out_ref = refs[-1]
    rows = r_refs[0].shape[1]
    me = me_ref[0]
    for h in range(ret_local):
        ends = []
        for j in range(n_sp):
            tail = got_ref[j, h, RK : RK + EXTRA, :].astype(F32)
            ends.append(jnp.sum(tail, axis=0, keepdims=True))
        fwd = jnp.zeros((RK, RV), F32)
        run = jnp.zeros((1, RV), F32)
        for j in range(n_sp - 1, -1, -1):
            here = j < me
            term = jnp.exp(run) * got_ref[j, h, 0:RK, :].astype(F32)
            fwd = fwd + jnp.where(here, term, 0.0)
            run = run + jnp.where(here, ends[j], 0.0)
        fwd = fwd + jnp.exp(run) * init_ref[0, h]
        bwd = jnp.zeros((RK, RV), F32)
        run = jnp.zeros((1, RV), F32)
        for j in range(n_sp):
            here = j > me
            term = jnp.exp(run) * got_ref[j, h, 0:RK, :].astype(F32)
            bwd = bwd + jnp.where(here, term, 0.0)
            run = run + jnp.where(here, ends[j], 0.0)
        bwd = bwd + jnp.exp(run) * init_ref[1, h]
        state = jnp.concatenate([fwd, bwd], axis=1).astype(BF16)
        for c in range(n_chunks):
            here = pl.ds(c * rows, rows)
            q = r_refs[c][0, :, h * RK : (h + 1) * RK]
            both = dot(q, state)
            col = ccol_ref[here, h : h + 1]
            ret = (
                loc_ref[here, h * RV : (h + 1) * RV]
                + jnp.exp(col) * both[:, :RV]
                + jnp.exp(end_ref[h] - col) * both[:, RV:]
            )
            centered = ret - jnp.mean(ret, axis=1, keepdims=True)
            scale = lax.rsqrt(jnp.mean(centered * centered, axis=1, keepdims=True) + NORM_EPS)
            gate = g_refs[c][0, :, h * RV : (h + 1) * RV].astype(F32)
            gated = gate / (1.0 + jnp.exp(-gate))
            out_ref[here, h * RV : (h + 1) * RV] = (gated * (centered * scale)).astype(BF16)


def cross(me, end, ccol, got, init, loc, proj, ret_local, n_sp):
    n = len(proj)
    _, rows, width = proj[0].shape
    total = rows * n
    return pl.pallas_call(
        functools.partial(cross_kernel, n, ret_local, n_sp),
        grid=(1,),
        out_shape=jax.ShapeDtypeStruct((total, width), BF16),
        in_specs=[SMEM, SMEM, VMEM, VMEM, VMEM, VMEM]
        + [group_spec(2, rows, width)] * n
        + [group_spec(4, rows, width)] * n,
        out_specs=pl.BlockSpec((total, width), lambda i: (0, 0)),
        cost_estimate=cost(0.5e9, 4 << 20),
        name="cross",
    )(me, end, ccol, got, init, loc, *proj, *proj)


def output_kernel(n_src, *refs):
    att = refs[:n_src]
    ret = refs[n_src : 2 * n_src]
    weights = refs[2 * n_src : 3 * n_src]
    out_ref = refs[3 * n_src]
    width = att[0].shape[1]
    total = jnp.zeros(out_ref.shape, F32)
    for a, r, w in zip(att, ret, weights):
        total = total + dot(a[...], w[0:width]) + dot(r[...], w[width : 2 * width])
    out_ref[...] = total.astype(BF16)


def output(att, ret, weights):
    n_src = len(att)
    total, width = att[0].shape
    cols = weights[0].shape[1]
    rows = min(256, total)
    data = pl.BlockSpec((rows, width), lambda i: (i, 0))
    return pl.pallas_call(
        functools.partial(output_kernel, n_src),
        grid=(total // rows,),
        out_shape=jax.ShapeDtypeStruct((total, cols), BF16),
        in_specs=[data] * (2 * n_src) + [VMEM] * n_src,
        out_specs=pl.BlockSpec((rows, cols), lambda i: (i, 0)),
        cost_estimate=cost(1e9, 8 << 20),
        name="output",
    )(*att, *ret, *weights)


def core_swap(value):
    n = lax.axis_size("tp")
    return lax.ppermute(value, "tp", [(i, i ^ 1) for i in range(n)])


def chip_turn(value, by):
    n = lax.axis_size("tp")
    return lax.ppermute(value, "tp", [(i, (i + 2 * by) % n) for i in range(n)])


def gather_tp(value):
    blocks = [value, core_swap(value)]
    for by in range(1, lax.axis_size("tp") // 2):
        far = chip_turn(value, by)
        blocks += [far, core_swap(far)]
    return blocks


def sources():
    n = lax.axis_size("tp")
    me = lax.axis_index("tp")
    out = [me, me ^ 1]
    for by in range(1, n // 2):
        far = (me + n - 2 * by) % n
        out += [far, far ^ 1]
    return out


def output_weights(out_att, out_ret):
    n_tp, n_sp = lax.axis_size("tp"), lax.axis_size("sp")
    tp, sp = lax.axis_index("tp"), lax.axis_index("sp")
    stacked = jnp.concatenate([out_att, out_ret], axis=0)
    depth, model = stacked.shape
    cols = model // n_tp
    own = lax.dynamic_slice_in_dim(stacked, tp * cols, cols, axis=1)
    peer = core_swap(lax.dynamic_slice_in_dim(stacked, (tp ^ 1) * cols, cols, axis=1))
    share = depth // n_sp
    slab = lax.dynamic_slice_in_dim(stacked, sp * share, share, axis=0)
    slab = jnp.transpose(slab.reshape(share, n_tp, cols), (1, 0, 2))
    slab = lax.all_to_all(slab, "tp", 0, 0, tiled=True)
    far = sources()[2:]
    mine = jnp.concatenate([lax.dynamic_slice_in_dim(slab, s, 1, axis=0) for s in far], axis=0)
    spread = jnp.broadcast_to(mine[None], (n_sp,) + mine.shape)
    spread = lax.all_to_all(spread, "sp", 0, 0, tiled=True)
    spread = jnp.transpose(spread, (1, 0, 2, 3)).reshape(len(far), depth, cols)
    return [own, peer] + [spread[i] for i in range(len(far))]


def body(
    tokens,
    norm_gain,
    att_query,
    att_key,
    att_value,
    ret_query,
    ret_key,
    ret_value,
    ret_gate,
    att_sink,
    decay_log,
    init_state,
    out_att,
    out_ret,
):
    n_sp = lax.axis_size("sp")
    me = lax.axis_index("sp")
    total = tokens.shape[0]
    seq_len = total * n_sp
    width = att_query.shape[1]
    half = width // 2
    kv_local = att_key.shape[1] // HD
    groups = att_sink.shape[0] // kv_local
    ret_local = decay_log.shape[0]
    rows = total // CHUNKS

    pieces = [tokens[c * rows : (c + 1) * rows] for c in range(CHUNKS)]
    order = [0, CHUNKS - 1] + list(range(1, CHUNKS - 1))
    near = core_swap(tokens)
    far = {c: [] for c in order}
    for c in order:
        for by in range(1, lax.axis_size("tp") // 2):
            block = chip_turn(pieces[c], by)
            far[c] += [block, core_swap(block)]
    idx = jnp.stack(sources()).astype(jnp.int32)

    position = (me * total + jnp.arange(total, dtype=jnp.int32)).astype(F32)
    inverse = ROPE_BASE ** (-2.0 * jnp.arange(RK // 2, dtype=F32) / RK)
    angles = position[:, None] * inverse[None, :]
    cos, sin = lax.optimization_barrier((jnp.cos(angles), jnp.sin(angles)))
    key_scale = RK ** (-0.5)
    cos = jnp.concatenate([cos] * (2 * ret_local) + [cos * key_scale] * (2 * ret_local), axis=1)
    sin = jnp.concatenate(
        [-sin, sin] * ret_local + [-sin * key_scale, sin * key_scale] * ret_local, axis=1
    )
    lane = np.arange(width)
    perm = np.zeros((width, width), np.float32)
    perm[lane ^ (RK // 2), lane] = 1.0
    perm = jnp.asarray(perm, BF16)

    if half % 128 == 0:
        weights = [att_query, att_key, att_value, ret_query, ret_key, ret_value, ret_gate]
        parts = [(0, 0), (1, 0), (1, half), (2, 0), (2, half), (3, 0), (4, 0)]
    else:
        weights = [
            att_query,
            jnp.concatenate([att_key, att_value], axis=1),
            jnp.concatenate([ret_query, ret_key], axis=1),
            ret_value,
            ret_gate,
        ]
        parts = [(i, 0) for i in range(5)]
    gain = norm_gain[None, :]
    proj = [None] * CHUNKS
    for c in order:
        blocks = [tokens, near] + far[c]
        proj[c] = project(idx, gain, blocks, cos, sin, perm, weights, parts, c, rows, width)

    forward = [(i, (i + 1) % n_sp) for i in range(n_sp)]
    backward = [(target, source) for source, target in forward]
    low = lax.ppermute(proj[-1][1, rows - WINDOW :], "sp", forward)
    high = lax.ppermute(proj[0][1, :WINDOW], "sp", backward)

    crow = jnp.cumsum(decay_log, axis=1)
    ccol = crow.T
    end = crow[:, -1]
    me_arr = me.reshape(1).astype(jnp.int32)
    offset = (me * total).reshape(1).astype(jnp.int32)

    sent = totals(me_arr, ccol, end, proj, ret_local, n_sp)
    got = lax.all_to_all(sent, "sp", 0, 0, tiled=True)
    attended = attend(offset, att_sink, proj, low, high, kv_local, groups, seq_len)
    att_blocks = gather_tp(attended)
    loc = local(ccol, crow, proj, ret_local)
    kept = cross(me_arr, end, ccol, got, init_state, loc, proj, ret_local, n_sp)
    ret_blocks = gather_tp(kept)
    out_w = output_weights(out_att, out_ret)
    return output(att_blocks, ret_blocks, out_w)


def solution(mesh):
    in_specs = (
        P("sp", "tp"),
        P(),
        P(None, "tp"),
        P(None, "tp"),
        P(None, "tp"),
        P(None, "tp"),
        P(None, "tp"),
        P(None, "tp"),
        P(None, "tp"),
        P("tp"),
        P("tp", "sp"),
        P(None, "tp", None, None),
        P("tp", None),
        P("tp", None),
    )
    out_specs = P("sp", "tp")
    return jax.shard_map(body, mesh=mesh, in_specs=in_specs, out_specs=out_specs, check_vma=False)
```

time: 278 us -> 165 us (0.59); the launches traced: 274 us -> 164 us
  Pallas kernels: 0 us -> 59.2 us
  waiting for transfers between devices: 87.9 us -> 41.5 us
  other arithmetic: 47.7 us -> 4.66 us
  matrix products: 35.8 us -> 0 us
  local copies, waits for them, and re-layouts: 44.6 us -> 26.9 us
  between operations: 14 us -> 0.26 us
  starting transfers between devices: 43.3 us -> 31.5 us
    pallas_call x0 -> x9, Pallas kernels: none -> 59.2 us  [the longest x4 24 us: project(): pl.pallas_call(functools.partial(project_kernel, len(blocks), len(weights...]
    reduce_scatter x1 -> x0, waiting for transfers between devices: 53.9 us -> none  [body(): lax.psum_scatter((att_part + lax.dot_general(out_ret, ret_out, contract_d...]
    dot_general x13 -> x0, matrix products: 35.8 us -> none  [the longest x1 8.93 us: body(): proj_sums = jnp.dot(scaled, joined, preferred_element_type=jnp.float32)]
    ppermute x16 -> x18, starting transfers between devices: 43.2 us -> 16 us  [the longest x10 9.12 us: core_swap(): return lax.ppermute(value, 'tp', [(i, i ^ 1) for i in range(n)])]
    add x23 -> x0, other arithmetic: 15.7 us -> none  [the longest x16 14.6 us: advance(): return (factor_now[:, None, None] * state_now + term_now, state_now)]
    all_to_all x0 -> x3, starting transfers between devices: none -> 15.5 us  [the longest x1 5.58 us: body(): got = lax.all_to_all(sent, 'sp', 0, 0, tiled=True)]
    ppermute x16 -> x18, waiting for transfers between devices: 18.3 us -> 33.7 us  [the longest x6 18.6 us: chip_turn(): return lax.ppermute(value, 'tp', [(i, (i + 2 * by) % n) for i in range(n)])]
    all_gather x1 -> x0, waiting for transfers between devices: 15 us -> none  [body(): lax.all_gather(tokens, 'tp', axis=1, tiled=True).astype(jnp.float32)]
  transfers between devices with their start and end apart: 18 -> 21, of which waited for: 9 -> 7; matrix products, arithmetic and copies ran while one was open for 31% -> 17% of each run, Pallas kernels for 0% -> 32%
where the time goes in v1:
time: 165 us; the launch traced here: 164 us
  Pallas kernels  59.2 us (36%)
  waiting for transfers between devices  41.5 us (25%)
  starting transfers between devices  31.5 us (19%)
  local copies, waits for them, and re-layouts  26.9 us (16%)
  other arithmetic  4.66 us (3%)
    pallas_call x4, Pallas kernels, project(): pl.pallas_call(functools.partial(project_kernel, len(blocks), len(weights...  24 us
    ppermute x6, waiting for transfers between devices, chip_turn(): return lax.ppermute(value, 'tp', [(i, (i + 2 * by) % n) for i in range(n)])  18.6 us
    ppermute x1, waiting for transfers between devices, body(): low = lax.ppermute(proj[-1][1, rows - WINDOW:], 'sp', forward)  14.3 us
    pallas_call x1, Pallas kernels, attend(): pl.pallas_call(functools.partial(attend_kernel, n, kv_local, groups, seq_...  13.1 us
    ppermute x10, starting transfers between devices, core_swap(): return lax.ppermute(value, 'tp', [(i, i ^ 1) for i in range(n)])  9.12 us
    all_to_all x1, waiting for transfers between devices, body(): got = lax.all_to_all(sent, 'sp', 0, 0, tiled=True)  7.8 us
    pallas_call x1, Pallas kernels, local(): pl.pallas_call(functools.partial(local_kernel, n, ret_local), grid=(1,),...  7.26 us
    pallas_call x1, Pallas kernels, output(): pl.pallas_call(functools.partial(output_kernel, n_src), grid=(total // ro...  6.35 us
  transfers between devices with their start and end apart: 21, of which 7 were waited for; matrix products, arithmetic and copies ran while one was open for 17% of the time, Pallas kernels for 32%

profile of v1, /device:TPU:17, one launch (start us, length us, event | category | flops | bytes accessed | tf_op | source)
XLA Modules:
  0.0 164.0 jit_solution(1661327584400911490)
XLA Ops:
  0.7 2.2 %fusion.1 = (bf16[256,512]{1,0:T(8,128)(2,1)}, bf16[256,512]{1,0:T(8,128)(2,1)}, bf16[256,512]{1,0:T(8,128)(2,1)}, bf16[256,512]{1,0:T(8,128)(2,1)}) fusion(bf16[1024,512]{1,0:T(8,128)(2,1)} %refs_2_.7), kind=kLoop, calls=%fused_computation.23 | loop fusion | bytes 2097152 | tf_op jit(solution)/shard_map/slice | solution.py:441
  2.9 1.2 collective-permute-start.7
  4.4 1.2 collective-permute-start.3
  5.8 1.3 constant_dynamic-update-slice_fusion.1
  7.1 1.3 constant_dynamic-update-slice_fusion
  9.6 1.7 %copy.23 = bf16[4,64,512]{2,1,0:T(8,128)(2,1)} copy(bf16[4,64,512]{2,0,1:T(4,128)(2,1)} %bitcast.33) | data formatting | bytes 524288 | tf_op jit(solution)/shard_map/transpose | solution.py:404
  11.3 4.5 %all-to-all-start.1 = ((bf16[4,64,512]{2,1,0:T(8,128)(2,1)}), bf16[4,64,512]{2,1,0:T(8,128)(2,1)S(1)}, u32[]{:S(2)}, u32[]{:S(2)}) async-start(bf16[4,64,512]{2,1,0:T(8,128)(2,1)} %copy.23), calls=%async_computation.1 | async-start | bytes 524288 | tf_op jit(solution)/shard_map/all_to_all | solution.py:405
  16.8 1.9 %multiply_sine_fusion = (f32[1024,32]{1,0:T(8,128)S(1)}, f32[1024,32]{1,0:T(8,128)S(1)}) fusion(f32[32]{0:T(128)S(1)} %multiply_power_fusion, f32[1024]{0:T(1024)S(1)} %add_convert_fusion), kind=kLoop, calls=%fused_computation | loop fusion | flops 32768 | bytes 266368 | tf_op jit(solution)/shard_map/sin | solution.py:454
  20.8 1.5 collective-permute-done.3.refs_4_
  22.3 1.3 collective-permute-start.4
  23.6 4.3 %collective-permute-done.1.refs_4_ = bf16[256,512]{1,0:T(8,128)(2,1)} collective-permute-done((bf16[256,512]{1,0:T(8,128)(2,1)}, bf16[256,512]{1,0:T(8,128)(2,1)}, u32[]{:S(2)}, u32[]{:S(2)}) %collective-permute-start.1) | collective-permute-done | bytes 262176 | tf_op jit(solution)/shard_map/ppermute | solution.py:373
  27.9 1.3 collective-permute-start.2
  30.5 4.2 %concatenate.12.refs_6_ = f32[1024,256]{1,0:T(8,128)} concatenate(f32[1024,32]{1,0:T(8,128)S(1)} %get-tuple-element.7, f32[1024,32]{1,0:T(8,128)S(1)} %get-tuple-element.7, f32[1024,32]{1,0:T(8,128)S(1)} %get-tuple-element.7, f32[1024,32]{1,0:T(8,128)S(1)} %get-tuple-element.7, f32[1024,32]{1,0:T(8,128)S(1)} %broadcast_multiply_fusion.2, ...), dimensions={1} | concatenate | bytes 2097152 | tf_op jit(solution)/shard_map/concatenate | solution.py:456
  34.6 4.6 %concatenate.13.refs_7_ = f32[1024,256]{1,0:T(8,128)} concatenate(f32[1024,32]{1,0:T(8,128)} %get-tuple-element.19, f32[1024,32]{1,0:T(8,128)S(1)} %get-tuple-element.8, f32[1024,32]{1,0:T(8,128)} %get-tuple-element.19, f32[1024,32]{1,0:T(8,128)S(1)} %get-tuple-element.8, f32[1024,32]{1,0:T(8,128)} %get-tuple-element.18, f32[1024,32]{1,0:T(8,128)} %get-tuple-element.17, ...), dimensions={1} | concatenate | bytes 2097152 | tf_op jit(solution)/shard_map/concatenate | solution.py:457
  40.2 6.0 %project.7.refs_5_.refs_9_.refs_6_.refs_10_.refs_13_ = bf16[5,256,256]{2,1,0:T(8,128)(2,1)} custom-call(s32[4]{0:T(128)} %pad_add_fusion.refs_0_, f32[1,2048]{1,0:T(1,128)} %bitcast.34, bf16[1024,512]{1,0:T(8,128)(2,1)} %refs_2_.7, bf16[1024,512]{1,0:T(8,128)(2,1)} %copy-done, bf16[256,512]{1,0:T(8,128)(2,1)} %collective-permute-done.7.refs_4_, ...), custom_call_target="tpu_custom_call" | custom-call | flops 335544320 | bytes 7340032 | tf_op jit(solution)/shard_map/project/pallas_call | solution.py:92
  46.2 6.0 %project.4.refs_2_.refs_6_.refs_3_.refs_7_.refs_10_ = bf16[5,256,256]{2,1,0:T(8,128)(2,1)} custom-call(s32[4]{0:T(128)} %pad_add_fusion.refs_0_, f32[1,2048]{1,0:T(1,128)} %bitcast.35, bf16[1024,512]{1,0:T(8,128)(2,1)} %refs_2_.7, bf16[1024,512]{1,0:T(8,128)(2,1)} %copy-done, bf16[256,512]{1,0:T(8,128)(2,1)} %collective-permute-done.1.refs_4_, ...), custom_call_target="tpu_custom_call" | custom-call | flops 335544320 | bytes 7340032 | tf_op jit(solution)/shard_map/project/pallas_call | solution.py:92
  52.2 6.0 %project.6.refs_4_.refs_8_.refs_5_.refs_9_.refs_12_ = bf16[5,256,256]{2,1,0:T(8,128)(2,1)} custom-call(s32[4]{0:T(128)} %pad_add_fusion.refs_0_, f32[1,2048]{1,0:T(1,128)} %bitcast.36, bf16[1024,512]{1,0:T(8,128)(2,1)} %refs_2_.7, bf16[1024,512]{1,0:T(8,128)(2,1)} %copy-done, bf16[256,512]{1,0:T(8,128)(2,1)} %collective-permute-done.5.refs_4_, ...), custom_call_target="tpu_custom_call" | custom-call | flops 335544320 | bytes 7340032 | tf_op jit(solution)/shard_map/project/pallas_call | solution.py:92
  58.2 6.0 %project.5.refs_3_.refs_7_.refs_4_.refs_8_.refs_11_ = bf16[5,256,256]{2,1,0:T(8,128)(2,1)} custom-call(s32[4]{0:T(128)} %pad_add_fusion.refs_0_, f32[1,2048]{1,0:T(1,128)} %bitcast.37, bf16[1024,512]{1,0:T(8,128)(2,1)} %refs_2_.7, bf16[1024,512]{1,0:T(8,128)(2,1)} %copy-done, bf16[256,512]{1,0:T(8,128)(2,1)} %collective-permute-done.3.refs_4_, ...), custom_call_target="tpu_custom_call" | custom-call | flops 335544320 | bytes 7340032 | tf_op jit(solution)/shard_map/project/pallas_call | solution.py:92
  64.2 3.4 %totals.1 = bf16[8,2,80,128]{3,2,1,0:T(8,128)(2,1)} custom-call(s32[1]{0:T(128)} %bitcast.8.refs_0_, f32[1024,2]{1,0:T(8,128)} %bitcast.26, f32[2]{0:T(128)} %slice_bitcast_fusion.2.refs_2_.refs_1_, bf16[5,256,256]{2,1,0:T(8,128)(2,1)} %project.4.refs_2_.refs_6_.refs_3_.refs_7_.refs_10_, ...), custom_call_target="tpu_custom_call" | custom-call | flops 300000000 | bytes 2097152 | tf_op jit(solution)/shard_map/totals/pallas_call | solution.py:215
  68.4 5.6 %all-to-all-start = ((bf16[8,2,80,128]{3,2,1,0:T(8,128)(2,1)}), bf16[8,2,80,128]{3,2,1,0:T(8,128)(2,1)S(1)}, u32[]{:S(2)}, u32[]{:S(2)}) async-start(bf16[8,2,80,128]{3,2,1,0:T(8,128)(2,1)} %totals.1), calls=%async_computation | async-start | bytes 655360 | tf_op jit(solution)/shard_map/all_to_all | solution.py:495
  74.8 7.8 %all-to-all-done.refs_3_ = bf16[8,2,80,128]{3,2,1,0:T(8,128)(2,1)S(1)} async-done(((bf16[8,2,80,128]{3,2,1,0:T(8,128)(2,1)}), bf16[8,2,80,128]{3,2,1,0:T(8,128)(2,1)S(1)}, u32[]{:S(2)}, u32[]{:S(2)}) %all-to-all-start) | async-done | bytes 327712 | tf_op jit(solution)/shard_map/all_to_all | solution.py:495
  83.8 5.4 %all-to-all-start.2 = ((bf16[8,2,64,512]{3,2,1,0:T(8,128)(2,1)}), bf16[8,2,64,512]{3,2,1,0:T(8,128)(2,1)S(1)}, u32[]{:S(2)}, u32[]{:S(2)}) async-start(bf16[8,2,64,512]{3,2,1,0:T(8,128)(2,1)} %broadcast_in_dim.5), calls=%async_computation.2 | async-start | bytes 2097152 | tf_op jit(solution)/shard_map/all_to_all | solution.py:409
  94.0 7.3 %local.1.refs_5_ = f32[1024,256]{1,0:T(8,128)} custom-call(f32[1024,2]{1,0:T(8,128)} %bitcast.27, f32[2,1024]{1,0:T(2,128)} %copy.22.refs_1_, bf16[5,256,256]{2,1,0:T(8,128)(2,1)} %project.4.refs_2_.refs_6_.refs_3_.refs_7_.refs_10_, bf16[5,256,256]{2,1,0:T(8,128)(2,1)} %project.5.refs_3_.refs_7_.refs_4_.refs_8_.refs_11_, ...), custom_call_target="tpu_custom_call" | custom-call | flops 1000000000 | bytes 3145728 | tf_op jit(solution)/shard_map/local/pallas_call | solution.py:260
  101.3 14.3 %collective-permute-done.9.refs_10_ = bf16[128,256]{1,0:T(8,128)(2,1)S(1)} collective-permute-done((bf16[128,256]{1,0:T(8,128)(2,1)S(1)}, bf16[128,256]{1,0:T(8,128)(2,1)S(1)}, u32[]{:S(2)}, u32[]{:S(2)}) %collective-permute-start.9) | collective-permute-done | bytes 65568 | tf_op jit(solution)/shard_map/ppermute | solution.py:485
  116.3 13.1 %attend.1.refs_0_ = bf16[1024,256]{1,0:T(8,128)(2,1)} custom-call(s32[1]{0:T(128)} %bitcast.refs_0_, f32[4]{0:T(128)} %refs_1_.1, bf16[5,256,256]{2,1,0:T(8,128)(2,1)} %project.4.refs_2_.refs_6_.refs_3_.refs_7_.refs_10_, bf16[5,256,256]{2,1,0:T(8,128)(2,1)} %project.5.refs_3_.refs_7_.refs_4_.refs_8_.refs_11_, ...), custom_call_target="tpu_custom_call" | custom-call | flops 1500000000 | bytes 3145728 | tf_op jit(solution)/shard_map/attend/pallas_call | solution.py:162
  129.4 1.2 collective-permute-start.12
  130.6 5.1 %cross.1.refs_4_ = bf16[1024,256]{1,0:T(8,128)(2,1)} custom-call(s32[1]{0:T(128)} %bitcast.8.refs_0_, f32[2]{0:T(128)} %slice_bitcast_fusion.2.refs_2_.refs_1_, f32[1024,2]{1,0:T(8,128)} %bitcast.28, bf16[8,2,80,128]{3,2,1,0:T(8,128)(2,1)} %copy-done.5, f32[2,2,64,128]{3,2,1,0:T(8,128)} %refs_4_.1, f32[1024,256]{1,0:T(8,128)} %local.1.refs_5_, ...), custom_call_target="tpu_custom_call" | custom-call | flops 500000000 | bytes 4194304 | tf_op jit(solution)/shard_map/cross/pallas_call | solution.py:324
  138.7 3.9 %collective-permute-done.12.refs_2_ = bf16[1024,256]{1,0:T(8,128)(2,1)} collective-permute-done((bf16[1024,256]{1,0:T(8,128)(2,1)}, bf16[1024,256]{1,0:T(8,128)(2,1)}, u32[]{:S(2)}, u32[]{:S(2)}) %collective-permute-start.12) | collective-permute-done | bytes 524320 | tf_op jit(solution)/shard_map/ppermute | solution.py:373
  142.7 2.3 %collective-permute-start.13 = (bf16[1024,256]{1,0:T(8,128)(2,1)}, bf16[1024,256]{1,0:T(8,128)(2,1)S(1)}, u32[]{:S(2)}, u32[]{:S(2)}) collective-permute-start(bf16[1024,256]{1,0:T(8,128)(2,1)} %collective-permute-done.12.refs_2_), channel_id=1, source_target_pairs={{0,1},{1,0},{2,3},{3,2},{4,5},{5,4},{6,7},{7,6},{8,9},{9,8},{10,11... | collective-permute-start | bytes 1572872 | tf_op jit(solution)/shard_map/ppermute | solution.py:368
  145.0 8.9 %collective-permute-done.15.refs_6_ = bf16[1024,256]{1,0:T(8,128)(2,1)} collective-permute-done((bf16[1024,256]{1,0:T(8,128)(2,1)}, bf16[1024,256]{1,0:T(8,128)(2,1)}, u32[]{:S(2)}, u32[]{:S(2)}) %collective-permute-start.15) | collective-permute-done | bytes 524320 | tf_op jit(solution)/shard_map/ppermute | solution.py:373
  153.9 1.4 collective-permute-start.16
  157.7 6.3 %output.1 = bf16[1024,512]{1,0:T(8,128)(2,1)} custom-call(bf16[1024,256]{1,0:T(8,128)(2,1)} %attend.1.refs_0_, bf16[1024,256]{1,0:T(8,128)(2,1)} %copy-done.8, bf16[1024,256]{1,0:T(8,128)(2,1)} %collective-permute-done.12.refs_2_, bf16[1024,256]{1,0:T(8,128)(2,1)} %copy-done.10, bf16[1024,256]{1,0:T(8,128)(2,1)} %cross.1.refs_4_, ...), custom_call_target="tpu_custom_call" | custom-call | flops 1000000000 | bytes 8388608 | tf_op jit(solution)/shard_map/output/pallas_call | solution.py:355
  (76 shorter events, 21.2 us)
Async XLA Ops:
  0.0 39.2 %collective-permute-start = (bf16[1024,512]{1,0:T(8,128)(2,1)}, bf16[1024,512]{1,0:T(8,128)(2,1)S(1)}, u32[]{:S(2)}, u32[]{:S(2)}) collective-permute-start(bf16[1024,512]{1,0:T(8,128)(2,1)} %refs_2_.7), channel_id=1, source_target_pairs={{0,1},{1,0},{2,3},{3,2},{4,5},{5,4},{6,7},{7,6},{8,9},{9,8},{10,11... | collective-permute-start | bytes 3145736 | tf_op jit(solution)/shard_map/ppermute | solution.py:368
  2.9 17.4 %collective-permute-start.7 = (bf16[256,512]{1,0:T(8,128)(2,1)}, bf16[256,512]{1,0:T(8,128)(2,1)}, u32[]{:S(2)}, u32[]{:S(2)}) collective-permute-start(bf16[256,512]{1,0:T(8,128)(2,1)} %get-tuple-element.13), channel_id=1, source_target_pairs={{0,2},{1,3},{2,0},{3,1},{4,6},{5,7},{6,4},{7,5},{8,10},{9,11},{10,... | collective-permute-start | bytes 786440 | tf_op jit(solution)/shard_map/ppermute | solution.py:373
  4.1 16.2 %collective-permute-start.5 = (bf16[256,512]{1,0:T(8,128)(2,1)}, bf16[256,512]{1,0:T(8,128)(2,1)}, u32[]{:S(2)}, u32[]{:S(2)}) collective-permute-start(bf16[256,512]{1,0:T(8,128)(2,1)} %get-tuple-element.14), channel_id=1, source_target_pairs={{0,2},{1,3},{2,0},{3,1},{4,6},{5,7},{6,4},{7,5},{8,10},{9,11},{10,... | collective-permute-start | bytes 786440 | tf_op jit(solution)/shard_map/ppermute | solution.py:373
  4.4 17.9 %collective-permute-start.3 = (bf16[256,512]{1,0:T(8,128)(2,1)}, bf16[256,512]{1,0:T(8,128)(2,1)}, u32[]{:S(2)}, u32[]{:S(2)}) collective-permute-start(bf16[256,512]{1,0:T(8,128)(2,1)} %get-tuple-element.15), channel_id=1, source_target_pairs={{0,2},{1,3},{2,0},{3,1},{4,6},{5,7},{6,4},{7,5},{8,10},{9,11},{10,... | collective-permute-start | bytes 786440 | tf_op jit(solution)/shard_map/ppermute | solution.py:373
  5.6 22.3 %collective-permute-start.1 = (bf16[256,512]{1,0:T(8,128)(2,1)}, bf16[256,512]{1,0:T(8,128)(2,1)}, u32[]{:S(2)}, u32[]{:S(2)}) collective-permute-start(bf16[256,512]{1,0:T(8,128)(2,1)} %get-tuple-element.16), channel_id=1, source_target_pairs={{0,2},{1,3},{2,0},{3,1},{4,6},{5,7},{6,4},{7,5},{8,10},{9,11},{10,... | collective-permute-start | bytes 786440 | tf_op jit(solution)/shard_map/ppermute | solution.py:373
  7.1 8.7 %copy-start.13 = (f32[2,1024]{1,0:T(2,128)S(1)}, f32[2,1024]{1,0:T(2,128)}, u32[]{:S(2)}) copy-start(f32[2,1024]{1,0:T(2,128)} %param.25) | copy-start | bytes 24580
  8.4 8.2 %copy-start.3 = (bf16[512,2048]{1,0:T(8,128)(2,1)}, bf16[512,2048]{1,0:T(8,128)(2,1)S(1)}, u32[]{:S(2)}) copy-start(bf16[512,2048]{1,0:T(8,128)(2,1)S(1)} %constant_dynamic-update-slice_fusion) | copy-start | bytes 6291460
  11.3 56.3 %all-to-all-start.1 = ((bf16[4,64,512]{2,1,0:T(8,128)(2,1)}), bf16[4,64,512]{2,1,0:T(8,128)(2,1)S(1)}, u32[]{:S(2)}, u32[]{:S(2)}) async-start(bf16[4,64,512]{2,1,0:T(8,128)(2,1)} %copy.23), calls=%async_computation.1 | async-start | bytes 524288 | tf_op jit(solution)/shard_map/all_to_all | solution.py:405
  20.2 14.4 %copy-start.1 = (f32[2,8,128]{0,2,1:T(8,128)}, f32[2,8,128]{0,2,1:T(8,128)S(1)}, u32[]{:S(2)}) copy-start(f32[2,8,128]{0,2,1:T(8,128)S(1)} %copy.21) | copy-start | bytes 24580
  20.3 19.0 %collective-permute-start.8 = (bf16[256,512]{1,0:T(8,128)(2,1)}, bf16[256,512]{1,0:T(8,128)(2,1)}, u32[]{:S(2)}, u32[]{:S(2)}) collective-permute-start(bf16[256,512]{1,0:T(8,128)(2,1)} %collective-permute-done.7.refs_4_), channel_id=1, source_target_pairs={{0,1},{1,0},{2,3},{3,2},{4,5},{5,4},{6,7},{7,6},{8,9},{9,8},{10,11... | collective-permute-start | bytes 786440 | tf_op jit(solution)/shard_map/ppermute | solution.py:368
  20.4 31.8 %collective-permute-start.6 = (bf16[256,512]{1,0:T(8,128)(2,1)}, bf16[256,512]{1,0:T(8,128)(2,1)}, u32[]{:S(2)}, u32[]{:S(2)}) collective-permute-start(bf16[256,512]{1,0:T(8,128)(2,1)} %collective-permute-done.5.refs_4_), channel_id=1, source_target_pairs={{0,1},{1,0},{2,3},{3,2},{4,5},{5,4},{6,7},{7,6},{8,9},{9,8},{10,11... | collective-permute-start | bytes 786440 | tf_op jit(solution)/shard_map/ppermute | solution.py:368
  22.3 35.9 %collective-permute-start.4 = (bf16[256,512]{1,0:T(8,128)(2,1)}, bf16[256,512]{1,0:T(8,128)(2,1)}, u32[]{:S(2)}, u32[]{:S(2)}) collective-permute-start(bf16[256,512]{1,0:T(8,128)(2,1)} %collective-permute-done.3.refs_4_), channel_id=1, source_target_pairs={{0,1},{1,0},{2,3},{3,2},{4,5},{5,4},{6,7},{7,6},{8,9},{9,8},{10,11... | collective-permute-start | bytes 786440 | tf_op jit(solution)/shard_map/ppermute | solution.py:368
  27.9 18.3 %collective-permute-start.2 = (bf16[256,512]{1,0:T(8,128)(2,1)}, bf16[256,512]{1,0:T(8,128)(2,1)}, u32[]{:S(2)}, u32[]{:S(2)}) collective-permute-start(bf16[256,512]{1,0:T(8,128)(2,1)} %collective-permute-done.1.refs_4_), channel_id=1, source_target_pairs={{0,1},{1,0},{2,3},{3,2},{4,5},{5,4},{6,7},{7,6},{8,9},{9,8},{10,11... | collective-permute-start | bytes 786440 | tf_op jit(solution)/shard_map/ppermute | solution.py:368
  39.2 1.0 copy-start
  67.7 21.5 %copy-start.2 = (f32[2,8,128]{0,2,1:T(8,128)S(1)}, f32[2,8,128]{0,2,1:T(8,128)}, u32[]{:S(2)}) copy-start(f32[2,8,128]{0,2,1:T(8,128)} %copy-done.1) | copy-start | bytes 24580
  68.4 14.3 %all-to-all-start = ((bf16[8,2,80,128]{3,2,1,0:T(8,128)(2,1)}), bf16[8,2,80,128]{3,2,1,0:T(8,128)(2,1)S(1)}, u32[]{:S(2)}, u32[]{:S(2)}) async-start(bf16[8,2,80,128]{3,2,1,0:T(8,128)(2,1)} %totals.1), calls=%async_computation | async-start | bytes 655360 | tf_op jit(solution)/shard_map/all_to_all | solution.py:495
  82.6 18.6 %copy-start.5 = (bf16[8,2,80,128]{3,2,1,0:T(8,128)(2,1)}, bf16[8,2,80,128]{3,2,1,0:T(8,128)(2,1)S(1)}, u32[]{:S(2)}) copy-start(bf16[8,2,80,128]{3,2,1,0:T(8,128)(2,1)S(1)} %all-to-all-done.refs_3_) | copy-start | bytes 983044
  83.8 71.5 %all-to-all-start.2 = ((bf16[8,2,64,512]{3,2,1,0:T(8,128)(2,1)}), bf16[8,2,64,512]{3,2,1,0:T(8,128)(2,1)S(1)}, u32[]{:S(2)}, u32[]{:S(2)}) async-start(bf16[8,2,64,512]{3,2,1,0:T(8,128)(2,1)} %broadcast_in_dim.5), calls=%async_computation.2 | async-start | bytes 2097152 | tf_op jit(solution)/shard_map/all_to_all | solution.py:409
  90.8 24.8 %collective-permute-start.9 = (bf16[128,256]{1,0:T(8,128)(2,1)S(1)}, bf16[128,256]{1,0:T(8,128)(2,1)S(1)}, u32[]{:S(2)}, u32[]{:S(2)}) collective-permute-start(bf16[128,256]{1,0:T(8,128)(2,1)S(1)} %slice_bitcast_fusion.1), channel_id=1, source_target_pairs={{0,4},{4,8},{8,12},{12,16},{16,20},{20,24},{24,28},{28,0},{1,5},{5... | collective-permute-start | bytes 196616 | tf_op jit(solution)/shard_map/ppermute | solution.py:485
  92.8 22.8 %collective-permute-start.10 = (bf16[128,256]{1,0:T(8,128)(2,1)S(1)}, bf16[128,256]{1,0:T(8,128)(2,1)S(1)}, u32[]{:S(2)}, u32[]{:S(2)}) collective-permute-start(bf16[128,256]{1,0:T(8,128)(2,1)S(1)} %slice_bitcast_fusion), channel_id=1, source_target_pairs={{4,0},{8,4},{12,8},{16,12},{20,16},{24,20},{28,24},{0,28},{5,1},{9... | collective-permute-start | bytes 196616 | tf_op jit(solution)/shard_map/ppermute | solution.py:486
  129.4 6.7 %copy-start.4 = (bf16[512,2048]{1,0:T(8,128)(2,1)S(1)}, bf16[512,2048]{1,0:T(8,128)(2,1)}, u32[]{:S(2)}) copy-start(bf16[512,2048]{1,0:T(8,128)(2,1)} %copy-done.3) | copy-start | bytes 6291460
  129.4 13.3 %collective-permute-start.12 = (bf16[1024,256]{1,0:T(8,128)(2,1)}, bf16[1024,256]{1,0:T(8,128)(2,1)}, u32[]{:S(2)}, u32[]{:S(2)}) collective-permute-start(bf16[1024,256]{1,0:T(8,128)(2,1)} %attend.1.refs_0_), channel_id=1, source_target_pairs={{0,2},{1,3},{2,0},{3,1},{4,6},{5,7},{6,4},{7,5},{8,10},{9,11},{10,... | collective-permute-start | bytes 1572872 | tf_op jit(solution)/shard_map/ppermute | solution.py:373
  135.7 18.2 %collective-permute-start.15 = (bf16[1024,256]{1,0:T(8,128)(2,1)}, bf16[1024,256]{1,0:T(8,128)(2,1)}, u32[]{:S(2)}, u32[]{:S(2)}) collective-permute-start(bf16[1024,256]{1,0:T(8,128)(2,1)} %cross.1.refs_4_), channel_id=1, source_target_pairs={{0,2},{1,3},{2,0},{3,1},{4,6},{5,7},{6,4},{7,5},{8,10},{9,11},{10,... | collective-permute-start | bytes 1572872 | tf_op jit(solution)/shard_map/ppermute | solution.py:373
  137.2 19.2 %collective-permute-start.17 = (bf16[512,512]{1,0:T(8,128)(2,1)}, bf16[512,512]{1,0:T(8,128)(2,1)S(1)}, u32[]{:S(2)}, u32[]{:S(2)}) collective-permute-start(bf16[512,512]{1,0:T(8,128)(2,1)} %get-tuple-element.9), channel_id=1, source_target_pairs={{0,1},{1,0},{2,3},{3,2},{4,5},{5,4},{6,7},{7,6},{8,9},{9,8},{10,11... | collective-permute-start | bytes 1572872 | tf_op jit(solution)/shard_map/ppermute | solution.py:368
  138.2 18.1 %collective-permute-start.11 = (bf16[1024,256]{1,0:T(8,128)(2,1)}, bf16[1024,256]{1,0:T(8,128)(2,1)S(1)}, u32[]{:S(2)}, u32[]{:S(2)}) collective-permute-start(bf16[1024,256]{1,0:T(8,128)(2,1)} %attend.1.refs_0_), channel_id=1, source_target_pairs={{0,1},{1,0},{2,3},{3,2},{4,5},{5,4},{6,7},{7,6},{8,9},{9,8},{10,11... | collective-permute-start | bytes 1572872 | tf_op jit(solution)/shard_map/ppermute | solution.py:368
  138.2 18.2 %collective-permute-start.14 = (bf16[1024,256]{1,0:T(8,128)(2,1)}, bf16[1024,256]{1,0:T(8,128)(2,1)S(1)}, u32[]{:S(2)}, u32[]{:S(2)}) collective-permute-start(bf16[1024,256]{1,0:T(8,128)(2,1)} %cross.1.refs_4_), channel_id=1, source_target_pairs={{0,1},{1,0},{2,3},{3,2},{4,5},{5,4},{6,7},{7,6},{8,9},{9,8},{10,11... | collective-permute-start | bytes 1572872 | tf_op jit(solution)/shard_map/ppermute | solution.py:368
  142.7 13.7 %collective-permute-start.13 = (bf16[1024,256]{1,0:T(8,128)(2,1)}, bf16[1024,256]{1,0:T(8,128)(2,1)S(1)}, u32[]{:S(2)}, u32[]{:S(2)}) collective-permute-start(bf16[1024,256]{1,0:T(8,128)(2,1)} %collective-permute-done.12.refs_2_), channel_id=1, source_target_pairs={{0,1},{1,0},{2,3},{3,2},{4,5},{5,4},{6,7},{7,6},{8,9},{9,8},{10,11... | collective-permute-start | bytes 1572872 | tf_op jit(solution)/shard_map/ppermute | solution.py:368
  153.9 3.2 %collective-permute-start.16 = (bf16[1024,256]{1,0:T(8,128)(2,1)}, bf16[1024,256]{1,0:T(8,128)(2,1)}, u32[]{:S(2)}, u32[]{:S(2)}) collective-permute-start(bf16[1024,256]{1,0:T(8,128)(2,1)} %collective-permute-done.15.refs_6_), channel_id=1, source_target_pairs={{0,1},{1,0},{2,3},{3,2},{4,5},{5,4},{6,7},{7,6},{8,9},{9,8},{10,11... | collective-permute-start | bytes 1572872 | tf_op jit(solution)/shard_map/ppermute | solution.py:368
  156.4 0.8 copy-start.7
  156.4 1.0 copy-start.8
  156.4 1.1 copy-start.9
  156.4 1.3 copy-start.10
  (3 other events, 2.0 us)

commit v2 on v1

v2 whole, which is shorter than its diff:
```python
import functools
import math

import jax
import jax.numpy as jnp
import numpy as np
from jax import lax
from jax.experimental import pallas as pl
from jax.experimental.pallas import tpu as pltpu
from jax.sharding import PartitionSpec as P


HD = 64
RK = 64
RV = 128
WINDOW = 128
NORM_EPS = 1e-06
ROPE_BASE = 10000.0
NEG = -1e30
EXTRA = 16
CHUNKS = ((0, 1), (1, 1), (2, 2))
ORDER = (2, 0, 1)
TABLE = 32
F32 = jnp.float32
BF16 = jnp.bfloat16

VMEM = pl.BlockSpec(memory_space=pltpu.VMEM)
SMEM = pl.BlockSpec(memory_space=pltpu.SMEM)
ANY = pl.BlockSpec(memory_space=pl.ANY)
PARAMS = pltpu.CompilerParams(vmem_limit_bytes=16 << 20)


def cost(flops, nbytes):
    return pl.CostEstimate(flops=int(flops), bytes_accessed=int(nbytes), transcendentals=0)


def dot(a, b):
    return jnp.dot(a, b, preferred_element_type=F32)


def dot_t(a, b):
    return lax.dot_general(a, b, (((1,), (1,)), ((), ())), preferred_element_type=F32)


def t_dot(a, b):
    return lax.dot_general(a, b, (((0,), (0,)), ((), ())), preferred_element_type=F32)


def split_kernel(n_pieces, n_far, *refs):
    tokens, att, ret = refs[:3]
    pieces = refs[3 : 3 + n_pieces]
    slabs = refs[3 + n_pieces : 3 + n_pieces + n_far]
    sems = refs[-1]
    n_tp = lax.axis_size("tp")
    tp, sp = lax.axis_index("tp"), lax.axis_index("sp")
    chips = n_tp // 2
    copies = []
    for by in range(1, chips):
        slab = slabs[by - 1]
        share, width = slab.shape[0] // 2, slab.shape[1]
        target = lax.rem(tp // 2 + by, chips)
        rows = pl.ds(pl.multiple_of(sp * share, share), share)
        cols = pl.ds(pl.multiple_of(target * width, width), width)
        for i, ref in enumerate((att, ret)):
            dst = slab.at[pl.ds(i * share, share)]
            copies.append(pltpu.make_async_copy(ref.at[rows, cols], dst, sems.at[2 * by - 2 + i]))
    for copy in copies:
        copy.start()
    for c, piece in enumerate(pieces):
        first = CHUNKS[c][0] * tokens.shape[0] // 4
        piece[...] = tokens[first : first + piece.shape[0]]
    for copy in copies:
        copy.wait()


def split(tokens, att, ret):
    total, cols = tokens.shape
    chips = lax.axis_size("tp") // 2
    share = att.shape[0] // lax.axis_size("sp")
    shapes = [jax.ShapeDtypeStruct((n * total // 4, cols), BF16) for _, n in CHUNKS]
    shapes += [jax.ShapeDtypeStruct((2 * share, 2 * cols), BF16)] * (chips - 1)
    if share % 16:
        rows = lax.axis_index("sp") * share
        out = [tokens[f * total // 4 : (f + n) * total // 4] for f, n in CHUNKS]
        for by in range(1, chips):
            target = lax.rem(lax.axis_index("tp") // 2 + by, chips) * 2 * cols
            parts = [lax.dynamic_slice(w, (rows, target), (share, 2 * cols)) for w in (att, ret)]
            out.append(jnp.concatenate(parts, axis=0))
    else:
        out = pl.pallas_call(
            functools.partial(split_kernel, len(CHUNKS), chips - 1),
            out_shape=tuple(shapes),
            in_specs=[VMEM, ANY, ANY],
            out_specs=(VMEM,) * len(shapes),
            scratch_shapes=[pltpu.SemaphoreType.DMA((2 * chips,))],
            cost_estimate=cost(0.1e9, 3 << 20),
            compiler_params=PARAMS,
            name="split",
        )(tokens, att, ret)
    return out[: len(CHUNKS)], out[len(CHUNKS) :]


def repeat_kernel(*refs):
    out_ref = refs[-1]
    for s in range(out_ref.shape[0]):
        for i, ref in enumerate(refs[:-1]):
            out_ref[s, i] = ref[...]


def repeat(slabs, count):
    return pl.pallas_call(
        repeat_kernel,
        out_shape=jax.ShapeDtypeStruct((count, len(slabs)) + slabs[0].shape, BF16),
        in_specs=[VMEM] * len(slabs),
        out_specs=VMEM,
        cost_estimate=cost(0.1e9, 1 << 20),
        compiler_params=PARAMS,
        name="repeat",
    )(*slabs)


def prepare_kernel(log_ref, row_ref, col_ref, cos_ref, sin_ref):
    total = log_ref.shape[1]
    heads = log_ref.shape[0]
    sums = jnp.concatenate([log_ref[...], jnp.zeros((8 - heads, total), F32)], axis=0)
    lane = lax.broadcasted_iota(jnp.int32, sums.shape, 1)
    step = 1
    while step < total:
        sums = sums + jnp.where(lane >= step, pltpu.roll(sums, step, 1), 0.0)
        step *= 2
    row_ref[...] = sums
    col_ref[...] = sums.T
    rows, lanes = cos_ref.shape
    row = lax.broadcasted_iota(jnp.int32, (rows, lanes), 0)
    pair = lax.broadcasted_iota(jnp.int32, (rows, lanes), 1) & (RK // 2 - 1)
    count = total // TABLE
    place = jnp.where(row < count, lax.axis_index("sp") * total + TABLE * row, row - count)
    inverse = jnp.exp(pair.astype(F32) * (-2.0 * math.log(ROPE_BASE) / RK))
    angles = place.astype(F32) * inverse
    cos_ref[...] = jnp.cos(angles)
    sin_ref[...] = jnp.sin(angles)


def prepare(log):
    heads, total = log.shape
    table = jax.ShapeDtypeStruct((total // TABLE + TABLE, heads * RK), F32)
    return pl.pallas_call(
        prepare_kernel,
        out_shape=(
            jax.ShapeDtypeStruct((8, total), F32),
            jax.ShapeDtypeStruct((total, 8), F32),
            table,
            table,
        ),
        in_specs=[VMEM],
        out_specs=(VMEM,) * 4,
        cost_estimate=cost(0.1e9, 1 << 16),
        compiler_params=PARAMS,
        name="prepare",
    )(log)


def project_kernel(n_blocks, n_w, parts, first, ret_local, *refs):
    gain_ref, crow_ref, ccol_ref, swap_ref, mix_ref, cos_ref, sin_ref = refs[:7]
    blocks = refs[7 : 7 + n_blocks]
    w_refs = refs[7 + n_blocks : 7 + n_blocks + n_w]
    out_ref, sum_ref, low_ref, high_ref = refs[7 + n_blocks + n_w : 11 + n_blocks + n_w]
    xn, inv = refs[-2:]
    width = blocks[0].shape[1]
    rows = xn.shape[0]
    group_width = inv.shape[1]
    half = group_width // 2
    total = crow_ref.shape[1]
    mine = pl.ds(first, rows)
    starts = [pl.multiple_of(i * width, width) for i in sources()]
    tile = min(128, rows)
    lanes = min(128, width)
    for r in range(rows // tile):
        here = pl.ds(r * tile, tile)
        squares = jnp.zeros((tile, lanes), F32)
        for start, block in zip(starts, blocks):
            at = here if block.shape[0] == rows else pl.ds(first + r * tile, tile)
            for low in range(0, width, lanes):
                part = block[at, low : low + lanes].astype(F32)
                squares = squares + part * part
                col = pl.ds(pl.multiple_of(start + low, lanes), lanes)
                xn[here, col] = (part * gain_ref[:, col]).astype(BF16)
        mean = jnp.sum(squares, axis=1, keepdims=True) / (width * n_blocks)
        inv[here, :] = jnp.broadcast_to(lax.rsqrt(mean + NORM_EPS), (tile, group_width))
    count = total // TABLE
    cos_b, sin_b = cos_ref[count:], sin_ref[count:]
    cosines, sines = [], []
    for k in range(first // TABLE, (first + rows) // TABLE):
        cos_k, sin_k = cos_ref[k : k + 1], sin_ref[k : k + 1]
        cosines.append(cos_k * cos_b - sin_k * sin_b)
        sines.append(sin_k * cos_b + cos_k * sin_b)
    cosine = jnp.concatenate(cosines, axis=0)
    sine = jnp.concatenate(sines, axis=0)
    for group in (2, 3, 0, 1, 4):
        ws = [w[...] for w, (g, _) in zip(w_refs, parts) if g == group]
        w = ws[0] if len(ws) == 1 else jnp.concatenate(ws, axis=1)
        raw = (dot(xn[...], w) * inv[...]).astype(BF16)
        if group == 0:
            raw = (dot(raw, mix_ref[...]) * HD ** (-0.5)).astype(BF16)
        if group == 2:
            sides = []
            for low, scale in ((0, 1.0), (half, RK ** (-0.5))):
                side = raw[:, low : low + half]
                turned = side.astype(F32) * cosine + dot(side, swap_ref[...]) * sine
                sides.append((turned * scale).astype(BF16))
            keys = sides[1]
            raw = jnp.concatenate(sides, axis=1)
        if group == 3:
            for h in range(ret_local):
                col = ccol_ref[mine, h : h + 1]
                end = crow_ref[h : h + 1, total - 1 : total]
                v = raw[:, h * RV : (h + 1) * RV].astype(F32)
                both = jnp.concatenate([v * jnp.exp(end - col), v * jnp.exp(col)], axis=1)
                sum_ref[h] = t_dot(keys, both.astype(BF16))[h * RK : (h + 1) * RK]
        if group == 1:
            low_ref[...] = raw[rows - WINDOW :]
            high_ref[...] = raw[:WINDOW]
        out_ref[group] = raw


def project(gain, crow, ccol, swap, mix, cos, sin, blocks, weights, parts, first, rows, ret_local):
    width = mix.shape[0]
    depth = gain.shape[1]
    n = len(blocks)
    return pl.pallas_call(
        functools.partial(project_kernel, n, len(weights), parts, first, ret_local),
        out_shape=(
            jax.ShapeDtypeStruct((5, rows, width), BF16),
            jax.ShapeDtypeStruct((ret_local, RK, 2 * RV), F32),
            jax.ShapeDtypeStruct((WINDOW, width), BF16),
            jax.ShapeDtypeStruct((WINDOW, width), BF16),
        ),
        in_specs=[VMEM] * (n + 7 + len(weights)),
        out_specs=(VMEM,) * 4,
        scratch_shapes=[pltpu.VMEM((rows, depth), BF16), pltpu.VMEM((rows, width), F32)],
        cost_estimate=cost(2 * rows * depth * 5 * width // 4, 7 << 20),
        compiler_params=PARAMS,
        name="project",
    )(gain, crow, ccol, swap, mix, cos, sin, *blocks, *weights)


def attend_kernel(n_chunks, kv_local, groups, seq_len, *refs):
    sink_ref = refs[0]
    proj = refs[1 : 1 + n_chunks]
    low_ref, high_ref, out_ref = refs[1 + n_chunks : 4 + n_chunks]
    qbuf, kbuf, vbuf, mask = refs[-4:]
    total = sum(ref.shape[1] for ref in proj)
    offset = lax.axis_index("sp") * total
    kv_cols = kv_local * HD
    block = WINDOW
    span = block + 2 * WINDOW
    pieces = [(0, low_ref[...])]
    at = 0
    for ref in proj:
        pieces.append((WINDOW + at, ref[1]))
        qbuf[pl.ds(at, ref.shape[1])] = ref[0]
        at += ref.shape[1]
    pieces.append((WINDOW + total, high_ref[...]))
    for first, kv in pieces:
        here = pl.ds(first, kv.shape[0])
        kbuf[here] = kv[:, :kv_cols]
        vbuf[0:kv_cols, here] = kv[:, kv_cols:].T
    vbuf[kv_cols:] = jnp.ones((vbuf.shape[0] - kv_cols, vbuf.shape[1]), BF16)
    row = lax.broadcasted_iota(jnp.int32, (span, block), 1)
    col = lax.broadcasted_iota(jnp.int32, (span, block), 0)
    band = (col >= row) & (col <= row + 2 * WINDOW)
    for i, first in enumerate((0, block, total - block)):
        pos = col + (offset + first - WINDOW)
        allowed = band & (pos >= 0) & (pos < seq_len)
        one = jnp.where(allowed, 0.0, NEG)
        mask[i] = jnp.concatenate([one] * groups, axis=1)
    lane = lax.broadcasted_iota(jnp.int32, (block, kv_cols), 1)
    n_steps = total // block

    def step(i, carry):
        first = pl.multiple_of(i * block, block)
        q = qbuf[pl.ds(first, block)]
        k = kbuf[pl.ds(first, span)]
        kind = jnp.where(i == 0, 0, jnp.where(i == n_steps - 1, 2, 1))
        bias = mask[kind]
        scores = []
        for g in range(kv_local):
            mine = (lane >= g * HD) & (lane < (g + 1) * HD)
            tiles = []
            for j in range(groups):
                tile = q[:, j * kv_cols : (j + 1) * kv_cols]
                tiles.append(jnp.where(mine, tile, jnp.zeros_like(tile)))
            scores.append(dot_t(k, jnp.concatenate(tiles, axis=0)))
        weights = []
        rests = []
        for g in range(kv_local):
            s = scores[g] + bias
            sink = jnp.concatenate(
                [jnp.full((1, block), sink_ref[g * groups + j], F32) for j in range(groups)], axis=1
            )
            top = jnp.maximum(jnp.max(s, axis=0, keepdims=True), sink)
            weights.append(jnp.exp(s - top).astype(BF16))
            rests.append(jnp.exp(sink - top))
        outs = []
        for g in range(kv_local):
            v = vbuf[g * HD : (g + 1) * HD, pl.ds(first, span)]
            ones = vbuf[kv_cols : kv_cols + 16, pl.ds(first, span)]
            o = dot(jnp.concatenate([v, ones], axis=0), weights[g])
            o = o[:HD] / (o[HD : HD + 1] + rests[g])
            outs += [o[:, j * block : (j + 1) * block] for j in range(groups)]
        out_ref[pl.ds(first, block)] = jnp.concatenate(outs, axis=0).T.astype(BF16)
        return carry

    lax.fori_loop(0, n_steps, step, 0, unroll=n_steps)


def attend(sink, proj, low, high, kv_local, groups, seq_len):
    n = len(proj)
    width = proj[0].shape[2]
    total = sum(p.shape[1] for p in proj)
    kv_cols = kv_local * HD
    return pl.pallas_call(
        functools.partial(attend_kernel, n, kv_local, groups, seq_len),
        out_shape=jax.ShapeDtypeStruct((total, width), BF16),
        in_specs=[SMEM] + [VMEM] * (n + 2),
        out_specs=VMEM,
        scratch_shapes=[
            pltpu.VMEM((total, width), BF16),
            pltpu.VMEM((total + 2 * WINDOW, kv_cols), BF16),
            pltpu.VMEM((kv_cols + 16, total + 2 * WINDOW), BF16),
            pltpu.VMEM((3, 3 * WINDOW, groups * WINDOW), F32),
        ],
        cost_estimate=cost(1.5e9, 3 << 20),
        compiler_params=PARAMS,
        name="attend",
    )(sink, *proj, low, high)


def totals_kernel(n_chunks, ret_local, n_sp, *refs):
    crow_ref = refs[0]
    sum_refs = refs[1 : 1 + n_chunks]
    out_ref = refs[-1]
    me = lax.axis_index("sp")
    last = crow_ref.shape[1] - 1
    line = lax.broadcasted_iota(jnp.int32, (EXTRA, RV), 0)
    for h in range(ret_local):
        sums = sum_refs[0][h]
        for ref in sum_refs[1:]:
            sums = sums + ref[h]
        end = jnp.broadcast_to(crow_ref[h : h + 1, last : last + 1], (EXTRA, RV))
        d0 = end.astype(BF16).astype(F32)
        d1 = (end - d0).astype(BF16).astype(F32)
        d2 = end - d0 - d1
        extra = jnp.where(line == 0, d0, jnp.where(line == 1, d1, jnp.where(line == 2, d2, 0.0)))
        fwd = jnp.concatenate([sums[:, :RV], extra], axis=0).astype(BF16)
        bwd = jnp.concatenate([sums[:, RV:], extra], axis=0).astype(BF16)
        for j in range(n_sp):
            out_ref[j, h] = jnp.where(j > me, fwd, bwd)


def totals(crow, sums, n_sp):
    ret_local = sums[0].shape[0]
    return pl.pallas_call(
        functools.partial(totals_kernel, len(sums), ret_local, n_sp),
        out_shape=jax.ShapeDtypeStruct((n_sp, ret_local, RK + EXTRA, RV), BF16),
        in_specs=[VMEM] * (1 + len(sums)),
        out_specs=VMEM,
        cost_estimate=cost(0.1e9, 1 << 20),
        compiler_params=PARAMS,
        name="totals",
    )(crow, *sums)


def local_kernel(n_chunks, ret_local, *refs):
    ccol_ref, crow_ref = refs[:2]
    proj = refs[2 : 2 + n_chunks]
    out_ref = refs[2 + n_chunks]
    qbuf, kbuf, vbuf = refs[-3:]
    total = crow_ref.shape[1]
    cols = ret_local * RK
    at = 0
    for ref in proj:
        here = pl.ds(at, ref.shape[1])
        qbuf[here] = ref[2, :, :cols]
        kbuf[here] = ref[2, :, cols:]
        vbuf[here] = ref[3]
        at += ref.shape[1]
    block = min(256, total)
    lane = lax.broadcasted_iota(jnp.int32, (block, cols), 1)

    def step(i, carry):
        here = pl.ds(pl.multiple_of(i * block, block), block)
        q = qbuf[here]
        for h in range(ret_local):
            mine = (lane >= h * RK) & (lane < (h + 1) * RK)
            qh = jnp.where(mine, q, jnp.zeros_like(q))
            gap = ccol_ref[here, h : h + 1] - crow_ref[h : h + 1, :]
            w = (dot_t(qh, kbuf[...]) * jnp.exp(-jnp.abs(gap))).astype(BF16)
            out_ref[here, h * RV : (h + 1) * RV] = dot(w, vbuf[:, h * RV : (h + 1) * RV])
        return carry

    lax.fori_loop(0, total // block, step, 0)


def local(ccol, crow, proj, ret_local):
    n = len(proj)
    width = proj[0].shape[2]
    total = crow.shape[1]
    return pl.pallas_call(
        functools.partial(local_kernel, n, ret_local),
        out_shape=jax.ShapeDtypeStruct((total, width), F32),
        in_specs=[VMEM] * (n + 2),
        out_specs=VMEM,
        scratch_shapes=[
            pltpu.VMEM((total, ret_local * RK), BF16),
            pltpu.VMEM((total, ret_local * RK), BF16),
            pltpu.VMEM((total, width), BF16),
        ],
        cost_estimate=cost(1e9, 3 << 20),
        compiler_params=PARAMS,
        name="local",
    )(ccol, crow, *proj)


def cross_kernel(n_chunks, ret_local, n_sp, *refs):
    crow_ref, ccol_ref, got_ref, init_ref, loc_ref = refs[:5]
    proj = refs[5 : 5 + n_chunks]
    out_ref, states = refs[-2:]
    me = lax.axis_index("sp")
    last = crow_ref.shape[1] - 1
    states[...] = jnp.zeros(states.shape, BF16)
    for h in range(ret_local):
        ends = []
        for j in range(n_sp):
            tail = got_ref[j, h, RK : RK + EXTRA, :].astype(F32)
            ends.append(jnp.sum(tail, axis=0, keepdims=True))
        for side, order in enumerate((range(n_sp - 1, -1, -1), range(n_sp))):
            state = jnp.zeros((RK, RV), F32)
            run = jnp.zeros((1, RV), F32)
            for j in order:
                here = (j < me) if side == 0 else (j > me)
                term = jnp.exp(run) * got_ref[j, h, 0:RK, :].astype(F32)
                state = state + jnp.where(here, term, 0.0)
                run = run + jnp.where(here, ends[j], 0.0)
            state = state + jnp.exp(run) * init_ref[side, h]
            col = (2 * h + side) * RV
            states[h * RK : (h + 1) * RK, col : col + RV] = state.astype(BF16)
    block = min(256, last + 1)
    first = 0
    for ref in proj:

        def step(i, carry, ref=ref, first=first):
            inner = pl.ds(pl.multiple_of(i * block, block), block)
            here = pl.ds(pl.multiple_of(first + i * block, block), block)
            both = dot(ref[2, inner, : ret_local * RK], states[...])
            for h in range(ret_local):
                col = ccol_ref[here, h : h + 1]
                ret = (
                    loc_ref[here, h * RV : (h + 1) * RV]
                    + jnp.exp(col) * both[:, 2 * h * RV : (2 * h + 1) * RV]
                    + jnp.exp(crow_ref[h : h + 1, last : last + 1] - col) * both[:, (2 * h + 1) * RV : (2 * h + 2) * RV]
                )
                centered = ret - jnp.mean(ret, axis=1, keepdims=True)
                scale = lax.rsqrt(jnp.mean(centered * centered, axis=1, keepdims=True) + NORM_EPS)
                gate = ref[4, inner, h * RV : (h + 1) * RV].astype(F32)
                gated = gate / (1.0 + jnp.exp(-gate))
                out_ref[here, h * RV : (h + 1) * RV] = (gated * (centered * scale)).astype(BF16)
            return carry

        lax.fori_loop(0, ref.shape[1] // block, step, 0)
        first += ref.shape[1]


def cross(crow, ccol, got, init, loc, proj, ret_local, n_sp):
    n = len(proj)
    width = proj[0].shape[2]
    total = crow.shape[1]
    return pl.pallas_call(
        functools.partial(cross_kernel, n, ret_local, n_sp),
        out_shape=jax.ShapeDtypeStruct((total, width), BF16),
        in_specs=[VMEM] * (n + 5),
        out_specs=VMEM,
        scratch_shapes=[pltpu.VMEM((ret_local * RK, 2 * ret_local * RV), BF16)],
        cost_estimate=cost(0.5e9, 4 << 20),
        compiler_params=PARAMS,
        name="cross",
    )(crow, ccol, got, init, loc, *proj)


def rows_of(ref, part, far, cols, core):
    share = ref.shape[2] // 2
    at = pl.ds(pl.multiple_of(core * cols, cols), cols)
    pieces = [ref[s, far, part * share : (part + 1) * share, at] for s in range(ref.shape[0])]
    return jnp.concatenate(pieces, axis=0)


def far_rows(spread, peer_spread, part, cols):
    core = lax.rem(lax.axis_index("tp"), 2)
    out = []
    for far in range(spread.shape[1]):
        out.append(rows_of(spread, part, far, cols, core))
        out.append(rows_of(peer_spread, part, far, cols, core))
    return out


def most_kernel(*refs):
    near_att, near_ret, peer_att, peer_ret, spread, peer_spread = refs[:6]
    data = refs[6:-1]
    out_ref = refs[-1]
    cols = out_ref.shape[1]
    mine = pl.ds(pl.multiple_of(lax.axis_index("tp") * cols, cols), cols)
    pieces = [near_att[:, mine], peer_att[:, mine]] + far_rows(spread, peer_spread, 0, cols)
    pieces += [near_ret[:, mine], peer_ret[:, mine]]
    right = jnp.concatenate(pieces, axis=0)
    rows = min(256, out_ref.shape[0])
    for i in range(out_ref.shape[0] // rows):
        here = pl.ds(i * rows, rows)
        out_ref[here] = dot(jnp.concatenate([ref[here] for ref in data], axis=1), right)


def last_kernel(*refs):
    spread, peer_spread, base = refs[:3]
    data = refs[3:-1]
    out_ref = refs[-1]
    right = jnp.concatenate(far_rows(spread, peer_spread, 1, out_ref.shape[1]), axis=0)
    rows = min(256, out_ref.shape[0])
    for i in range(out_ref.shape[0] // rows):
        here = pl.ds(i * rows, rows)
        part = dot(jnp.concatenate([ref[here] for ref in data], axis=1), right)
        out_ref[here] = (part + base[here]).astype(BF16)


def output(kernel, operands, shape, dtype):
    return pl.pallas_call(
        kernel,
        out_shape=jax.ShapeDtypeStruct(shape, dtype),
        in_specs=[VMEM] * len(operands),
        out_specs=VMEM,
        cost_estimate=cost(1e9, 8 << 20),
        compiler_params=PARAMS,
    )(*operands)


def core_swap(value):
    n = lax.axis_size("tp")
    return lax.ppermute(value, "tp", [(i, i ^ 1) for i in range(n)])


def chip_turn(value, by):
    n = lax.axis_size("tp")
    return lax.ppermute(value, "tp", [(i, (i + 2 * by) % n) for i in range(n)])


def gather_tp(value):
    blocks = [value, core_swap(value)]
    for by in range(1, lax.axis_size("tp") // 2):
        far = chip_turn(value, by)
        blocks += [far, core_swap(far)]
    return blocks


def sources():
    n = lax.axis_size("tp")
    me = lax.axis_index("tp")
    out = [me, me ^ 1]
    for by in range(1, n // 2):
        far = lax.rem(me + (n - 2 * by), n)
        out += [far, far ^ 1]
    return out


def output_weights(out_att, out_ret, slabs):
    n_sp = lax.axis_size("sp")
    moved = []
    for by, slab in enumerate(slabs, 1):
        moved.append(chip_turn(slab, by))
    spread = repeat(moved, n_sp)
    spread = lax.all_to_all(spread, "sp", 0, 0, tiled=True)
    share, cols = slabs[0].shape[0] // 2, slabs[0].shape[1]
    if share % 16:
        shape = (n_sp, len(slabs), 2, share, cols)
        spread = jnp.transpose(spread.reshape(shape), (1, 2, 0, 3, 4))
        spread = spread.reshape(1, len(slabs), -1, cols)
    peers = [core_swap(w) for w in (out_att, out_ret)]
    peer_spread = core_swap(spread)
    return [out_att, out_ret] + peers + [spread, peer_spread]


def body(
    tokens,
    norm_gain,
    att_query,
    att_key,
    att_value,
    ret_query,
    ret_key,
    ret_value,
    ret_gate,
    att_sink,
    decay_log,
    init_state,
    out_att,
    out_ret,
):
    n_sp = lax.axis_size("sp")
    total = tokens.shape[0]
    seq_len = total * n_sp
    width = att_query.shape[1]
    half = width // 2
    kv_local = att_key.shape[1] // HD
    groups = att_sink.shape[0] // kv_local
    ret_local = decay_log.shape[0]
    cols = tokens.shape[1]

    pieces, slabs = split(tokens, out_att, out_ret)
    near = core_swap(tokens)
    far = {}
    for c in ORDER:
        far[c] = []
        for by in range(1, lax.axis_size("tp") // 2):
            block = chip_turn(pieces[c], by)
            far[c] += [block, core_swap(block)]

    lane = np.arange(ret_local * RK)
    swap = np.zeros((lane.size, lane.size), np.float32)
    swap[lane ^ (RK // 2), lane] = np.where(lane % RK < RK // 2, -1.0, 1.0)
    swap = jnp.asarray(swap, BF16)
    mix = np.zeros((width, width), np.float32)
    for g in range(kv_local):
        for j in range(groups):
            for i in range(HD):
                mix[(g * groups + j) * HD + i, (j * kv_local + g) * HD + i] = 1.0
    mix = jnp.asarray(mix, BF16)
    crow, ccol, cos, sin = prepare(decay_log)

    if half % 128 == 0:
        weights = [att_query, att_key, att_value, ret_query, ret_key, ret_value, ret_gate]
        parts = [(0, 0), (1, 0), (1, half), (2, 0), (2, half), (3, 0), (4, 0)]
    else:
        weights = [
            att_query,
            jnp.concatenate([att_key, att_value], axis=1),
            jnp.concatenate([ret_query, ret_key], axis=1),
            ret_value,
            ret_gate,
        ]
        parts = [(i, 0) for i in range(5)]
    gain = norm_gain[None, :]
    out_w = output_weights(out_att, out_ret, slabs)
    proj = [None] * len(CHUNKS)
    sums = [None] * len(CHUNKS)
    edges = [None] * len(CHUNKS)
    for c in ORDER:
        first, rows = CHUNKS[c][0] * total // 4, CHUNKS[c][1] * total // 4
        proj[c], sums[c], *edges[c] = project(
            gain, crow, ccol, swap, mix, cos, sin, [tokens, near] + far[c], weights, parts,
            first, rows, ret_local,
        )

    forward = [(i, (i + 1) % n_sp) for i in range(n_sp)]
    backward = [(target, source) for source, target in forward]
    low = lax.ppermute(edges[-1][0], "sp", forward)
    high = lax.ppermute(edges[0][1], "sp", backward)

    sent = totals(crow, sums, n_sp)
    got = lax.all_to_all(sent, "sp", 0, 0, tiled=True)
    attended = attend(att_sink, proj, low, high, kv_local, groups, seq_len)
    att_blocks = gather_tp(attended)
    loc = local(ccol, crow, proj, ret_local)
    kept = cross(crow, ccol, got, init_state, loc, proj, ret_local, n_sp)
    ret_blocks = gather_tp(kept)
    operands = out_w + att_blocks + ret_blocks[:2]
    most = output(most_kernel, operands, (total, cols), F32)
    operands = out_w[4:] + [most] + ret_blocks[2:]
    return output(last_kernel, operands, (total, cols), BF16)


def solution(mesh):
    in_specs = (
        P("sp", "tp"),
        P(),
        P(None, "tp"),
        P(None, "tp"),
        P(None, "tp"),
        P(None, "tp"),
        P(None, "tp"),
        P(None, "tp"),
        P(None, "tp"),
        P("tp"),
        P("tp", "sp"),
        P(None, "tp", None, None),
        P("tp", None),
        P("tp", None),
    )
    out_specs = P("sp", "tp")
    return jax.shard_map(body, mesh=mesh, in_specs=in_specs, out_specs=out_specs, check_vma=False)
```

time: 165 us -> 130 us (0.79)
  the two profiles are of different devices: /device:TPU:17 before, /device:TPU:1 now
where the time goes in v2:
time: 130 us; the launch traced here: 129 us
  waiting for transfers between devices  41.3 us (32%)
  Pallas kernels  35.4 us (27%)
  starting transfers between devices  31.2 us (24%)
  local copies, waits for them, and re-layouts  20.7 us (16%)
    ppermute x6, waiting for transfers between devices, chip_turn(): return lax.ppermute(value, 'tp', [(i, (i + 2 * by) % n) for i in range(n)])  34.8 us
    unnamed x70, local copies, waits for them, and re-layouts  20.7 us
    pallas_call x3, Pallas kernels, project(): pl.pallas_call(functools.partial(project_kernel, n, len(weights), parts,...  12.5 us
    ppermute x11, starting transfers between devices, core_swap(): return lax.ppermute(value, 'tp', [(i, i ^ 1) for i in range(n)])  9.46 us
    pallas_call x2, Pallas kernels, output(): pl.pallas_call(kernel, out_shape=jax.ShapeDtypeStruct(shape, dtype), in_s...  7.49 us
    ppermute x1, waiting for transfers between devices, body(): low = lax.ppermute(edges[-1][0], 'sp', forward)  6.48 us
    ppermute x6, starting transfers between devices, chip_turn(): return lax.ppermute(value, 'tp', [(i, (i + 2 * by) % n) for i in range(n)])  6.37 us
    all_to_all x1, starting transfers between devices, body(): got = lax.all_to_all(sent, 'sp', 0, 0, tiled=True)  5.65 us
  transfers between devices with their start and end apart: 21, of which 6 were waited for; matrix products, arithmetic and copies ran while one was open for 0% of the time, Pallas kernels for 25%

profile of v2, /device:TPU:1, one launch (start us, length us, event | category | flops | bytes accessed | tf_op | source)
XLA Modules:
  0.0 128.9 jit_solution(6002423782983281000)
XLA Ops:
  0.0 1.2 copy-done
  1.2 1.2 copy-done.14
  2.5 1.2 copy-done.16
  5.3 2.1 %collective-permute-start = (bf16[64,1024]{1,0:T(8,128)(2,1)S(1)}, bf16[64,1024]{1,0:T(8,128)(2,1)S(1)}, u32[]{:S(2)}, u32[]{:S(2)}) collective-permute-start(bf16[64,1024]{1,0:T(8,128)(2,1)S(1)} %get-tuple-element.21), channel_id=1, source_target_pairs={{0,2},{1,3},{2,0},{3,1},{4,6},{5,7},{6,4},{7,5},{8,10},{9,11},{10,... | collective-permute-start | bytes 393224 | tf_op jit(solution)/shard_map/ppermute | solution.py:551
  7.4 3.2 %collective-permute-done.refs_0_ = bf16[64,1024]{1,0:T(8,128)(2,1)S(1)} collective-permute-done((bf16[64,1024]{1,0:T(8,128)(2,1)S(1)}, bf16[64,1024]{1,0:T(8,128)(2,1)S(1)}, u32[]{:S(2)}, u32[]{:S(2)}) %collective-permute-start) | collective-permute-done | bytes 131104 | tf_op jit(solution)/shard_map/ppermute | solution.py:551
  11.7 5.5 %all-to-all-start = ((bf16[8,1,64,1024]{3,2,1,0:T(8,128)(2,1)}), bf16[8,1,64,1024]{3,2,1,0:T(8,128)(2,1)}, u32[]{:S(2)}, u32[]{:S(2)}) async-start(bf16[8,1,64,1024]{3,2,1,0:T(8,128)(2,1)} %copy-done.13), calls=%async_computation | async-start | bytes 2097152 | tf_op jit(solution)/shard_map/all_to_all | solution.py:578
  17.2 1.9 %collective-permute-start.4 = (bf16[1024,512]{1,0:T(8,128)(2,1)S(1)}, bf16[1024,512]{1,0:T(8,128)(2,1)S(1)}, u32[]{:S(2)}, u32[]{:S(2)}) collective-permute-start(bf16[1024,512]{1,0:T(8,128)(2,1)S(1)} %copy-done.1), channel_id=1, source_target_pairs={{0,1},{1,0},{2,3},{3,2},{4,5},{5,4},{6,7},{7,6},{8,9},{9,8},{10,11... | collective-permute-start | bytes 3145736 | tf_op jit(solution)/shard_map/ppermute | solution.py:546
  19.0 1.2 collective-permute-start.9
  20.5 1.2 collective-permute-start.7
  21.7 10.7 %collective-permute-done.9.refs_9_ = bf16[512,512]{1,0:T(8,128)(2,1)S(1)} collective-permute-done((bf16[512,512]{1,0:T(8,128)(2,1)S(1)}, bf16[512,512]{1,0:T(8,128)(2,1)S(1)}, u32[]{:S(2)}, u32[]{:S(2)}) %collective-permute-start.9) | collective-permute-done | bytes 524320 | tf_op jit(solution)/shard_map/ppermute | solution.py:551
  32.4 1.5 %collective-permute-start.10 = (bf16[512,512]{1,0:T(8,128)(2,1)S(1)}, bf16[512,512]{1,0:T(8,128)(2,1)S(1)}, u32[]{:S(2)}, u32[]{:S(2)}) collective-permute-start(bf16[512,512]{1,0:T(8,128)(2,1)S(1)} %collective-permute-done.9.refs_9_), channel_id=1, source_target_pairs={{0,1},{1,0},{2,3},{3,2},{4,5},{5,4},{6,7},{7,6},{8,9},{9,8},{10,11... | collective-permute-start | bytes 1572872 | tf_op jit(solution)/shard_map/ppermute | solution.py:546
  33.9 4.2 %collective-permute-done.5.refs_9_ = bf16[256,512]{1,0:T(8,128)(2,1)S(1)} collective-permute-done((bf16[256,512]{1,0:T(8,128)(2,1)}, bf16[256,512]{1,0:T(8,128)(2,1)S(1)}, u32[]{:S(2)}, u32[]{:S(2)}) %collective-permute-start.5) | collective-permute-done | bytes 262176 | tf_op jit(solution)/shard_map/ppermute | solution.py:551
  38.2 1.4 %collective-permute-start.6 = (bf16[256,512]{1,0:T(8,128)(2,1)S(1)}, bf16[256,512]{1,0:T(8,128)(2,1)S(1)}, u32[]{:S(2)}, u32[]{:S(2)}) collective-permute-start(bf16[256,512]{1,0:T(8,128)(2,1)S(1)} %collective-permute-done.5.refs_9_), channel_id=1, source_target_pairs={{0,1},{1,0},{2,3},{3,2},{4,5},{5,4},{6,7},{7,6},{8,9},{9,8},{10,11... | collective-permute-start | bytes 786440 | tf_op jit(solution)/shard_map/ppermute | solution.py:546
  39.5 4.2 %collective-permute-done.7.refs_9_ = bf16[256,512]{1,0:T(8,128)(2,1)S(1)} collective-permute-done((bf16[256,512]{1,0:T(8,128)(2,1)}, bf16[256,512]{1,0:T(8,128)(2,1)S(1)}, u32[]{:S(2)}, u32[]{:S(2)}) %collective-permute-start.7) | collective-permute-done | bytes 262176 | tf_op jit(solution)/shard_map/ppermute | solution.py:551
  45.5 1.2 copy-done.3
  46.7 1.2 copy-done.4
  51.0 3.4 %project.3 = (bf16[5,256,256]{2,1,0:T(8,128)(2,1)S(1)}, f32[2,64,256]{2,1,0:T(8,128)S(1)}, bf16[128,256]{1,0:T(8,128)(2,1)}, bf16[128,256]{1,0:T(8,128)(2,1)S(1)}) custom-call(f32[1,2048]{1,0:T(1,128)S(1)} %bitcast.1, f32[8,1024]{1,0:T(8,128)S(1)} %get-tuple-element.22.refs_1_.refs_0_, f32[1024,8]{1,0:T(8,128)S(1)} %get-tuple-element.23.refs_2_.refs_0_.refs_1_, ...), custom_call_target="tpu_custom_call" | custom-call | flops 335544320 | bytes 7340032 | tf_op jit(solution)/shard_map/project/pallas_call | solution.py:230
  55.3 3.4 %project.4 = (bf16[5,256,256]{2,1,0:T(8,128)(2,1)S(1)}, f32[2,64,256]{2,1,0:T(8,128)S(1)}, bf16[128,256]{1,0:T(8,128)(2,1)}, bf16[128,256]{1,0:T(8,128)(2,1)}) custom-call(f32[1,2048]{1,0:T(1,128)S(1)} %bitcast.2, f32[8,1024]{1,0:T(8,128)S(1)} %get-tuple-element.22.refs_1_.refs_0_, f32[1024,8]{1,0:T(8,128)S(1)} %get-tuple-element.23.refs_2_.refs_0_.refs_1_, ...), custom_call_target="tpu_custom_call" | custom-call | flops 335544320 | bytes 7340032 | tf_op jit(solution)/shard_map/project/pallas_call | solution.py:230
  59.5 5.7 %project.5 = (bf16[5,512,256]{2,1,0:T(8,128)(2,1)S(1)}, f32[2,64,256]{2,1,0:T(8,128)S(1)}, bf16[128,256]{1,0:T(8,128)(2,1)S(1)}, bf16[128,256]{1,0:T(8,128)(2,1)}) custom-call(f32[1,2048]{1,0:T(1,128)S(1)} %bitcast.3, f32[8,1024]{1,0:T(8,128)S(1)} %get-tuple-element.22.refs_1_.refs_0_, f32[1024,8]{1,0:T(8,128)S(1)} %get-tuple-element.23.refs_2_.refs_0_.refs_1_, ...), custom_call_target="tpu_custom_call" | custom-call | flops 671088640 | bytes 7340032 | tf_op jit(solution)/shard_map/project/pallas_call | solution.py:230
  67.2 5.7 %all-to-all-start.1 = ((bf16[8,2,80,128]{3,2,1,0:T(8,128)(2,1)}), bf16[8,2,80,128]{3,2,1,0:T(8,128)(2,1)}, u32[]{:S(2)}, u32[]{:S(2)}) async-start(bf16[8,2,80,128]{3,2,1,0:T(8,128)(2,1)} %totals.1), calls=%async_computation.1 | async-start | bytes 655360 | tf_op jit(solution)/shard_map/all_to_all | solution.py:666
  73.3 1.5 %collective-permute-start.11 = (bf16[128,256]{1,0:T(8,128)(2,1)S(1)}, bf16[128,256]{1,0:T(8,128)(2,1)S(1)}, u32[]{:S(2)}, u32[]{:S(2)}) collective-permute-start(bf16[128,256]{1,0:T(8,128)(2,1)S(1)} %get-tuple-element.32), channel_id=1, source_target_pairs={{0,4},{4,8},{8,12},{12,16},{16,20},{20,24},{24,28},{28,0},{1,5},{5... | collective-permute-start | bytes 196616 | tf_op jit(solution)/shard_map/ppermute | solution.py:662
  74.9 2.7 %collective-permute-start.12 = (bf16[128,256]{1,0:T(8,128)(2,1)S(1)}, bf16[128,256]{1,0:T(8,128)(2,1)S(1)}, u32[]{:S(2)}, u32[]{:S(2)}) collective-permute-start(bf16[128,256]{1,0:T(8,128)(2,1)S(1)} %get-tuple-element.33), channel_id=1, source_target_pairs={{4,0},{8,4},{12,8},{16,12},{20,16},{24,20},{28,24},{0,28},{5,1},{9... | collective-permute-start | bytes 196616 | tf_op jit(solution)/shard_map/ppermute | solution.py:663
  77.6 6.5 %collective-permute-done.11.refs_4_ = bf16[128,256]{1,0:T(8,128)(2,1)S(1)} collective-permute-done((bf16[128,256]{1,0:T(8,128)(2,1)S(1)}, bf16[128,256]{1,0:T(8,128)(2,1)S(1)}, u32[]{:S(2)}, u32[]{:S(2)}) %collective-permute-start.11) | collective-permute-done | bytes 65568 | tf_op jit(solution)/shard_map/ppermute | solution.py:662
  84.1 1.3 %copy-done.7 = bf16[5,512,256]{2,1,0:T(8,128)(2,1)S(1)} copy-done((bf16[5,512,256]{2,1,0:T(8,128)(2,1)S(1)}, bf16[5,512,256]{2,1,0:T(8,128)(2,1)}, u32[]{:S(2)}) %copy-start.7) | copy-done | bytes 1310744
  87.6 4.7 %attend.1.refs_6_ = bf16[1024,256]{1,0:T(8,128)(2,1)} custom-call(f32[4]{0:T(128)S(1)} %copy-done.34, bf16[5,256,256]{2,1,0:T(8,128)(2,1)S(1)} %copy-done.19, bf16[5,256,256]{2,1,0:T(8,128)(2,1)S(1)} %copy-done.22, bf16[5,512,256]{2,1,0:T(8,128)(2,1)S(1)} %copy-done.7, bf16[128,256]{1,0:T(8,128)(2,1)S(1)} %collective-permute-done.11.refs_4_, ...), custom_call_target="tpu_custom_call" | custom-call | flops 1500000000 | bytes 3145728 | tf_op jit(solution)/shard_map/attend/pallas_call | solution.py:322
  92.3 1.2 collective-permute-start.14
  93.5 1.7 %collective-permute-start.1 = (bf16[8,1,64,1024]{3,2,1,0:T(8,128)(2,1)}, bf16[8,1,64,1024]{3,2,1,0:T(8,128)(2,1)}, u32[]{:S(2)}, u32[]{:S(2)}) collective-permute-start(bf16[8,1,64,1024]{3,2,1,0:T(8,128)(2,1)} %all-to-all-done.refs_4_.refs_0_), channel_id=1, source_target_pairs={{0,1},{1,0},{2,3},{3,2},{4,5},{5,4},{6,7},{7,6},{8,9},{9,8},{10,11... | collective-permute-start | bytes 3145736 | tf_op jit(solution)/shard_map/ppermute | solution.py:546
  95.3 3.3 %local.1.refs_4_ = f32[1024,256]{1,0:T(8,128)S(1)} custom-call(f32[1024,8]{1,0:T(8,128)S(1)} %get-tuple-element.23.refs_2_.refs_0_.refs_1_, f32[8,1024]{1,0:T(8,128)S(1)} %copy-done.25, bf16[5,256,256]{2,1,0:T(8,128)(2,1)S(1)} %copy-done.20, bf16[5,256,256]{2,1,0:T(8,128)(2,1)S(1)} %copy-done.22, bf16[5,512,256]{2,1,0:T(8,128)(2,1)S(1)} %copy-done.8), custom_call_target="tpu_custom_call" | custom-call | flops 1000000000 | bytes 3145728 | tf_op jit(solution)/shard_map/local/pallas_call | solution.py:409
  101.3 5.6 %cross.1.refs_10_ = bf16[1024,256]{1,0:T(8,128)(2,1)S(1)} custom-call(f32[8,1024]{1,0:T(8,128)S(1)} %copy-done.26, f32[1024,8]{1,0:T(8,128)S(1)} %get-tuple-element.23.refs_2_.refs_0_.refs_1_, bf16[8,2,80,128]{3,2,1,0:T(8,128)(2,1)} %all-to-all-done.1.refs_2_, f32[2,2,64,128]{3,2,1,0:T(8,128)S(1)} %copy-done.29, f32[1024,256]{1,0:T(8,128)S(1)} %local.1.refs_4_, ...), custom_call_target="tpu_custom_call" | custom-call | flops 500000000 | bytes 4194304 | tf_op jit(solution)/shard_map/cross/pallas_call | solution.py:478
  108.0 12.4 %collective-permute-done.17.refs_3_ = bf16[1024,256]{1,0:T(8,128)(2,1)S(1)} collective-permute-done((bf16[1024,256]{1,0:T(8,128)(2,1)S(1)}, bf16[1024,256]{1,0:T(8,128)(2,1)S(1)}, u32[]{:S(2)}, u32[]{:S(2)}) %collective-permute-start.17) | collective-permute-done | bytes 524320 | tf_op jit(solution)/shard_map/ppermute | solution.py:551
  121.4 4.3 %shard_map.154.refs_2_ = f32[1024,512]{1,0:T(8,128)S(1)} custom-call(bf16[256,2048]{1,0:T(8,128)(2,1)S(1)} %copy-done.15, bf16[256,2048]{1,0:T(8,128)(2,1)S(1)} %copy-done.17, bf16[256,2048]{1,0:T(8,128)(2,1)} %collective-permute-done.2.refs_2_, bf16[256,2048]{1,0:T(8,128)(2,1)} %collective-permute-done.3.refs_3_, ...), custom_call_target="tpu_custom_call" | custom-call | flops 1000000000 | bytes 8388608 | tf_op jit(solution)/shard_map/pallas_call | solution.py:534
  125.6 3.2 %shard_map.155 = bf16[1024,512]{1,0:T(8,128)(2,1)} custom-call(bf16[8,1,64,1024]{3,2,1,0:T(8,128)(2,1)} %all-to-all-done.refs_4_.refs_0_, bf16[8,1,64,1024]{3,2,1,0:T(8,128)(2,1)} %collective-permute-done.1.refs_5_.refs_1_, f32[1024,512]{1,0:T(8,128)S(1)} %shard_map.154.refs_2_, bf16[1024,256]{1,0:T(8,128)(2,1)S(1)} %collective-permute-done.17.refs_3_, ...), custom_call_target="tpu_custom_call" | custom-call | flops 1000000000 | bytes 8388608 | tf_op jit(solution)/shard_map/pallas_call | solution.py:534
  (92 shorter events, 18.7 us)
Async XLA Ops:
  5.3 11.9 %copy-start.1 = (bf16[1024,512]{1,0:T(8,128)(2,1)S(1)}, bf16[1024,512]{1,0:T(8,128)(2,1)}, u32[]{:S(2)}) copy-start(bf16[1024,512]{1,0:T(8,128)(2,1)} %refs_7_.5) | copy-start | bytes 3145732
  5.3 39.3 %copy-start.33 = (f32[2,1024]{1,0:T(2,128)S(1)}, f32[2,1024]{1,0:T(2,128)}, u32[]{:S(2)}) copy-start(f32[2,1024]{1,0:T(2,128)} %log_ref.1) | copy-start | bytes 24580
  5.3 40.1 %copy-start.2 = (bf16[2048,256]{1,0:T(8,128)(2,1)S(1)}, bf16[2048,256]{1,0:T(8,128)(2,1)}, u32[]{:S(2)}) copy-start(bf16[2048,256]{1,0:T(8,128)(2,1)} %refs_11_.5) | copy-start | bytes 3145732
  5.3 40.2 %copy-start.9 = (bf16[2048,128]{1,0:T(8,128)(2,1)S(1)}, bf16[2048,128]{1,0:T(8,128)(2,1)}, u32[]{:S(2)}) copy-start(bf16[2048,128]{1,0:T(8,128)(2,1)} %refs_12_.5) | copy-start | bytes 1572868
  5.3 40.2 %copy-start.27 = (bf16[256,256]{1,0:T(8,128)(2,1)S(1)}, bf16[256,256]{1,0:T(8,128)(2,1)}, u32[]{:S(2)}) copy-start(bf16[256,256]{1,0:T(8,128)(2,1)} %constant.5.clone.refs_4_) | copy-start | bytes 393220
  5.3 40.2 %copy-start.28 = (bf16[128,128]{1,0:T(8,128)(2,1)S(1)}, bf16[128,128]{1,0:T(8,128)(2,1)}, u32[]{:S(2)}) copy-start(bf16[128,128]{1,0:T(8,128)(2,1)} %constant.4.clone.refs_3_) | copy-start | bytes 98308
  5.3 40.2 %copy-start.30 = (f32[2048]{0:T(1024)S(1)}, f32[2048]{0:T(1024)}, u32[]{:S(2)}) copy-start(f32[2048]{0:T(1024)} %param.17) | copy-start | bytes 24580
  5.3 5.3 %collective-permute-start = (bf16[64,1024]{1,0:T(8,128)(2,1)S(1)}, bf16[64,1024]{1,0:T(8,128)(2,1)S(1)}, u32[]{:S(2)}, u32[]{:S(2)}) collective-permute-start(bf16[64,1024]{1,0:T(8,128)(2,1)S(1)} %get-tuple-element.21), channel_id=1, source_target_pairs={{0,2},{1,3},{2,0},{3,1},{4,6},{5,7},{6,4},{7,5},{8,10},{9,11},{10,... | collective-permute-start | bytes 393224 | tf_op jit(solution)/shard_map/ppermute | solution.py:551
  11.7 55.5 %all-to-all-start = ((bf16[8,1,64,1024]{3,2,1,0:T(8,128)(2,1)}), bf16[8,1,64,1024]{3,2,1,0:T(8,128)(2,1)}, u32[]{:S(2)}, u32[]{:S(2)}) async-start(bf16[8,1,64,1024]{3,2,1,0:T(8,128)(2,1)} %copy-done.13), calls=%async_computation | async-start | bytes 2097152 | tf_op jit(solution)/shard_map/all_to_all | solution.py:578
  17.2 28.2 %collective-permute-start.4 = (bf16[1024,512]{1,0:T(8,128)(2,1)S(1)}, bf16[1024,512]{1,0:T(8,128)(2,1)S(1)}, u32[]{:S(2)}, u32[]{:S(2)}) collective-permute-start(bf16[1024,512]{1,0:T(8,128)(2,1)S(1)} %copy-done.1), channel_id=1, source_target_pairs={{0,1},{1,0},{2,3},{3,2},{4,5},{5,4},{6,7},{7,6},{8,9},{9,8},{10,11... | collective-permute-start | bytes 3145736 | tf_op jit(solution)/shard_map/ppermute | solution.py:546
  19.0 13.4 %collective-permute-start.9 = (bf16[512,512]{1,0:T(8,128)(2,1)S(1)}, bf16[512,512]{1,0:T(8,128)(2,1)S(1)}, u32[]{:S(2)}, u32[]{:S(2)}) collective-permute-start(bf16[512,512]{1,0:T(8,128)(2,1)S(1)} %get-tuple-element.30), channel_id=1, source_target_pairs={{0,2},{1,3},{2,0},{3,1},{4,6},{5,7},{6,4},{7,5},{8,10},{9,11},{10,... | collective-permute-start | bytes 1572872 | tf_op jit(solution)/shard_map/ppermute | solution.py:551
  20.3 17.9 %collective-permute-start.5 = (bf16[256,512]{1,0:T(8,128)(2,1)}, bf16[256,512]{1,0:T(8,128)(2,1)S(1)}, u32[]{:S(2)}, u32[]{:S(2)}) collective-permute-start(bf16[256,512]{1,0:T(8,128)(2,1)} %copy-done.32), channel_id=1, source_target_pairs={{0,2},{1,3},{2,0},{3,1},{4,6},{5,7},{6,4},{7,5},{8,10},{9,11},{10,... | collective-permute-start | bytes 786440 | tf_op jit(solution)/shard_map/ppermute | solution.py:551
  20.5 23.3 %collective-permute-start.7 = (bf16[256,512]{1,0:T(8,128)(2,1)}, bf16[256,512]{1,0:T(8,128)(2,1)S(1)}, u32[]{:S(2)}, u32[]{:S(2)}) collective-permute-start(bf16[256,512]{1,0:T(8,128)(2,1)} %copy-done.31), channel_id=1, source_target_pairs={{0,2},{1,3},{2,0},{3,1},{4,6},{5,7},{6,4},{7,5},{8,10},{9,11},{10,... | collective-permute-start | bytes 786440 | tf_op jit(solution)/shard_map/ppermute | solution.py:551
  32.4 27.1 %collective-permute-start.10 = (bf16[512,512]{1,0:T(8,128)(2,1)S(1)}, bf16[512,512]{1,0:T(8,128)(2,1)S(1)}, u32[]{:S(2)}, u32[]{:S(2)}) collective-permute-start(bf16[512,512]{1,0:T(8,128)(2,1)S(1)} %collective-permute-done.9.refs_9_), channel_id=1, source_target_pairs={{0,1},{1,0},{2,3},{3,2},{4,5},{5,4},{6,7},{7,6},{8,9},{9,8},{10,11... | collective-permute-start | bytes 1572872 | tf_op jit(solution)/shard_map/ppermute | solution.py:546
  38.2 7.2 %collective-permute-start.6 = (bf16[256,512]{1,0:T(8,128)(2,1)S(1)}, bf16[256,512]{1,0:T(8,128)(2,1)S(1)}, u32[]{:S(2)}, u32[]{:S(2)}) collective-permute-start(bf16[256,512]{1,0:T(8,128)(2,1)S(1)} %collective-permute-done.5.refs_9_), channel_id=1, source_target_pairs={{0,1},{1,0},{2,3},{3,2},{4,5},{5,4},{6,7},{7,6},{8,9},{9,8},{10,11... | collective-permute-start | bytes 786440 | tf_op jit(solution)/shard_map/ppermute | solution.py:546
  43.8 11.5 %collective-permute-start.8 = (bf16[256,512]{1,0:T(8,128)(2,1)S(1)}, bf16[256,512]{1,0:T(8,128)(2,1)S(1)}, u32[]{:S(2)}, u32[]{:S(2)}) collective-permute-start(bf16[256,512]{1,0:T(8,128)(2,1)S(1)} %collective-permute-done.7.refs_9_), channel_id=1, source_target_pairs={{0,1},{1,0},{2,3},{3,2},{4,5},{5,4},{6,7},{7,6},{8,9},{9,8},{10,11... | collective-permute-start | bytes 786440 | tf_op jit(solution)/shard_map/ppermute | solution.py:546
  45.4 20.9 %copy-start.24 = (f32[8,1024]{1,0:T(8,128)}, f32[8,1024]{1,0:T(8,128)S(1)}, u32[]{:S(2)}) copy-start(f32[8,1024]{1,0:T(8,128)S(1)} %get-tuple-element.22.refs_1_.refs_0_) | copy-start | bytes 98308
  59.5 24.5 %copy-start.34 = (f32[4]{0:T(128)S(1)}, f32[4]{0:T(128)}, u32[]{:S(2)}) copy-start(f32[4]{0:T(128)} %refs_0_.4) | copy-start | bytes 52
  67.2 31.4 %all-to-all-start.1 = ((bf16[8,2,80,128]{3,2,1,0:T(8,128)(2,1)}), bf16[8,2,80,128]{3,2,1,0:T(8,128)(2,1)}, u32[]{:S(2)}, u32[]{:S(2)}) async-start(bf16[8,2,80,128]{3,2,1,0:T(8,128)(2,1)} %totals.1), calls=%async_computation.1 | async-start | bytes 655360 | tf_op jit(solution)/shard_map/all_to_all | solution.py:666
  72.8 34.4 %collective-permute-start.2 = (bf16[256,2048]{1,0:T(8,128)(2,1)}, bf16[256,2048]{1,0:T(8,128)(2,1)}, u32[]{:S(2)}, u32[]{:S(2)}) collective-permute-start(bf16[256,2048]{1,0:T(8,128)(2,1)} %refs_0_.5), channel_id=1, source_target_pairs={{0,1},{1,0},{2,3},{3,2},{4,5},{5,4},{6,7},{7,6},{8,9},{9,8},{10,11... | collective-permute-start | bytes 3145736 | tf_op jit(solution)/shard_map/ppermute | solution.py:546
  73.1 34.4 %collective-permute-start.3 = (bf16[256,2048]{1,0:T(8,128)(2,1)}, bf16[256,2048]{1,0:T(8,128)(2,1)}, u32[]{:S(2)}, u32[]{:S(2)}) collective-permute-start(bf16[256,2048]{1,0:T(8,128)(2,1)} %refs_1_.3), channel_id=1, source_target_pairs={{0,1},{1,0},{2,3},{3,2},{4,5},{5,4},{6,7},{7,6},{8,9},{9,8},{10,11... | collective-permute-start | bytes 3145736 | tf_op jit(solution)/shard_map/ppermute | solution.py:546
  73.3 10.7 %collective-permute-start.11 = (bf16[128,256]{1,0:T(8,128)(2,1)S(1)}, bf16[128,256]{1,0:T(8,128)(2,1)S(1)}, u32[]{:S(2)}, u32[]{:S(2)}) collective-permute-start(bf16[128,256]{1,0:T(8,128)(2,1)S(1)} %get-tuple-element.32), channel_id=1, source_target_pairs={{0,4},{4,8},{8,12},{12,16},{16,20},{20,24},{24,28},{28,0},{1,5},{5... | collective-permute-start | bytes 196616 | tf_op jit(solution)/shard_map/ppermute | solution.py:662
  74.9 9.2 %collective-permute-start.12 = (bf16[128,256]{1,0:T(8,128)(2,1)S(1)}, bf16[128,256]{1,0:T(8,128)(2,1)S(1)}, u32[]{:S(2)}, u32[]{:S(2)}) collective-permute-start(bf16[128,256]{1,0:T(8,128)(2,1)S(1)} %get-tuple-element.33), channel_id=1, source_target_pairs={{4,0},{8,4},{12,8},{16,12},{20,16},{24,20},{28,24},{0,28},{5,1},{9... | collective-permute-start | bytes 196616 | tf_op jit(solution)/shard_map/ppermute | solution.py:663
  92.3 15.4 %collective-permute-start.14 = (bf16[1024,256]{1,0:T(8,128)(2,1)}, bf16[1024,256]{1,0:T(8,128)(2,1)}, u32[]{:S(2)}, u32[]{:S(2)}) collective-permute-start(bf16[1024,256]{1,0:T(8,128)(2,1)} %attend.1.refs_6_), channel_id=1, source_target_pairs={{0,2},{1,3},{2,0},{3,1},{4,6},{5,7},{6,4},{7,5},{8,10},{9,11},{10,... | collective-permute-start | bytes 1572872 | tf_op jit(solution)/shard_map/ppermute | solution.py:551
  93.5 27.8 %collective-permute-start.1 = (bf16[8,1,64,1024]{3,2,1,0:T(8,128)(2,1)}, bf16[8,1,64,1024]{3,2,1,0:T(8,128)(2,1)}, u32[]{:S(2)}, u32[]{:S(2)}) collective-permute-start(bf16[8,1,64,1024]{3,2,1,0:T(8,128)(2,1)} %all-to-all-done.refs_4_.refs_0_), channel_id=1, source_target_pairs={{0,1},{1,0},{2,3},{3,2},{4,5},{5,4},{6,7},{7,6},{8,9},{9,8},{10,11... | collective-permute-start | bytes 3145736 | tf_op jit(solution)/shard_map/ppermute | solution.py:546
  101.3 20.0 %copy-start.15 = (bf16[256,2048]{1,0:T(8,128)(2,1)S(1)}, bf16[256,2048]{1,0:T(8,128)(2,1)}, u32[]{:S(2)}) copy-start(bf16[256,2048]{1,0:T(8,128)(2,1)} %refs_0_.5) | copy-start | bytes 3145732
  101.3 20.1 %copy-start.17 = (bf16[256,2048]{1,0:T(8,128)(2,1)S(1)}, bf16[256,2048]{1,0:T(8,128)(2,1)}, u32[]{:S(2)}) copy-start(bf16[256,2048]{1,0:T(8,128)(2,1)} %refs_1_.3) | copy-start | bytes 3145732
  106.9 13.5 %collective-permute-start.17 = (bf16[1024,256]{1,0:T(8,128)(2,1)S(1)}, bf16[1024,256]{1,0:T(8,128)(2,1)S(1)}, u32[]{:S(2)}, u32[]{:S(2)}) collective-permute-start(bf16[1024,256]{1,0:T(8,128)(2,1)S(1)} %cross.1.refs_10_), channel_id=1, source_target_pairs={{0,2},{1,3},{2,0},{3,1},{4,6},{5,7},{6,4},{7,5},{8,10},{9,11},{10,... | collective-permute-start | bytes 1572872 | tf_op jit(solution)/shard_map/ppermute | solution.py:551
  107.2 14.1 %collective-permute-start.13 = (bf16[1024,256]{1,0:T(8,128)(2,1)}, bf16[1024,256]{1,0:T(8,128)(2,1)S(1)}, u32[]{:S(2)}, u32[]{:S(2)}) collective-permute-start(bf16[1024,256]{1,0:T(8,128)(2,1)} %attend.1.refs_6_), channel_id=1, source_target_pairs={{0,1},{1,0},{2,3},{3,2},{4,5},{5,4},{6,7},{7,6},{8,9},{9,8},{10,11... | collective-permute-start | bytes 1572872 | tf_op jit(solution)/shard_map/ppermute | solution.py:546
  107.5 13.8 %collective-permute-start.16 = (bf16[1024,256]{1,0:T(8,128)(2,1)S(1)}, bf16[1024,256]{1,0:T(8,128)(2,1)S(1)}, u32[]{:S(2)}, u32[]{:S(2)}) collective-permute-start(bf16[1024,256]{1,0:T(8,128)(2,1)S(1)} %cross.1.refs_10_), channel_id=1, source_target_pairs={{0,1},{1,0},{2,3},{3,2},{4,5},{5,4},{6,7},{7,6},{8,9},{9,8},{10,11... | collective-permute-start | bytes 1572872 | tf_op jit(solution)/shard_map/ppermute | solution.py:546
  107.7 13.6 %collective-permute-start.15 = (bf16[1024,256]{1,0:T(8,128)(2,1)}, bf16[1024,256]{1,0:T(8,128)(2,1)S(1)}, u32[]{:S(2)}, u32[]{:S(2)}) collective-permute-start(bf16[1024,256]{1,0:T(8,128)(2,1)} %collective-permute-done.14.refs_8_), channel_id=1, source_target_pairs={{0,1},{1,0},{2,3},{3,2},{4,5},{5,4},{6,7},{7,6},{8,9},{9,8},{10,11... | collective-permute-start | bytes 1572872 | tf_op jit(solution)/shard_map/ppermute | solution.py:546
  120.4 5.2 %collective-permute-start.18 = (bf16[1024,256]{1,0:T(8,128)(2,1)S(1)}, bf16[1024,256]{1,0:T(8,128)(2,1)S(1)}, u32[]{:S(2)}, u32[]{:S(2)}) collective-permute-start(bf16[1024,256]{1,0:T(8,128)(2,1)S(1)} %collective-permute-done.17.refs_3_), channel_id=1, source_target_pairs={{0,1},{1,0},{2,3},{3,2},{4,5},{5,4},{6,7},{7,6},{8,9},{9,8},{10,11... | collective-permute-start | bytes 1572872 | tf_op jit(solution)/shard_map/ppermute | solution.py:546
  (24 other events, 48.1 us)

commit v3 on v2

--- a/solution.py
+++ b/solution.py
@@ -26,7 +26,7 @@
 
 VMEM = pl.BlockSpec(memory_space=pltpu.VMEM)
 SMEM = pl.BlockSpec(memory_space=pltpu.SMEM)
-ANY = pl.BlockSpec(memory_space=pl.ANY)
+HBM = pl.BlockSpec(memory_space=pltpu.HBM)
 PARAMS = pltpu.CompilerParams(vmem_limit_bytes=16 << 20)
 
 
@@ -46,58 +46,90 @@
     return lax.dot_general(a, b, (((0,), (0,)), ((), ())), preferred_element_type=F32)
 
 
-def split_kernel(n_pieces, n_far, *refs):
-    tokens, att, ret = refs[:3]
-    pieces = refs[3 : 3 + n_pieces]
-    slabs = refs[3 + n_pieces : 3 + n_pieces + n_far]
-    sems = refs[-1]
-    n_tp = lax.axis_size("tp")
+def in_vmem(values):
+    return [pltpu.with_memory_space_constraint(v, pltpu.VMEM) for v in values]
+
+
+def in_hbm(values):
+    return [pltpu.with_memory_space_constraint(v, pltpu.HBM) for v in values]
+
+
+class Copies:
+    def __init__(self, sems):
+        self.sems = sems
+        self.copies = []
+
+    def start(self, src, dst):
+        copy = pltpu.make_async_copy(src, dst, self.sems.at[len(self.copies)])
+        copy.start()
+        self.copies.append(copy)
+
+    def wait(self, first=0, last=None):
+        for copy in self.copies[first:last]:
+            copy.wait()
+
+
+def slab_kernel(n_far, *refs):
+    att, ret = refs[:2]
+    slabs = refs[2 : 2 + n_far]
+    copies = Copies(refs[-1])
     tp, sp = lax.axis_index("tp"), lax.axis_index("sp")
-    chips = n_tp // 2
-    copies = []
-    for by in range(1, chips):
-        slab = slabs[by - 1]
+    chips = n_far + 1
+    for by, slab in enumerate(slabs, 1):
         share, width = slab.shape[0] // 2, slab.shape[1]
         target = lax.rem(tp // 2 + by, chips)
         rows = pl.ds(pl.multiple_of(sp * share, share), share)
         cols = pl.ds(pl.multiple_of(target * width, width), width)
         for i, ref in enumerate((att, ret)):
-            dst = slab.at[pl.ds(i * share, share)]
-            copies.append(pltpu.make_async_copy(ref.at[rows, cols], dst, sems.at[2 * by - 2 + i]))
-    for copy in copies:
-        copy.start()
-    for c, piece in enumerate(pieces):
-        first = CHUNKS[c][0] * tokens.shape[0] // 4
-        piece[...] = tokens[first : first + piece.shape[0]]
-    for copy in copies:
-        copy.wait()
-
-
-def split(tokens, att, ret):
-    total, cols = tokens.shape
+            copies.start(ref.at[rows, cols], slab.at[pl.ds(i * share, share)])
+    copies.wait()
+
+
+def slab(att, ret, cols):
     chips = lax.axis_size("tp") // 2
     share = att.shape[0] // lax.axis_size("sp")
-    shapes = [jax.ShapeDtypeStruct((n * total // 4, cols), BF16) for _, n in CHUNKS]
-    shapes += [jax.ShapeDtypeStruct((2 * share, 2 * cols), BF16)] * (chips - 1)
     if share % 16:
         rows = lax.axis_index("sp") * share
-        out = [tokens[f * total // 4 : (f + n) * total // 4] for f, n in CHUNKS]
+        out = []
         for by in range(1, chips):
             target = lax.rem(lax.axis_index("tp") // 2 + by, chips) * 2 * cols
             parts = [lax.dynamic_slice(w, (rows, target), (share, 2 * cols)) for w in (att, ret)]
             out.append(jnp.concatenate(parts, axis=0))
-    else:
-        out = pl.pallas_call(
-            functools.partial(split_kernel, len(CHUNKS), chips - 1),
-            out_shape=tuple(shapes),
-            in_specs=[VMEM, ANY, ANY],
-            out_specs=(VMEM,) * len(shapes),
-            scratch_shapes=[pltpu.SemaphoreType.DMA((2 * chips,))],
-            cost_estimate=cost(0.1e9, 3 << 20),
-            compiler_params=PARAMS,
-            name="split",
-        )(tokens, att, ret)
-    return out[: len(CHUNKS)], out[len(CHUNKS) :]
+        return out
+    return pl.pallas_call(
+        functools.partial(slab_kernel, chips - 1),
+        out_shape=(jax.ShapeDtypeStruct((2 * share, 2 * cols), BF16),) * (chips - 1),
+        in_specs=[HBM, HBM],
+        out_specs=(VMEM,) * (chips - 1),
+        scratch_shapes=[pltpu.SemaphoreType.DMA((2 * chips,))],
+        cost_estimate=cost(0.1e9, 3 << 20),
+        compiler_params=PARAMS,
+        name="slab",
+    )(*in_hbm([att, ret]))
+
+
+def split_kernel(n_pieces, *refs):
+    tokens = refs[0]
+    pieces = refs[1 : 1 + n_pieces]
+    copies = Copies(refs[-1])
+    for (first, _), piece in zip(CHUNKS, pieces):
+        rows = pl.ds(first * tokens.shape[0] // 4, piece.shape[0])
+        copies.start(tokens.at[rows], piece)
+    copies.wait()
+
+
+def split(tokens):
+    total, cols = tokens.shape
+    return pl.pallas_call(
+        functools.partial(split_kernel, len(CHUNKS)),
+        out_shape=tuple(jax.ShapeDtypeStruct((n * total // 4, cols), BF16) for _, n in CHUNKS),
+        in_specs=[HBM],
+        out_specs=(VMEM,) * len(CHUNKS),
+        scratch_shapes=[pltpu.SemaphoreType.DMA((len(CHUNKS),))],
+        cost_estimate=cost(0.1e9, 3 << 20),
+        compiler_params=PARAMS,
+        name="split",
+    )(*in_hbm([tokens]))
 
 
 def repeat_kernel(*refs):
@@ -119,7 +151,8 @@
     )(*slabs)
 
 
-def prepare_kernel(log_ref, row_ref, col_ref, cos_ref, sin_ref):
+def prepare_kernel(log_ref, *refs):
+    row_ref, col_ref, cos_ref, sin_ref = refs[-4:]
     total = log_ref.shape[1]
     heads = log_ref.shape[0]
     sums = jnp.concatenate([log_ref[...], jnp.zeros((8 - heads, total), F32)], axis=0)
@@ -141,36 +174,37 @@
     sin_ref[...] = jnp.sin(angles)
 
 
-def prepare(log):
+def prepare(log, weights):
     heads, total = log.shape
     table = jax.ShapeDtypeStruct((total // TABLE + TABLE, heads * RK), F32)
     return pl.pallas_call(
         prepare_kernel,
         out_shape=(
-            jax.ShapeDtypeStruct((8, total), F32),
-            jax.ShapeDtypeStruct((total, 8), F32),
+            pltpu.VMEM((8, total), F32),
+            pltpu.VMEM((total, 8), F32),
             table,
             table,
         ),
-        in_specs=[VMEM],
+        in_specs=[VMEM] * (1 + len(weights)),
         out_specs=(VMEM,) * 4,
-        cost_estimate=cost(0.1e9, 1 << 16),
+        cost_estimate=cost(8e9, 1 << 16),
         compiler_params=PARAMS,
         name="prepare",
-    )(log)
+    )(log, *weights)
 
 
 def project_kernel(n_blocks, n_w, parts, first, ret_local, *refs):
-    gain_ref, crow_ref, ccol_ref, swap_ref, mix_ref, cos_ref, sin_ref = refs[:7]
-    blocks = refs[7 : 7 + n_blocks]
-    w_refs = refs[7 + n_blocks : 7 + n_blocks + n_w]
-    out_ref, sum_ref, low_ref, high_ref = refs[7 + n_blocks + n_w : 11 + n_blocks + n_w]
-    xn, inv = refs[-2:]
+    gain_ref, ccol_ref, swap_ref, mix_ref, cos_ref, sin_ref = refs[:6]
+    blocks = refs[6 : 6 + n_blocks]
+    w_refs = refs[6 + n_blocks : 6 + n_blocks + n_w]
+    out_ref, sum_ref, low_ref, high_ref = refs[6 + n_blocks + n_w : 10 + n_blocks + n_w]
+    xn, inv, held, sems = refs[-4:]
+    copies = Copies(sems)
     width = blocks[0].shape[1]
     rows = xn.shape[0]
     group_width = inv.shape[1]
     half = group_width // 2
-    total = crow_ref.shape[1]
+    total = ccol_ref.shape[0]
     mine = pl.ds(first, rows)
     starts = [pl.multiple_of(i * width, width) for i in sources()]
     tile = min(128, rows)
@@ -213,58 +247,61 @@
         if group == 3:
             for h in range(ret_local):
                 col = ccol_ref[mine, h : h + 1]
-                end = crow_ref[h : h + 1, total - 1 : total]
+                end = ccol_ref[total - 1 : total, h : h + 1]
                 v = raw[:, h * RV : (h + 1) * RV].astype(F32)
                 both = jnp.concatenate([v * jnp.exp(end - col), v * jnp.exp(col)], axis=1)
                 sum_ref[h] = t_dot(keys, both.astype(BF16))[h * RK : (h + 1) * RK]
         if group == 1:
             low_ref[...] = raw[rows - WINDOW :]
             high_ref[...] = raw[:WINDOW]
-        out_ref[group] = raw
-
-
-def project(gain, crow, ccol, swap, mix, cos, sin, blocks, weights, parts, first, rows, ret_local):
+        held[group] = raw
+        copies.start(held.at[group], out_ref.at[group])
+    copies.wait()
+
+
+def project(gain, ccol, swap, mix, cos, sin, blocks, weights, parts, first, rows, ret_local):
     width = mix.shape[0]
     depth = gain.shape[1]
     n = len(blocks)
     return pl.pallas_call(
         functools.partial(project_kernel, n, len(weights), parts, first, ret_local),
         out_shape=(
-            jax.ShapeDtypeStruct((5, rows, width), BF16),
-            jax.ShapeDtypeStruct((ret_local, RK, 2 * RV), F32),
+            pltpu.HBM((5, rows, width), BF16),
+            pltpu.VMEM((ret_local, RK, 2 * RV), F32),
             jax.ShapeDtypeStruct((WINDOW, width), BF16),
             jax.ShapeDtypeStruct((WINDOW, width), BF16),
         ),
-        in_specs=[VMEM] * (n + 7 + len(weights)),
-        out_specs=(VMEM,) * 4,
-        scratch_shapes=[pltpu.VMEM((rows, depth), BF16), pltpu.VMEM((rows, width), F32)],
+        in_specs=[VMEM] * (n + 6 + len(weights)),
+        out_specs=(HBM, VMEM, VMEM, VMEM),
+        scratch_shapes=[
+            pltpu.VMEM((rows, depth), BF16),
+            pltpu.VMEM((rows, width), F32),
+            pltpu.VMEM((5, rows, width), BF16),
+            pltpu.SemaphoreType.DMA((5,)),
+        ],
         cost_estimate=cost(2 * rows * depth * 5 * width // 4, 7 << 20),
         compiler_params=PARAMS,
         name="project",
-    )(gain, crow, ccol, swap, mix, cos, sin, *blocks, *weights)
+    )(gain, ccol, swap, mix, cos, sin, *blocks, *weights)
 
 
 def attend_kernel(n_chunks, kv_local, groups, seq_len, *refs):
     sink_ref = refs[0]
     proj = refs[1 : 1 + n_chunks]
     low_ref, high_ref, out_ref = refs[1 + n_chunks : 4 + n_chunks]
-    qbuf, kbuf, vbuf, mask = refs[-4:]
+    qbuf, kvbuf, vbuf, mask, sems = refs[-5:]
+    copies = Copies(sems)
     total = sum(ref.shape[1] for ref in proj)
     offset = lax.axis_index("sp") * total
     kv_cols = kv_local * HD
     block = WINDOW
     span = block + 2 * WINDOW
-    pieces = [(0, low_ref[...])]
-    at = 0
-    for ref in proj:
-        pieces.append((WINDOW + at, ref[1]))
-        qbuf[pl.ds(at, ref.shape[1])] = ref[0]
-        at += ref.shape[1]
-    pieces.append((WINDOW + total, high_ref[...]))
-    for first, kv in pieces:
-        here = pl.ds(first, kv.shape[0])
-        kbuf[here] = kv[:, :kv_cols]
-        vbuf[0:kv_cols, here] = kv[:, kv_cols:].T
+    copies.start(low_ref, kvbuf.at[pl.ds(0, WINDOW)])
+    copies.start(high_ref, kvbuf.at[pl.ds(WINDOW + total, WINDOW)])
+    for group, buf, at in ((1, kvbuf, WINDOW), (0, qbuf, 0)):
+        for ref in proj:
+            copies.start(ref.at[group], buf.at[pl.ds(at, ref.shape[1])])
+            at += ref.shape[1]
     vbuf[kv_cols:] = jnp.ones((vbuf.shape[0] - kv_cols, vbuf.shape[1]), BF16)
     row = lax.broadcasted_iota(jnp.int32, (span, block), 1)
     col = lax.broadcasted_iota(jnp.int32, (span, block), 0)
@@ -274,13 +311,17 @@
         allowed = band & (pos >= 0) & (pos < seq_len)
         one = jnp.where(allowed, 0.0, NEG)
         mask[i] = jnp.concatenate([one] * groups, axis=1)
+    copies.wait()
+    for i in range(kvbuf.shape[0] // block):
+        here = pl.ds(i * block, block)
+        vbuf[0:kv_cols, here] = kvbuf[here, kv_cols:].T
     lane = lax.broadcasted_iota(jnp.int32, (block, kv_cols), 1)
     n_steps = total // block
 
     def step(i, carry):
         first = pl.multiple_of(i * block, block)
         q = qbuf[pl.ds(first, block)]
-        k = kbuf[pl.ds(first, span)]
+        k = kvbuf[pl.ds(first, span), :kv_cols]
         kind = jnp.where(i == 0, 0, jnp.where(i == n_steps - 1, 2, 1))
         bias = mask[kind]
         scores = []
@@ -322,32 +363,33 @@
     return pl.pallas_call(
         functools.partial(attend_kernel, n, kv_local, groups, seq_len),
         out_shape=jax.ShapeDtypeStruct((total, width), BF16),
-        in_specs=[SMEM] + [VMEM] * (n + 2),
+        in_specs=[SMEM] + [HBM] * (n + 2),
         out_specs=VMEM,
         scratch_shapes=[
             pltpu.VMEM((total, width), BF16),
-            pltpu.VMEM((total + 2 * WINDOW, kv_cols), BF16),
+            pltpu.VMEM((total + 2 * WINDOW, 2 * kv_cols), BF16),
             pltpu.VMEM((kv_cols + 16, total + 2 * WINDOW), BF16),
             pltpu.VMEM((3, 3 * WINDOW, groups * WINDOW), F32),
+            pltpu.SemaphoreType.DMA((2 * n + 2,)),
         ],
         cost_estimate=cost(1.5e9, 3 << 20),
         compiler_params=PARAMS,
         name="attend",
-    )(sink, *proj, low, high)
+    )(sink, *in_hbm([*proj, low, high]))
 
 
 def totals_kernel(n_chunks, ret_local, n_sp, *refs):
-    crow_ref = refs[0]
+    ccol_ref = refs[0]
     sum_refs = refs[1 : 1 + n_chunks]
     out_ref = refs[-1]
     me = lax.axis_index("sp")
-    last = crow_ref.shape[1] - 1
+    last = ccol_ref.shape[0] - 1
     line = lax.broadcasted_iota(jnp.int32, (EXTRA, RV), 0)
     for h in range(ret_local):
         sums = sum_refs[0][h]
         for ref in sum_refs[1:]:
             sums = sums + ref[h]
-        end = jnp.broadcast_to(crow_ref[h : h + 1, last : last + 1], (EXTRA, RV))
+        end = jnp.broadcast_to(ccol_ref[last : last + 1, h : h + 1], (EXTRA, RV))
         d0 = end.astype(BF16).astype(F32)
         d1 = (end - d0).astype(BF16).astype(F32)
         d2 = end - d0 - d1
@@ -358,7 +400,7 @@
             out_ref[j, h] = jnp.where(j > me, fwd, bwd)
 
 
-def totals(crow, sums, n_sp):
+def totals(ccol, sums, n_sp):
     ret_local = sums[0].shape[0]
     return pl.pallas_call(
         functools.partial(totals_kernel, len(sums), ret_local, n_sp),
@@ -368,34 +410,34 @@
         cost_estimate=cost(0.1e9, 1 << 20),
         compiler_params=PARAMS,
         name="totals",
-    )(crow, *sums)
+    )(ccol, *sums)
 
 
 def local_kernel(n_chunks, ret_local, *refs):
     ccol_ref, crow_ref = refs[:2]
     proj = refs[2 : 2 + n_chunks]
     out_ref = refs[2 + n_chunks]
-    qbuf, kbuf, vbuf = refs[-3:]
+    rbuf, vbuf, sems = refs[-3:]
     total = crow_ref.shape[1]
     cols = ret_local * RK
-    at = 0
-    for ref in proj:
-        here = pl.ds(at, ref.shape[1])
-        qbuf[here] = ref[2, :, :cols]
-        kbuf[here] = ref[2, :, cols:]
-        vbuf[here] = ref[3]
-        at += ref.shape[1]
+    copies = Copies(sems)
+    for group, buf in ((2, rbuf), (3, vbuf)):
+        at = 0
+        for ref in proj:
+            copies.start(ref.at[group], buf.at[pl.ds(at, ref.shape[1])])
+            at += ref.shape[1]
+    copies.wait()
     block = min(256, total)
     lane = lax.broadcasted_iota(jnp.int32, (block, cols), 1)
 
     def step(i, carry):
         here = pl.ds(pl.multiple_of(i * block, block), block)
-        q = qbuf[here]
+        q = rbuf[here, :cols]
         for h in range(ret_local):
             mine = (lane >= h * RK) & (lane < (h + 1) * RK)
             qh = jnp.where(mine, q, jnp.zeros_like(q))
             gap = ccol_ref[here, h : h + 1] - crow_ref[h : h + 1, :]
-            w = (dot_t(qh, kbuf[...]) * jnp.exp(-jnp.abs(gap))).astype(BF16)
+            w = (dot_t(qh, rbuf[:, cols:]) * jnp.exp(-jnp.abs(gap))).astype(BF16)
             out_ref[here, h * RV : (h + 1) * RV] = dot(w, vbuf[:, h * RV : (h + 1) * RV])
         return carry
 
@@ -408,26 +450,35 @@
     total = crow.shape[1]
     return pl.pallas_call(
         functools.partial(local_kernel, n, ret_local),
-        out_shape=jax.ShapeDtypeStruct((total, width), F32),
-        in_specs=[VMEM] * (n + 2),
+        out_shape=pltpu.VMEM((total, width), F32),
+        in_specs=[VMEM, VMEM] + [HBM] * n,
         out_specs=VMEM,
         scratch_shapes=[
-            pltpu.VMEM((total, ret_local * RK), BF16),
-            pltpu.VMEM((total, ret_local * RK), BF16),
             pltpu.VMEM((total, width), BF16),
+            pltpu.VMEM((total, width), BF16),
+            pltpu.SemaphoreType.DMA((2 * n,)),
         ],
         cost_estimate=cost(1e9, 3 << 20),
         compiler_params=PARAMS,
         name="local",
-    )(ccol, crow, *proj)
+    )(*in_vmem([ccol, crow]), *in_hbm(proj))
 
 
 def cross_kernel(n_chunks, ret_local, n_sp, *refs):
-    crow_ref, ccol_ref, got_ref, init_ref, loc_ref = refs[:5]
-    proj = refs[5 : 5 + n_chunks]
-    out_ref, states = refs[-2:]
+    ccol_ref, loc_ref, got_hbm, init_hbm = refs[:4]
+    proj = refs[4 : 4 + n_chunks]
+    out_ref, states, got_ref, init_ref, qbuf, gbuf, sems = refs[-7:]
     me = lax.axis_index("sp")
-    last = crow_ref.shape[1] - 1
+    last = ccol_ref.shape[0] - 1
+    copies = Copies(sems)
+    copies.start(got_hbm, got_ref)
+    copies.start(init_hbm, init_ref)
+    for group, buf in ((2, qbuf), (4, gbuf)):
+        at = 0
+        for ref in proj:
+            copies.start(ref.at[group], buf.at[pl.ds(at, ref.shape[1])])
+            at += ref.shape[1]
+    copies.wait(0, 2)
     states[...] = jnp.zeros(states.shape, BF16)
     for h in range(ret_local):
         ends = []
@@ -445,100 +496,142 @@
             state = state + jnp.exp(run) * init_ref[side, h]
             col = (2 * h + side) * RV
             states[h * RK : (h + 1) * RK, col : col + RV] = state.astype(BF16)
+    copies.wait(2)
     block = min(256, last + 1)
-    first = 0
-    for ref in proj:
-
-        def step(i, carry, ref=ref, first=first):
-            inner = pl.ds(pl.multiple_of(i * block, block), block)
-            here = pl.ds(pl.multiple_of(first + i * block, block), block)
-            both = dot(ref[2, inner, : ret_local * RK], states[...])
-            for h in range(ret_local):
-                col = ccol_ref[here, h : h + 1]
-                ret = (
-                    loc_ref[here, h * RV : (h + 1) * RV]
-                    + jnp.exp(col) * both[:, 2 * h * RV : (2 * h + 1) * RV]
-                    + jnp.exp(crow_ref[h : h + 1, last : last + 1] - col) * both[:, (2 * h + 1) * RV : (2 * h + 2) * RV]
-                )
-                centered = ret - jnp.mean(ret, axis=1, keepdims=True)
-                scale = lax.rsqrt(jnp.mean(centered * centered, axis=1, keepdims=True) + NORM_EPS)
-                gate = ref[4, inner, h * RV : (h + 1) * RV].astype(F32)
-                gated = gate / (1.0 + jnp.exp(-gate))
-                out_ref[here, h * RV : (h + 1) * RV] = (gated * (centered * scale)).astype(BF16)
-            return carry
-
-        lax.fori_loop(0, ref.shape[1] // block, step, 0)
-        first += ref.shape[1]
-
-
-def cross(crow, ccol, got, init, loc, proj, ret_local, n_sp):
+    for i in range((last + 1) // block):
+        here = pl.ds(i * block, block)
+        both = dot(qbuf[here, : ret_local * RK], states[...])
+        for h in range(ret_local):
+            col = ccol_ref[here, h : h + 1]
+            end = ccol_ref[last : last + 1, h : h + 1]
+            ret = (
+                loc_ref[here, h * RV : (h + 1) * RV]
+                + jnp.exp(col) * both[:, 2 * h * RV : (2 * h + 1) * RV]
+                + jnp.exp(end - col) * both[:, (2 * h + 1) * RV : (2 * h + 2) * RV]
+            )
+            centered = ret - jnp.mean(ret, axis=1, keepdims=True)
+            scale = lax.rsqrt(jnp.mean(centered * centered, axis=1, keepdims=True) + NORM_EPS)
+            gate = gbuf[here, h * RV : (h + 1) * RV].astype(F32)
+            gated = gate / (1.0 + jnp.exp(-gate))
+            out_ref[here, h * RV : (h + 1) * RV] = (gated * (centered * scale)).astype(BF16)
+
+
+def cross(ccol, got, init, loc, proj, ret_local, n_sp):
     n = len(proj)
     width = proj[0].shape[2]
-    total = crow.shape[1]
+    total = ccol.shape[0]
     return pl.pallas_call(
         functools.partial(cross_kernel, n, ret_local, n_sp),
         out_shape=jax.ShapeDtypeStruct((total, width), BF16),
-        in_specs=[VMEM] * (n + 5),
+        in_specs=[VMEM, VMEM] + [HBM] * (n + 2),
         out_specs=VMEM,
-        scratch_shapes=[pltpu.VMEM((ret_local * RK, 2 * ret_local * RV), BF16)],
+        scratch_shapes=[
+            pltpu.VMEM((ret_local * RK, 2 * ret_local * RV), BF16),
+            pltpu.VMEM(got.shape, BF16),
+            pltpu.VMEM(init.shape, F32),
+            pltpu.VMEM((total, width), BF16),
+            pltpu.VMEM((total, width), BF16),
+            pltpu.SemaphoreType.DMA((2 * n + 2,)),
+        ],
         cost_estimate=cost(0.5e9, 4 << 20),
         compiler_params=PARAMS,
         name="cross",
-    )(crow, ccol, got, init, loc, *proj)
-
-
-def rows_of(ref, part, far, cols, core):
-    share = ref.shape[2] // 2
-    at = pl.ds(pl.multiple_of(core * cols, cols), cols)
-    pieces = [ref[s, far, part * share : (part + 1) * share, at] for s in range(ref.shape[0])]
-    return jnp.concatenate(pieces, axis=0)
-
-
-def far_rows(spread, peer_spread, part, cols):
-    core = lax.rem(lax.axis_index("tp"), 2)
-    out = []
+    )(*in_vmem([ccol, loc]), *in_hbm([got, init]), *in_vmem(proj))
+
+
+def most_kernel(n_data, *refs):
+    near_att, near_ret, peer_att, peer_ret, spread, peer_spread = refs[:6]
+    data = refs[6 : 6 + n_data]
+    out_ref, rest_ref = refs[6 + n_data : 8 + n_data]
+    left, right, sems = refs[-3:]
+    copies = Copies(sems)
+    cols = out_ref.shape[1]
+    tp = lax.axis_index("tp")
+    mine = pl.ds(pl.multiple_of(tp * cols, cols), cols)
+    half = pl.ds(pl.multiple_of(lax.rem(tp, 2) * cols, cols), cols)
+    depth = near_att.shape[0]
+    share = spread.shape[2] // 2
+    at = 0
+    for ref in (near_att, peer_att):
+        copies.start(ref.at[:, mine], right.at[pl.ds(at, depth)])
+        at += depth
+    below = 0
     for far in range(spread.shape[1]):
-        out.append(rows_of(spread, part, far, cols, core))
-        out.append(rows_of(peer_spread, part, far, cols, core))
-    return out
-
-
-def most_kernel(*refs):
-    near_att, near_ret, peer_att, peer_ret, spread, peer_spread = refs[:6]
-    data = refs[6:-1]
-    out_ref = refs[-1]
-    cols = out_ref.shape[1]
-    mine = pl.ds(pl.multiple_of(lax.axis_index("tp") * cols, cols), cols)
-    pieces = [near_att[:, mine], peer_att[:, mine]] + far_rows(spread, peer_spread, 0, cols)
-    pieces += [near_ret[:, mine], peer_ret[:, mine]]
-    right = jnp.concatenate(pieces, axis=0)
+        for ref in (spread, peer_spread):
+            for s in range(spread.shape[0]):
+                from_att = ref.at[s, far, pl.ds(0, share), half]
+                from_ret = ref.at[s, far, pl.ds(share, share), half]
+                copies.start(from_att, right.at[pl.ds(at + s * share, share)])
+                copies.start(from_ret, rest_ref.at[pl.ds(below + s * share, share)])
+            at += depth
+            below += depth
+    for ref in (near_ret, peer_ret):
+        copies.start(ref.at[:, mine], right.at[pl.ds(at, depth)])
+        at += depth
+    for i, ref in enumerate(data):
+        copies.start(ref, left.at[:, pl.ds(i * depth, depth)])
+    copies.wait()
     rows = min(256, out_ref.shape[0])
     for i in range(out_ref.shape[0] // rows):
         here = pl.ds(i * rows, rows)
-        out_ref[here] = dot(jnp.concatenate([ref[here] for ref in data], axis=1), right)
-
-
-def last_kernel(*refs):
-    spread, peer_spread, base = refs[:3]
-    data = refs[3:-1]
-    out_ref = refs[-1]
-    right = jnp.concatenate(far_rows(spread, peer_spread, 1, out_ref.shape[1]), axis=0)
-    rows = min(256, out_ref.shape[0])
-    for i in range(out_ref.shape[0] // rows):
+        out_ref[here] = dot(left[here], right[...])
+
+
+def most(weights, data, cols):
+    total, depth = data[0].shape
+    n = len(data)
+    spread = weights[4]
+    count = 4 + 4 * spread.shape[0] * spread.shape[1] + n
+    rest = 2 * spread.shape[1] * depth
+    return pl.pallas_call(
+        functools.partial(most_kernel, n),
+        out_shape=(
+            pltpu.VMEM((total, cols), F32),
+            pltpu.VMEM((rest, cols), BF16),
+        ),
+        in_specs=[HBM] * (6 + n),
+        out_specs=(VMEM, VMEM),
+        scratch_shapes=[
+            pltpu.VMEM((total, n * depth), BF16),
+            pltpu.VMEM((n * depth, cols), BF16),
+            pltpu.SemaphoreType.DMA((count,)),
+        ],
+        cost_estimate=cost(1e9, 8 << 20),
+        compiler_params=PARAMS,
+        name="most",
+    )(*in_hbm(weights), *in_hbm(data))
+
+
+def last_kernel(n_data, *refs):
+    base, right = refs[:2]
+    data = refs[2 : 2 + n_data]
+    out_ref, held, sems = refs[-3:]
+    copies = Copies(sems)
+    rows = held.shape[1]
+    for i in range(held.shape[0]):
         here = pl.ds(i * rows, rows)
-        part = dot(jnp.concatenate([ref[here] for ref in data], axis=1), right)
-        out_ref[here] = (part + base[here]).astype(BF16)
-
-
-def output(kernel, operands, shape, dtype):
-    return pl.pallas_call(
-        kernel,
-        out_shape=jax.ShapeDtypeStruct(shape, dtype),
-        in_specs=[VMEM] * len(operands),
-        out_specs=VMEM,
+        part = dot(jnp.concatenate([ref[here] for ref in data], axis=1), right[...])
+        held[i] = (part + base[here]).astype(BF16)
+        copies.start(held.at[i], out_ref.at[here])
+    copies.wait()
+
+
+def last(base, right, data):
+    total, cols = base.shape
+    rows = min(256, total)
+    return pl.pallas_call(
+        functools.partial(last_kernel, len(data)),
+        out_shape=jax.ShapeDtypeStruct((total, cols), BF16),
+        in_specs=[VMEM] * (2 + len(data)),
+        out_specs=HBM,
+        scratch_shapes=[
+            pltpu.VMEM((total // rows, rows, cols), BF16),
+            pltpu.SemaphoreType.DMA((total // rows,)),
+        ],
         cost_estimate=cost(1e9, 8 << 20),
         compiler_params=PARAMS,
-    )(*operands)
+        name="last",
+    )(*in_vmem([base, right]), *data)
 
 
 def core_swap(value):
@@ -612,7 +705,8 @@
     ret_local = decay_log.shape[0]
     cols = tokens.shape[1]
 
-    pieces, slabs = split(tokens, out_att, out_ret)
+    slabs = slab(out_att, out_ret, cols)
+    pieces = split(tokens)
     near = core_swap(tokens)
     far = {}
     for c in ORDER:
@@ -631,7 +725,6 @@
             for i in range(HD):
                 mix[(g * groups + j) * HD + i, (j * kv_local + g) * HD + i] = 1.0
     mix = jnp.asarray(mix, BF16)
-    crow, ccol, cos, sin = prepare(decay_log)
 
     if half % 128 == 0:
         weights = [att_query, att_key, att_value, ret_query, ret_key, ret_value, ret_gate]
@@ -646,6 +739,8 @@
         ]
         parts = [(i, 0) for i in range(5)]
     gain = norm_gain[None, :]
+    weights = in_vmem(weights)
+    crow, ccol, cos, sin = prepare(decay_log, [])
     out_w = output_weights(out_att, out_ret, slabs)
     proj = [None] * len(CHUNKS)
     sums = [None] * len(CHUNKS)
@@ -653,7 +748,7 @@
     for c in ORDER:
         first, rows = CHUNKS[c][0] * total // 4, CHUNKS[c][1] * total // 4
         proj[c], sums[c], *edges[c] = project(
-            gain, crow, ccol, swap, mix, cos, sin, [tokens, near] + far[c], weights, parts,
+            gain, ccol, swap, mix, cos, sin, [tokens, near] + far[c], weights, parts,
             first, rows, ret_local,
         )
 
@@ -662,17 +757,15 @@
     low = lax.ppermute(edges[-1][0], "sp", forward)
     high = lax.ppermute(edges[0][1], "sp", backward)
 
-    sent = totals(crow, sums, n_sp)
+    sent = totals(ccol, sums, n_sp)
     got = lax.all_to_all(sent, "sp", 0, 0, tiled=True)
     attended = attend(att_sink, proj, low, high, kv_local, groups, seq_len)
     att_blocks = gather_tp(attended)
     loc = local(ccol, crow, proj, ret_local)
-    kept = cross(crow, ccol, got, init_state, loc, proj, ret_local, n_sp)
+    kept = cross(ccol, got, init_state, loc, proj, ret_local, n_sp)
     ret_blocks = gather_tp(kept)
-    operands = out_w + att_blocks + ret_blocks[:2]
-    most = output(most_kernel, operands, (total, cols), F32)
-    operands = out_w[4:] + [most] + ret_blocks[2:]
-    return output(last_kernel, operands, (total, cols), BF16)
+    base, right = most(out_w, att_blocks + ret_blocks[:2], cols)
+    return last(base, right, ret_blocks[2:])
 
 
 def solution(mesh):

time: 130 us -> 115 us (0.88)
  local copies, waits for them, and re-layouts: 20.7 us -> 2.94 us
  waiting for transfers between devices: 41.3 us -> 33.3 us
  starting transfers between devices: 31.2 us -> 37.2 us
  Pallas kernels: 35.4 us -> 40.2 us
    unnamed x70 -> x48, local copies, waits for them, and re-layouts: 20.7 us -> 2.94 us
    ppermute x6, waiting for transfers between devices: 34.8 us -> 27.3 us  [chip_turn(): return lax.ppermute(value, 'tp', [(i, (i + 2 * by) % n) for i in range(n)])]
    ppermute x11, starting transfers between devices: 9.46 us -> 15.3 us  [core_swap(): return lax.ppermute(value, 'tp', [(i, i ^ 1) for i in range(n)])]
    pallas_call x3, Pallas kernels: 12.5 us -> 15.2 us  [project(): pl.pallas_call(functools.partial(project_kernel, n, len(weights), parts,...]
    pallas_call x1, Pallas kernels: 5.6 us -> 3.47 us  [cross(): pl.pallas_call(functools.partial(cross_kernel, n, ret_local, n_sp), out_s...]
    pallas_call x5 -> x6, Pallas kernels: 11.6 us -> 13.6 us  [the longest x1 4.67 us: most(): pl.pallas_call(functools.partial(most_kernel, n), out_shape=(pltpu.VMEM((...]
    pallas_call x1, Pallas kernels: 4.74 us -> 6.07 us  [attend(): pl.pallas_call(functools.partial(attend_kernel, n, kv_local, groups, seq_...]
  transfers between devices with their start and end apart: 21 -> 21, of which waited for: 6 -> 5; matrix products, arithmetic and copies ran while one was open for 0% -> 0% of each run, Pallas kernels for 25% -> 32%
where the time goes in v3:
time: 115 us; the launch traced here: 114 us
  Pallas kernels  40.2 us (35%)
  starting transfers between devices  37.2 us (32%)
  waiting for transfers between devices  33.3 us (29%)
  local copies, waits for them, and re-layouts  2.94 us (3%)
    ppermute x6, waiting for transfers between devices, chip_turn(): return lax.ppermute(value, 'tp', [(i, (i + 2 * by) % n) for i in range(n)])  27.3 us
    ppermute x11, starting transfers between devices, core_swap(): return lax.ppermute(value, 'tp', [(i, i ^ 1) for i in range(n)])  15.3 us
    pallas_call x3, Pallas kernels, project(): pl.pallas_call(functools.partial(project_kernel, n, len(weights), parts,...  15.2 us
    ppermute x6, starting transfers between devices, chip_turn(): return lax.ppermute(value, 'tp', [(i, (i + 2 * by) % n) for i in range(n)])  6.56 us
    pallas_call x1, Pallas kernels, attend(): pl.pallas_call(functools.partial(attend_kernel, n, kv_local, groups, seq_...  6.07 us
    ppermute x1, waiting for transfers between devices, body(): low = lax.ppermute(edges[-1][0], 'sp', forward)  5.95 us
    all_to_all x1, starting transfers between devices, output_weights(): spread = lax.all_to_all(spread, 'sp', 0, 0, tiled=True)  5.47 us
    all_to_all x1, starting transfers between devices, body(): got = lax.all_to_all(sent, 'sp', 0, 0, tiled=True)  5.44 us
  transfers between devices with their start and end apart: 21, of which 5 were waited for; matrix products, arithmetic and copies ran while one was open for 0% of the time, Pallas kernels for 32%

profile of v3, /device:TPU:1, one launch (start us, length us, event | category | flops | bytes accessed | tf_op | source)
XLA Modules:
  0.0 114.2 jit_solution(13478883213522059771)
XLA Ops:
  0.0 0.9 slab.1
  0.9 2.1 %collective-permute-start.2 = (bf16[64,1024]{1,0:T(8,128)(2,1)S(1)}, bf16[64,1024]{1,0:T(8,128)(2,1)S(1)}, u32[]{:S(2)}, u32[]{:S(2)}) collective-permute-start(bf16[64,1024]{1,0:T(8,128)(2,1)S(1)} %slab.1), channel_id=1, source_target_pairs={{0,2},{1,3},{2,0},{3,1},{4,6},{5,7},{6,4},{7,5},{8,10},{9,11},{10,... | collective-permute-start | bytes 393224 | tf_op jit(solution)/shard_map/ppermute | solution.py:644
  3.1 3.2 %collective-permute-done.2.refs_0_ = bf16[64,1024]{1,0:T(8,128)(2,1)S(1)} collective-permute-done((bf16[64,1024]{1,0:T(8,128)(2,1)S(1)}, bf16[64,1024]{1,0:T(8,128)(2,1)S(1)}, u32[]{:S(2)}, u32[]{:S(2)}) %collective-permute-start.2) | collective-permute-done | bytes 131104 | tf_op jit(solution)/shard_map/ppermute | solution.py:644
  6.3 1.0 repeat.1
  7.3 5.5 %all-to-all-start = ((bf16[8,1,64,1024]{3,2,1,0:T(8,128)(2,1)}), bf16[8,1,64,1024]{3,2,1,0:T(8,128)(2,1)}, u32[]{:S(2)}, u32[]{:S(2)}) async-start(bf16[8,1,64,1024]{3,2,1,0:T(8,128)(2,1)} %repeat.1), calls=%async_computation | async-start | bytes 2097152 | tf_op jit(solution)/shard_map/all_to_all | solution.py:671
  12.8 1.2 %split.1 = (bf16[256,512]{1,0:T(8,128)(2,1)S(1)}, bf16[256,512]{1,0:T(8,128)(2,1)S(1)}, bf16[512,512]{1,0:T(8,128)(2,1)S(1)}) custom-call(bf16[1024,512]{1,0:T(8,128)(2,1)} %refs_6_.5), custom_call_target="tpu_custom_call" | custom-call | flops 100000000 | bytes 3145728 | tf_op jit(solution)/shard_map/split/pallas_call | solution.py:123
  14.0 1.3 %collective-permute-start.9 = (bf16[512,512]{1,0:T(8,128)(2,1)S(1)}, bf16[512,512]{1,0:T(8,128)(2,1)S(1)}, u32[]{:S(2)}, u32[]{:S(2)}) collective-permute-start(bf16[512,512]{1,0:T(8,128)(2,1)S(1)} %get-tuple-element.29), channel_id=1, source_target_pairs={{0,2},{1,3},{2,0},{3,1},{4,6},{5,7},{6,4},{7,5},{8,10},{9,11},{10,... | collective-permute-start | bytes 1572872 | tf_op jit(solution)/shard_map/ppermute | solution.py:644
  15.3 2.1 %collective-permute-start.4 = (bf16[1024,512]{1,0:T(8,128)(2,1)S(1)}, bf16[1024,512]{1,0:T(8,128)(2,1)S(1)}, u32[]{:S(2)}, u32[]{:S(2)}) collective-permute-start(bf16[1024,512]{1,0:T(8,128)(2,1)S(1)} %copy-done), channel_id=1, source_target_pairs={{0,1},{1,0},{2,3},{3,2},{4,5},{5,4},{6,7},{7,6},{8,9},{9,8},{10,11... | collective-permute-start | bytes 3145736 | tf_op jit(solution)/shard_map/ppermute | solution.py:639
  17.7 1.3 %collective-permute-start.7 = (bf16[256,512]{1,0:T(8,128)(2,1)S(1)}, bf16[256,512]{1,0:T(8,128)(2,1)S(1)}, u32[]{:S(2)}, u32[]{:S(2)}) collective-permute-start(bf16[256,512]{1,0:T(8,128)(2,1)S(1)} %get-tuple-element.27), channel_id=1, source_target_pairs={{0,2},{1,3},{2,0},{3,1},{4,6},{5,7},{6,4},{7,5},{8,10},{9,11},{10,... | collective-permute-start | bytes 786440 | tf_op jit(solution)/shard_map/ppermute | solution.py:644
  19.0 12.3 %collective-permute-done.5.refs_8_ = bf16[256,512]{1,0:T(8,128)(2,1)S(1)} collective-permute-done((bf16[256,512]{1,0:T(8,128)(2,1)S(1)}, bf16[256,512]{1,0:T(8,128)(2,1)S(1)}, u32[]{:S(2)}, u32[]{:S(2)}) %collective-permute-start.5) | collective-permute-done | bytes 262176 | tf_op jit(solution)/shard_map/ppermute | solution.py:644
  31.4 4.9 %collective-permute-start.6 = (bf16[256,512]{1,0:T(8,128)(2,1)S(1)}, bf16[256,512]{1,0:T(8,128)(2,1)S(1)}, u32[]{:S(2)}, u32[]{:S(2)}) collective-permute-start(bf16[256,512]{1,0:T(8,128)(2,1)S(1)} %collective-permute-done.5.refs_8_), channel_id=1, source_target_pairs={{0,1},{1,0},{2,3},{3,2},{4,5},{5,4},{6,7},{7,6},{8,9},{9,8},{10,11... | collective-permute-start | bytes 786440 | tf_op jit(solution)/shard_map/ppermute | solution.py:639
  37.0 2.7 %collective-permute-start.8 = (bf16[256,512]{1,0:T(8,128)(2,1)S(1)}, bf16[256,512]{1,0:T(8,128)(2,1)S(1)}, u32[]{:S(2)}, u32[]{:S(2)}) collective-permute-start(bf16[256,512]{1,0:T(8,128)(2,1)S(1)} %collective-permute-done.7.refs_8_), channel_id=1, source_target_pairs={{0,1},{1,0},{2,3},{3,2},{4,5},{5,4},{6,7},{7,6},{8,9},{9,8},{10,11... | collective-permute-start | bytes 786440 | tf_op jit(solution)/shard_map/ppermute | solution.py:639
  39.7 0.8 prepare.1
  40.6 4.2 %project.3 = (bf16[5,256,256]{2,1,0:T(8,128)(2,1)}, f32[2,64,256]{2,1,0:T(8,128)S(1)}, bf16[128,256]{1,0:T(8,128)(2,1)}, bf16[128,256]{1,0:T(8,128)(2,1)S(1)}) custom-call(f32[1,2048]{1,0:T(1,128)S(1)} %bitcast.1, f32[1024,8]{1,0:T(8,128)S(1)} %get-tuple-element.22.refs_1_.refs_0_, bf16[128,128]{1,0:T(8,128)(2,1)S(1)} %copy-done.13, ...), custom_call_target="tpu_custom_call" | custom-call | flops 335544320 | bytes 7340032 | tf_op jit(solution)/shard_map/project/pallas_call | solution.py:266
  44.8 4.2 %project.4 = (bf16[5,256,256]{2,1,0:T(8,128)(2,1)}, f32[2,64,256]{2,1,0:T(8,128)S(1)}, bf16[128,256]{1,0:T(8,128)(2,1)}, bf16[128,256]{1,0:T(8,128)(2,1)}) custom-call(f32[1,2048]{1,0:T(1,128)S(1)} %bitcast.2, f32[1024,8]{1,0:T(8,128)S(1)} %get-tuple-element.22.refs_1_.refs_0_, bf16[128,128]{1,0:T(8,128)(2,1)S(1)} %copy-done.13, ...), custom_call_target="tpu_custom_call" | custom-call | flops 335544320 | bytes 7340032 | tf_op jit(solution)/shard_map/project/pallas_call | solution.py:266
  49.1 6.7 %project.5 = (bf16[5,512,256]{2,1,0:T(8,128)(2,1)}, f32[2,64,256]{2,1,0:T(8,128)S(1)}, bf16[128,256]{1,0:T(8,128)(2,1)S(1)}, bf16[128,256]{1,0:T(8,128)(2,1)}) custom-call(f32[1,2048]{1,0:T(1,128)S(1)} %bitcast.3, f32[1024,8]{1,0:T(8,128)S(1)} %get-tuple-element.22.refs_1_.refs_0_, bf16[128,128]{1,0:T(8,128)(2,1)S(1)} %copy-done.13, ...), custom_call_target="tpu_custom_call" | custom-call | flops 671088640 | bytes 7340032 | tf_op jit(solution)/shard_map/project/pallas_call | solution.py:266
  55.8 0.9 totals.1
  56.7 5.4 %all-to-all-start.1 = ((bf16[8,2,80,128]{3,2,1,0:T(8,128)(2,1)}), bf16[8,2,80,128]{3,2,1,0:T(8,128)(2,1)}, u32[]{:S(2)}, u32[]{:S(2)}) async-start(bf16[8,2,80,128]{3,2,1,0:T(8,128)(2,1)} %totals.1), calls=%async_computation.1 | async-start | bytes 655360 | tf_op jit(solution)/shard_map/all_to_all | solution.py:761
  63.0 1.7 %collective-permute-start.11 = (bf16[128,256]{1,0:T(8,128)(2,1)S(1)}, bf16[128,256]{1,0:T(8,128)(2,1)S(1)}, u32[]{:S(2)}, u32[]{:S(2)}) collective-permute-start(bf16[128,256]{1,0:T(8,128)(2,1)S(1)} %get-tuple-element.31), channel_id=1, source_target_pairs={{0,4},{4,8},{8,12},{12,16},{16,20},{20,24},{24,28},{28,0},{1,5},{5... | collective-permute-start | bytes 196616 | tf_op jit(solution)/shard_map/ppermute | solution.py:757
  64.7 2.7 %collective-permute-start.12 = (bf16[128,256]{1,0:T(8,128)(2,1)S(1)}, bf16[128,256]{1,0:T(8,128)(2,1)S(1)}, u32[]{:S(2)}, u32[]{:S(2)}) collective-permute-start(bf16[128,256]{1,0:T(8,128)(2,1)S(1)} %get-tuple-element.32), channel_id=1, source_target_pairs={{4,0},{8,4},{12,8},{16,12},{20,16},{24,20},{28,24},{0,28},{5,1},{9... | collective-permute-start | bytes 196616 | tf_op jit(solution)/shard_map/ppermute | solution.py:758
  67.4 6.0 %collective-permute-done.11.refs_4_ = bf16[128,256]{1,0:T(8,128)(2,1)S(1)} collective-permute-done((bf16[128,256]{1,0:T(8,128)(2,1)S(1)}, bf16[128,256]{1,0:T(8,128)(2,1)S(1)}, u32[]{:S(2)}, u32[]{:S(2)}) %collective-permute-start.11) | collective-permute-done | bytes 65568 | tf_op jit(solution)/shard_map/ppermute | solution.py:757
  74.0 6.1 %attend.1.refs_6_ = bf16[1024,256]{1,0:T(8,128)(2,1)} custom-call(f32[4]{0:T(128)S(1)} %copy-done.18, bf16[5,256,256]{2,1,0:T(8,128)(2,1)} %get-tuple-element.26.refs_1_.refs_2_.refs_4_, bf16[5,256,256]{2,1,0:T(8,128)(2,1)} %get-tuple-element.28.refs_2_.refs_3_.refs_5_, bf16[5,512,256]{2,1,0:T(8,128)(2,1)} %get-tuple-element.30.refs_3_.refs_4_.refs_6_, ...), custom_call_target="tpu_custom_call" | custom-call | flops 1500000000 | bytes 3145728 | tf_op jit(solution)/shard_map/attend/pallas_call | solution.py:363
  80.1 1.3 %collective-permute-start.14 = (bf16[1024,256]{1,0:T(8,128)(2,1)}, bf16[1024,256]{1,0:T(8,128)(2,1)}, u32[]{:S(2)}, u32[]{:S(2)}) collective-permute-start(bf16[1024,256]{1,0:T(8,128)(2,1)} %attend.1.refs_6_), channel_id=1, source_target_pairs={{0,2},{1,3},{2,0},{3,1},{4,6},{5,7},{6,4},{7,5},{8,10},{9,11},{10,... | collective-permute-start | bytes 1572872 | tf_op jit(solution)/shard_map/ppermute | solution.py:644
  81.4 1.8 %collective-permute-start.3 = (bf16[8,1,64,1024]{3,2,1,0:T(8,128)(2,1)}, bf16[8,1,64,1024]{3,2,1,0:T(8,128)(2,1)}, u32[]{:S(2)}, u32[]{:S(2)}) collective-permute-start(bf16[8,1,64,1024]{3,2,1,0:T(8,128)(2,1)} %all-to-all-done.refs_4_), channel_id=1, source_target_pairs={{0,1},{1,0},{2,3},{3,2},{4,5},{5,4},{6,7},{7,6},{8,9},{9,8},{10,11... | collective-permute-start | bytes 3145736 | tf_op jit(solution)/shard_map/ppermute | solution.py:639
  83.2 4.5 %local.1.refs_1_ = f32[1024,256]{1,0:T(8,128)S(1)} custom-call(f32[1024,8]{1,0:T(8,128)S(1)} %get-tuple-element.22.refs_1_.refs_0_, f32[8,1024]{1,0:T(8,128)S(1)} %copy-done.16, bf16[5,256,256]{2,1,0:T(8,128)(2,1)} %get-tuple-element.26.refs_1_.refs_2_.refs_4_, bf16[5,256,256]{2,1,0:T(8,128)(2,1)} %get-tuple-element.28.refs_2_.refs_3_.refs_5_, ...), custom_call_target="tpu_custom_call" | custom-call | flops 1000000000 | bytes 3145728 | tf_op jit(solution)/shard_map/local/pallas_call | solution.py:451
  87.8 1.1 copy-done.10
  88.8 3.5 %cross.1.refs_10_ = bf16[1024,256]{1,0:T(8,128)(2,1)S(1)} custom-call(f32[1024,8]{1,0:T(8,128)S(1)} %get-tuple-element.22.refs_1_.refs_0_, f32[1024,256]{1,0:T(8,128)S(1)} %local.1.refs_1_, bf16[8,2,80,128]{3,2,1,0:T(8,128)(2,1)} %all-to-all-done.1.refs_2_, f32[2,2,64,128]{3,2,1,0:T(8,128)} %refs_3_.4, bf16[5,256,256]{2,1,0:T(8,128)(2,1)S(1)} %copy-done.9, ...), custom_call_target="tpu_custom_call" | custom-call | flops 500000000 | bytes 4194304 | tf_op jit(solution)/shard_map/cross/pallas_call | solution.py:523
  93.2 1.6 %collective-permute-start.15 = (bf16[1024,256]{1,0:T(8,128)(2,1)}, bf16[1024,256]{1,0:T(8,128)(2,1)S(1)}, u32[]{:S(2)}, u32[]{:S(2)}) collective-permute-start(bf16[1024,256]{1,0:T(8,128)(2,1)} %collective-permute-done.14.refs_8_), channel_id=1, source_target_pairs={{0,1},{1,0},{2,3},{3,2},{4,5},{5,4},{6,7},{7,6},{8,9},{9,8},{10,11... | collective-permute-start | bytes 1572872 | tf_op jit(solution)/shard_map/ppermute | solution.py:639
  94.8 11.1 %collective-permute-done.17.refs_2_ = bf16[1024,256]{1,0:T(8,128)(2,1)S(1)} collective-permute-done((bf16[1024,256]{1,0:T(8,128)(2,1)S(1)}, bf16[1024,256]{1,0:T(8,128)(2,1)S(1)}, u32[]{:S(2)}, u32[]{:S(2)}) %collective-permute-start.17) | collective-permute-done | bytes 524320 | tf_op jit(solution)/shard_map/ppermute | solution.py:644
  105.9 0.9 collective-permute-start.18
  107.9 4.7 %most.1 = (f32[1024,512]{1,0:T(8,128)S(1)}, bf16[512,512]{1,0:T(8,128)(2,1)S(1)}) custom-call(bf16[256,2048]{1,0:T(8,128)(2,1)} %refs_0_.7, bf16[256,2048]{1,0:T(8,128)(2,1)} %refs_1_.3, bf16[256,2048]{1,0:T(8,128)(2,1)} %collective-permute-done.refs_2_, bf16[256,2048]{1,0:T(8,128)(2,1)} %collective-permute-done.1.refs_3_, ...), custom_call_target="tpu_custom_call" | custom-call | flops 1000000000 | bytes 8388608 | tf_op jit(solution)/shard_map/most/pallas_call | solution.py:586
  112.6 1.5 %last.1 = bf16[1024,512]{1,0:T(8,128)(2,1)} custom-call(f32[1024,512]{1,0:T(8,128)S(1)} %get-tuple-element.37.refs_0_, bf16[512,512]{1,0:T(8,128)(2,1)S(1)} %get-tuple-element.38.refs_1_, bf16[1024,256]{1,0:T(8,128)(2,1)S(1)} %collective-permute-done.17.refs_2_, bf16[1024,256]{1,0:T(8,128)(2,1)S(1)} %collective-permute-done.18.refs_3_), custom_call_target="tpu_custom_call" | custom-call | flops 1000000000 | bytes 8388608 | tf_op jit(solution)/shard_map/last/pallas_call | solution.py:622
  (71 shorter events, 4.5 us)
Async XLA Ops:
  0.9 38.7 %copy-start.17 = (f32[2,1024]{1,0:T(2,128)S(1)}, f32[2,1024]{1,0:T(2,128)}, u32[]{:S(2)}) copy-start(f32[2,1024]{1,0:T(2,128)} %log_ref.1) | copy-start | bytes 24580
  0.9 5.3 %collective-permute-start.2 = (bf16[64,1024]{1,0:T(8,128)(2,1)S(1)}, bf16[64,1024]{1,0:T(8,128)(2,1)S(1)}, u32[]{:S(2)}, u32[]{:S(2)}) collective-permute-start(bf16[64,1024]{1,0:T(8,128)(2,1)S(1)} %slab.1), channel_id=1, source_target_pairs={{0,2},{1,3},{2,0},{3,1},{4,6},{5,7},{6,4},{7,5},{8,10},{9,11},{10,... | collective-permute-start | bytes 393224 | tf_op jit(solution)/shard_map/ppermute | solution.py:644
  7.3 49.4 %all-to-all-start = ((bf16[8,1,64,1024]{3,2,1,0:T(8,128)(2,1)}), bf16[8,1,64,1024]{3,2,1,0:T(8,128)(2,1)}, u32[]{:S(2)}, u32[]{:S(2)}) async-start(bf16[8,1,64,1024]{3,2,1,0:T(8,128)(2,1)} %repeat.1), calls=%async_computation | async-start | bytes 2097152 | tf_op jit(solution)/shard_map/all_to_all | solution.py:671
  14.0 25.6 %collective-permute-start.9 = (bf16[512,512]{1,0:T(8,128)(2,1)S(1)}, bf16[512,512]{1,0:T(8,128)(2,1)S(1)}, u32[]{:S(2)}, u32[]{:S(2)}) collective-permute-start(bf16[512,512]{1,0:T(8,128)(2,1)S(1)} %get-tuple-element.29), channel_id=1, source_target_pairs={{0,2},{1,3},{2,0},{3,1},{4,6},{5,7},{6,4},{7,5},{8,10},{9,11},{10,... | collective-permute-start | bytes 1572872 | tf_op jit(solution)/shard_map/ppermute | solution.py:644
  15.3 25.1 %collective-permute-start.4 = (bf16[1024,512]{1,0:T(8,128)(2,1)S(1)}, bf16[1024,512]{1,0:T(8,128)(2,1)S(1)}, u32[]{:S(2)}, u32[]{:S(2)}) collective-permute-start(bf16[1024,512]{1,0:T(8,128)(2,1)S(1)} %copy-done), channel_id=1, source_target_pairs={{0,1},{1,0},{2,3},{3,2},{4,5},{5,4},{6,7},{7,6},{8,9},{9,8},{10,11... | collective-permute-start | bytes 3145736 | tf_op jit(solution)/shard_map/ppermute | solution.py:639
  17.4 14.0 %collective-permute-start.5 = (bf16[256,512]{1,0:T(8,128)(2,1)S(1)}, bf16[256,512]{1,0:T(8,128)(2,1)S(1)}, u32[]{:S(2)}, u32[]{:S(2)}) collective-permute-start(bf16[256,512]{1,0:T(8,128)(2,1)S(1)} %get-tuple-element.25), channel_id=1, source_target_pairs={{0,2},{1,3},{2,0},{3,1},{4,6},{5,7},{6,4},{7,5},{8,10},{9,11},{10,... | collective-permute-start | bytes 786440 | tf_op jit(solution)/shard_map/ppermute | solution.py:644
  17.6 22.8 %copy-start.2 = (bf16[2048,256]{1,0:T(8,128)(2,1)S(1)}, bf16[2048,256]{1,0:T(8,128)(2,1)}, u32[]{:S(2)}) copy-start(bf16[2048,256]{1,0:T(8,128)(2,1)} %refs_15_.5) | copy-start | bytes 3145732
  17.6 22.8 %copy-start.3 = (bf16[2048,256]{1,0:T(8,128)(2,1)S(1)}, bf16[2048,256]{1,0:T(8,128)(2,1)}, u32[]{:S(2)}) copy-start(bf16[2048,256]{1,0:T(8,128)(2,1)} %refs_16_.5) | copy-start | bytes 3145732
  17.6 22.9 %copy-start.5 = (bf16[2048,128]{1,0:T(8,128)(2,1)S(1)}, bf16[2048,128]{1,0:T(8,128)(2,1)}, u32[]{:S(2)}) copy-start(bf16[2048,128]{1,0:T(8,128)(2,1)} %refs_11_.5) | copy-start | bytes 1572868
  17.6 22.9 %copy-start.6 = (bf16[2048,128]{1,0:T(8,128)(2,1)S(1)}, bf16[2048,128]{1,0:T(8,128)(2,1)}, u32[]{:S(2)}) copy-start(bf16[2048,128]{1,0:T(8,128)(2,1)} %refs_12_.5) | copy-start | bytes 1572868
  17.7 22.9 %copy-start.7 = (bf16[2048,128]{1,0:T(8,128)(2,1)S(1)}, bf16[2048,128]{1,0:T(8,128)(2,1)}, u32[]{:S(2)}) copy-start(bf16[2048,128]{1,0:T(8,128)(2,1)} %refs_13_.5) | copy-start | bytes 1572868
  17.7 22.9 %copy-start.8 = (bf16[2048,128]{1,0:T(8,128)(2,1)S(1)}, bf16[2048,128]{1,0:T(8,128)(2,1)}, u32[]{:S(2)}) copy-start(bf16[2048,128]{1,0:T(8,128)(2,1)} %refs_14_.5) | copy-start | bytes 1572868
  17.7 22.9 %copy-start.12 = (bf16[256,256]{1,0:T(8,128)(2,1)S(1)}, bf16[256,256]{1,0:T(8,128)(2,1)}, u32[]{:S(2)}) copy-start(bf16[256,256]{1,0:T(8,128)(2,1)} %constant.5.clone.refs_3_) | copy-start | bytes 393220
  17.7 22.9 %copy-start.13 = (bf16[128,128]{1,0:T(8,128)(2,1)S(1)}, bf16[128,128]{1,0:T(8,128)(2,1)}, u32[]{:S(2)}) copy-start(bf16[128,128]{1,0:T(8,128)(2,1)} %constant.4.clone.refs_2_) | copy-start | bytes 98308
  17.7 22.8 %copy-start.14 = (f32[2048]{0:T(1024)S(1)}, f32[2048]{0:T(1024)}, u32[]{:S(2)}) copy-start(f32[2048]{0:T(1024)} %param.17) | copy-start | bytes 24580
  17.7 19.3 %collective-permute-start.7 = (bf16[256,512]{1,0:T(8,128)(2,1)S(1)}, bf16[256,512]{1,0:T(8,128)(2,1)S(1)}, u32[]{:S(2)}, u32[]{:S(2)}) collective-permute-start(bf16[256,512]{1,0:T(8,128)(2,1)S(1)} %get-tuple-element.27), channel_id=1, source_target_pairs={{0,2},{1,3},{2,0},{3,1},{4,6},{5,7},{6,4},{7,5},{8,10},{9,11},{10,... | collective-permute-start | bytes 786440 | tf_op jit(solution)/shard_map/ppermute | solution.py:644
  31.4 9.1 %collective-permute-start.6 = (bf16[256,512]{1,0:T(8,128)(2,1)S(1)}, bf16[256,512]{1,0:T(8,128)(2,1)S(1)}, u32[]{:S(2)}, u32[]{:S(2)}) collective-permute-start(bf16[256,512]{1,0:T(8,128)(2,1)S(1)} %collective-permute-done.5.refs_8_), channel_id=1, source_target_pairs={{0,1},{1,0},{2,3},{3,2},{4,5},{5,4},{6,7},{7,6},{8,9},{9,8},{10,11... | collective-permute-start | bytes 786440 | tf_op jit(solution)/shard_map/ppermute | solution.py:639
  37.0 7.8 %collective-permute-start.8 = (bf16[256,512]{1,0:T(8,128)(2,1)S(1)}, bf16[256,512]{1,0:T(8,128)(2,1)S(1)}, u32[]{:S(2)}, u32[]{:S(2)}) collective-permute-start(bf16[256,512]{1,0:T(8,128)(2,1)S(1)} %collective-permute-done.7.refs_8_), channel_id=1, source_target_pairs={{0,1},{1,0},{2,3},{3,2},{4,5},{5,4},{6,7},{7,6},{8,9},{9,8},{10,11... | collective-permute-start | bytes 786440 | tf_op jit(solution)/shard_map/ppermute | solution.py:639
  39.6 9.4 %collective-permute-start.10 = (bf16[512,512]{1,0:T(8,128)(2,1)S(1)}, bf16[512,512]{1,0:T(8,128)(2,1)S(1)}, u32[]{:S(2)}, u32[]{:S(2)}) collective-permute-start(bf16[512,512]{1,0:T(8,128)(2,1)S(1)} %collective-permute-done.9.refs_8_), channel_id=1, source_target_pairs={{0,1},{1,0},{2,3},{3,2},{4,5},{5,4},{6,7},{7,6},{8,9},{9,8},{10,11... | collective-permute-start | bytes 1572872 | tf_op jit(solution)/shard_map/ppermute | solution.py:639
  49.1 24.9 %copy-start.18 = (f32[4]{0:T(128)S(1)}, f32[4]{0:T(128)}, u32[]{:S(2)}) copy-start(f32[4]{0:T(128)} %refs_0_.6) | copy-start | bytes 52
  56.7 31.0 %all-to-all-start.1 = ((bf16[8,2,80,128]{3,2,1,0:T(8,128)(2,1)}), bf16[8,2,80,128]{3,2,1,0:T(8,128)(2,1)}, u32[]{:S(2)}, u32[]{:S(2)}) async-start(bf16[8,2,80,128]{3,2,1,0:T(8,128)(2,1)} %totals.1), calls=%async_computation.1 | async-start | bytes 655360 | tf_op jit(solution)/shard_map/all_to_all | solution.py:761
  62.2 30.5 %collective-permute-start = (bf16[256,2048]{1,0:T(8,128)(2,1)}, bf16[256,2048]{1,0:T(8,128)(2,1)}, u32[]{:S(2)}, u32[]{:S(2)}) collective-permute-start(bf16[256,2048]{1,0:T(8,128)(2,1)} %refs_0_.7), channel_id=1, source_target_pairs={{0,1},{1,0},{2,3},{3,2},{4,5},{5,4},{6,7},{7,6},{8,9},{9,8},{10,11... | collective-permute-start | bytes 3145736 | tf_op jit(solution)/shard_map/ppermute | solution.py:639
  62.9 30.0 %collective-permute-start.1 = (bf16[256,2048]{1,0:T(8,128)(2,1)}, bf16[256,2048]{1,0:T(8,128)(2,1)}, u32[]{:S(2)}, u32[]{:S(2)}) collective-permute-start(bf16[256,2048]{1,0:T(8,128)(2,1)} %refs_1_.3), channel_id=1, source_target_pairs={{0,1},{1,0},{2,3},{3,2},{4,5},{5,4},{6,7},{7,6},{8,9},{9,8},{10,11... | collective-permute-start | bytes 3145736 | tf_op jit(solution)/shard_map/ppermute | solution.py:639
  63.0 10.3 %collective-permute-start.11 = (bf16[128,256]{1,0:T(8,128)(2,1)S(1)}, bf16[128,256]{1,0:T(8,128)(2,1)S(1)}, u32[]{:S(2)}, u32[]{:S(2)}) collective-permute-start(bf16[128,256]{1,0:T(8,128)(2,1)S(1)} %get-tuple-element.31), channel_id=1, source_target_pairs={{0,4},{4,8},{8,12},{12,16},{16,20},{20,24},{24,28},{28,0},{1,5},{5... | collective-permute-start | bytes 196616 | tf_op jit(solution)/shard_map/ppermute | solution.py:757
  64.7 8.7 %collective-permute-start.12 = (bf16[128,256]{1,0:T(8,128)(2,1)S(1)}, bf16[128,256]{1,0:T(8,128)(2,1)S(1)}, u32[]{:S(2)}, u32[]{:S(2)}) collective-permute-start(bf16[128,256]{1,0:T(8,128)(2,1)S(1)} %get-tuple-element.32), channel_id=1, source_target_pairs={{4,0},{8,4},{12,8},{16,12},{20,16},{24,20},{28,24},{0,28},{5,1},{9... | collective-permute-start | bytes 196616 | tf_op jit(solution)/shard_map/ppermute | solution.py:758
  80.1 13.1 %collective-permute-start.14 = (bf16[1024,256]{1,0:T(8,128)(2,1)}, bf16[1024,256]{1,0:T(8,128)(2,1)}, u32[]{:S(2)}, u32[]{:S(2)}) collective-permute-start(bf16[1024,256]{1,0:T(8,128)(2,1)} %attend.1.refs_6_), channel_id=1, source_target_pairs={{0,2},{1,3},{2,0},{3,1},{4,6},{5,7},{6,4},{7,5},{8,10},{9,11},{10,... | collective-permute-start | bytes 1572872 | tf_op jit(solution)/shard_map/ppermute | solution.py:644
  81.4 25.4 %collective-permute-start.3 = (bf16[8,1,64,1024]{3,2,1,0:T(8,128)(2,1)}, bf16[8,1,64,1024]{3,2,1,0:T(8,128)(2,1)}, u32[]{:S(2)}, u32[]{:S(2)}) collective-permute-start(bf16[8,1,64,1024]{3,2,1,0:T(8,128)(2,1)} %all-to-all-done.refs_4_), channel_id=1, source_target_pairs={{0,1},{1,0},{2,3},{3,2},{4,5},{5,4},{6,7},{7,6},{8,9},{9,8},{10,11... | collective-permute-start | bytes 3145736 | tf_op jit(solution)/shard_map/ppermute | solution.py:639
  92.3 13.5 %collective-permute-start.17 = (bf16[1024,256]{1,0:T(8,128)(2,1)S(1)}, bf16[1024,256]{1,0:T(8,128)(2,1)S(1)}, u32[]{:S(2)}, u32[]{:S(2)}) collective-permute-start(bf16[1024,256]{1,0:T(8,128)(2,1)S(1)} %cross.1.refs_10_), channel_id=1, source_target_pairs={{0,2},{1,3},{2,0},{3,1},{4,6},{5,7},{6,4},{7,5},{8,10},{9,11},{10,... | collective-permute-start | bytes 1572872 | tf_op jit(solution)/shard_map/ppermute | solution.py:644
  92.6 14.1 %collective-permute-start.13 = (bf16[1024,256]{1,0:T(8,128)(2,1)}, bf16[1024,256]{1,0:T(8,128)(2,1)S(1)}, u32[]{:S(2)}, u32[]{:S(2)}) collective-permute-start(bf16[1024,256]{1,0:T(8,128)(2,1)} %attend.1.refs_6_), channel_id=1, source_target_pairs={{0,1},{1,0},{2,3},{3,2},{4,5},{5,4},{6,7},{7,6},{8,9},{9,8},{10,11... | collective-permute-start | bytes 1572872 | tf_op jit(solution)/shard_map/ppermute | solution.py:639
  92.9 13.8 %collective-permute-start.16 = (bf16[1024,256]{1,0:T(8,128)(2,1)S(1)}, bf16[1024,256]{1,0:T(8,128)(2,1)S(1)}, u32[]{:S(2)}, u32[]{:S(2)}) collective-permute-start(bf16[1024,256]{1,0:T(8,128)(2,1)S(1)} %cross.1.refs_10_), channel_id=1, source_target_pairs={{0,1},{1,0},{2,3},{3,2},{4,5},{5,4},{6,7},{7,6},{8,9},{9,8},{10,11... | collective-permute-start | bytes 1572872 | tf_op jit(solution)/shard_map/ppermute | solution.py:639
  93.2 13.6 %collective-permute-start.15 = (bf16[1024,256]{1,0:T(8,128)(2,1)}, bf16[1024,256]{1,0:T(8,128)(2,1)S(1)}, u32[]{:S(2)}, u32[]{:S(2)}) collective-permute-start(bf16[1024,256]{1,0:T(8,128)(2,1)} %collective-permute-done.14.refs_8_), channel_id=1, source_target_pairs={{0,1},{1,0},{2,3},{3,2},{4,5},{5,4},{6,7},{7,6},{8,9},{9,8},{10,11... | collective-permute-start | bytes 1572872 | tf_op jit(solution)/shard_map/ppermute | solution.py:639
  105.9 6.7 %collective-permute-start.18 = (bf16[1024,256]{1,0:T(8,128)(2,1)S(1)}, bf16[1024,256]{1,0:T(8,128)(2,1)S(1)}, u32[]{:S(2)}, u32[]{:S(2)}) collective-permute-start(bf16[1024,256]{1,0:T(8,128)(2,1)S(1)} %collective-permute-done.17.refs_2_), channel_id=1, source_target_pairs={{0,1},{1,0},{2,3},{3,2},{4,5},{5,4},{6,7},{7,6},{8,9},{9,8},{10,11... | collective-permute-start | bytes 1572872 | tf_op jit(solution)/shard_map/ppermute | solution.py:639
  (13 other events, 79.7 us)

commit v4 on v3

--- a/solution.py
+++ b/solution.py
@@ -18,9 +18,10 @@
 ROPE_BASE = 10000.0
 NEG = -1e30
 EXTRA = 16
-CHUNKS = ((0, 1), (1, 1), (2, 2))
+CHUNKS = ((0, 2), (2, 3), (5, 3))
 ORDER = (2, 0, 1)
 TABLE = 32
+HALVES = 2
 F32 = jnp.float32
 BF16 = jnp.bfloat16
 
@@ -69,86 +70,56 @@
             copy.wait()
 
 
-def slab_kernel(n_far, *refs):
-    att, ret = refs[:2]
-    slabs = refs[2 : 2 + n_far]
+def slab_kernel(chips, *refs):
+    weights = refs[:2]
+    slabs = refs[2:-1]
     copies = Copies(refs[-1])
-    tp, sp = lax.axis_index("tp"), lax.axis_index("sp")
-    chips = n_far + 1
-    for by, slab in enumerate(slabs, 1):
-        share, width = slab.shape[0] // 2, slab.shape[1]
-        target = lax.rem(tp // 2 + by, chips)
-        rows = pl.ds(pl.multiple_of(sp * share, share), share)
+    tp = lax.axis_index("tp")
+    for i, slab in enumerate(slabs):
+        target = lax.rem(tp // 2 + 1 + i // 2, chips)
+        width = slab.shape[1]
         cols = pl.ds(pl.multiple_of(target * width, width), width)
-        for i, ref in enumerate((att, ret)):
-            copies.start(ref.at[rows, cols], slab.at[pl.ds(i * share, share)])
+        copies.start(weights[i % 2].at[:, cols], slab)
     copies.wait()
 
 
 def slab(att, ret, cols):
     chips = lax.axis_size("tp") // 2
-    share = att.shape[0] // lax.axis_size("sp")
-    if share % 16:
-        rows = lax.axis_index("sp") * share
-        out = []
-        for by in range(1, chips):
-            target = lax.rem(lax.axis_index("tp") // 2 + by, chips) * 2 * cols
-            parts = [lax.dynamic_slice(w, (rows, target), (share, 2 * cols)) for w in (att, ret)]
-            out.append(jnp.concatenate(parts, axis=0))
-        return out
-    return pl.pallas_call(
-        functools.partial(slab_kernel, chips - 1),
-        out_shape=(jax.ShapeDtypeStruct((2 * share, 2 * cols), BF16),) * (chips - 1),
+    shape = jax.ShapeDtypeStruct((att.shape[0], 2 * cols), BF16)
+    return pl.pallas_call(
+        functools.partial(slab_kernel, chips),
+        out_shape=(shape,) * (2 * chips - 2),
         in_specs=[HBM, HBM],
-        out_specs=(VMEM,) * (chips - 1),
-        scratch_shapes=[pltpu.SemaphoreType.DMA((2 * chips,))],
+        out_specs=(VMEM,) * (2 * chips - 2),
+        scratch_shapes=[pltpu.SemaphoreType.DMA((2 * chips - 2,))],
         cost_estimate=cost(0.1e9, 3 << 20),
         compiler_params=PARAMS,
         name="slab",
     )(*in_hbm([att, ret]))
 
 
-def split_kernel(n_pieces, *refs):
+def split_kernel(chunks, *refs):
     tokens = refs[0]
-    pieces = refs[1 : 1 + n_pieces]
+    pieces = refs[1 : 1 + len(chunks)]
     copies = Copies(refs[-1])
-    for (first, _), piece in zip(CHUNKS, pieces):
-        rows = pl.ds(first * tokens.shape[0] // 4, piece.shape[0])
+    for (first, _), piece in zip(chunks, pieces):
+        rows = pl.ds(first * tokens.shape[0] // 8, piece.shape[0])
         copies.start(tokens.at[rows], piece)
     copies.wait()
 
 
-def split(tokens):
+def split(tokens, chunks):
     total, cols = tokens.shape
     return pl.pallas_call(
-        functools.partial(split_kernel, len(CHUNKS)),
-        out_shape=tuple(jax.ShapeDtypeStruct((n * total // 4, cols), BF16) for _, n in CHUNKS),
+        functools.partial(split_kernel, chunks),
+        out_shape=tuple(jax.ShapeDtypeStruct((n * total // 8, cols), BF16) for _, n in chunks),
         in_specs=[HBM],
-        out_specs=(VMEM,) * len(CHUNKS),
-        scratch_shapes=[pltpu.SemaphoreType.DMA((len(CHUNKS),))],
+        out_specs=(VMEM,) * len(chunks),
+        scratch_shapes=[pltpu.SemaphoreType.DMA((len(chunks),))],
         cost_estimate=cost(0.1e9, 3 << 20),
         compiler_params=PARAMS,
         name="split",
     )(*in_hbm([tokens]))
-
-
-def repeat_kernel(*refs):
-    out_ref = refs[-1]
-    for s in range(out_ref.shape[0]):
-        for i, ref in enumerate(refs[:-1]):
-            out_ref[s, i] = ref[...]
-
-
-def repeat(slabs, count):
-    return pl.pallas_call(
-        repeat_kernel,
-        out_shape=jax.ShapeDtypeStruct((count, len(slabs)) + slabs[0].shape, BF16),
-        in_specs=[VMEM] * len(slabs),
-        out_specs=VMEM,
-        cost_estimate=cost(0.1e9, 1 << 20),
-        compiler_params=PARAMS,
-        name="repeat",
-    )(*slabs)
 
 
 def prepare_kernel(log_ref, *refs):
@@ -180,8 +151,8 @@
     return pl.pallas_call(
         prepare_kernel,
         out_shape=(
-            pltpu.VMEM((8, total), F32),
-            pltpu.VMEM((total, 8), F32),
+            jax.ShapeDtypeStruct((8, total), F32),
+            jax.ShapeDtypeStruct((total, 8), F32),
             table,
             table,
         ),
@@ -193,11 +164,13 @@
     )(log, *weights)
 
 
-def project_kernel(n_blocks, n_w, parts, first, ret_local, *refs):
+def project_kernel(n_blocks, n_w, n_other, parts, first, ret_local, *refs):
     gain_ref, ccol_ref, swap_ref, mix_ref, cos_ref, sin_ref = refs[:6]
     blocks = refs[6 : 6 + n_blocks]
     w_refs = refs[6 + n_blocks : 6 + n_blocks + n_w]
-    out_ref, sum_ref, low_ref, high_ref = refs[6 + n_blocks + n_w : 10 + n_blocks + n_w]
+    other_refs = refs[6 + n_blocks + n_w : 6 + n_blocks + n_w + n_other]
+    at_out = 6 + n_blocks + n_w + n_other
+    out_ref, sum_ref, low_ref, high_ref = refs[at_out : at_out + 4]
     xn, inv, held, sems = refs[-4:]
     copies = Copies(sems)
     width = blocks[0].shape[1]
@@ -254,24 +227,28 @@
         if group == 1:
             low_ref[...] = raw[rows - WINDOW :]
             high_ref[...] = raw[:WINDOW]
+            for other in other_refs:
+                even = lax.rem(lax.axis_index("sp"), 2) == 0
+                low_ref[...] = jnp.where(even, other[...], raw[:WINDOW])
+                high_ref[...] = jnp.where(even, raw[:WINDOW], other[...])
         held[group] = raw
         copies.start(held.at[group], out_ref.at[group])
     copies.wait()
 
 
-def project(gain, ccol, swap, mix, cos, sin, blocks, weights, parts, first, rows, ret_local):
+def project(gain, ccol, swap, mix, cos, sin, blocks, weights, parts, first, rows, ret_local, other):
     width = mix.shape[0]
     depth = gain.shape[1]
     n = len(blocks)
     return pl.pallas_call(
-        functools.partial(project_kernel, n, len(weights), parts, first, ret_local),
+        functools.partial(project_kernel, n, len(weights), len(other), parts, first, ret_local),
         out_shape=(
             pltpu.HBM((5, rows, width), BF16),
             pltpu.VMEM((ret_local, RK, 2 * RV), F32),
             jax.ShapeDtypeStruct((WINDOW, width), BF16),
             jax.ShapeDtypeStruct((WINDOW, width), BF16),
         ),
-        in_specs=[VMEM] * (n + 6 + len(weights)),
+        in_specs=[VMEM] * (n + 6 + len(weights) + len(other)),
         out_specs=(HBM, VMEM, VMEM, VMEM),
         scratch_shapes=[
             pltpu.VMEM((rows, depth), BF16),
@@ -282,48 +259,66 @@
         cost_estimate=cost(2 * rows * depth * 5 * width // 4, 7 << 20),
         compiler_params=PARAMS,
         name="project",
-    )(gain, ccol, swap, mix, cos, sin, *blocks, *weights)
-
-
-def attend_kernel(n_chunks, kv_local, groups, seq_len, *refs):
+    )(gain, ccol, swap, mix, cos, sin, *blocks, *weights, *other)
+
+
+def overlaps(sizes, first, rows):
+    out = []
+    at = 0
+    for i, size in enumerate(sizes):
+        low, high = max(at, first), min(at + size, first + rows)
+        if low < high:
+            out.append((i, low - at, high - low, low - first))
+        at += size
+    return out
+
+
+def attend_kernel(n_chunks, kv_local, groups, seq_len, total, start, *refs):
     sink_ref = refs[0]
     proj = refs[1 : 1 + n_chunks]
     low_ref, high_ref, out_ref = refs[1 + n_chunks : 4 + n_chunks]
     qbuf, kvbuf, vbuf, mask, sems = refs[-5:]
     copies = Copies(sems)
-    total = sum(ref.shape[1] for ref in proj)
+    rows = out_ref.shape[0]
     offset = lax.axis_index("sp") * total
     kv_cols = kv_local * HD
     block = WINDOW
     span = block + 2 * WINDOW
-    copies.start(low_ref, kvbuf.at[pl.ds(0, WINDOW)])
-    copies.start(high_ref, kvbuf.at[pl.ds(WINDOW + total, WINDOW)])
-    for group, buf, at in ((1, kvbuf, WINDOW), (0, qbuf, 0)):
-        for ref in proj:
-            copies.start(ref.at[group], buf.at[pl.ds(at, ref.shape[1])])
-            at += ref.shape[1]
+    sizes = [WINDOW] + [ref.shape[1] for ref in proj] + [WINDOW]
+    for i, low, count, to in overlaps(sizes, start, rows + 2 * WINDOW):
+        if i in (0, n_chunks + 1):
+            even = lax.rem(lax.axis_index("sp"), 2) == 0
+            here = pl.ds(low, count)
+            near, far = (high_ref, low_ref) if i == 0 else (low_ref, high_ref)
+            kvbuf[pl.ds(to, count)] = jnp.where(even, near[here], far[here])
+        else:
+            copies.start(proj[i - 1].at[1, pl.ds(low, count)], kvbuf.at[pl.ds(to, count)])
+    n_kv = len(copies.copies)
+    for i, low, count, to in overlaps(sizes[1:-1], start, rows):
+        copies.start(proj[i].at[0, pl.ds(low, count)], qbuf.at[pl.ds(to, count)])
     vbuf[kv_cols:] = jnp.ones((vbuf.shape[0] - kv_cols, vbuf.shape[1]), BF16)
     row = lax.broadcasted_iota(jnp.int32, (span, block), 1)
     col = lax.broadcasted_iota(jnp.int32, (span, block), 0)
     band = (col >= row) & (col <= row + 2 * WINDOW)
-    for i, first in enumerate((0, block, total - block)):
-        pos = col + (offset + first - WINDOW)
-        allowed = band & (pos >= 0) & (pos < seq_len)
-        one = jnp.where(allowed, 0.0, NEG)
-        mask[i] = jnp.concatenate([one] * groups, axis=1)
-    copies.wait()
+    n_steps = rows // block
+    edges = [i for i in range(n_steps) if start + i * block in (0, total - block)]
+    inner = jnp.where(band, 0.0, NEG)
+    mask[0] = jnp.concatenate([inner] * groups, axis=1)
+    for kind, i in enumerate(edges, 1):
+        pos = col + (offset + start + i * block - WINDOW)
+        one = jnp.where((pos >= 0) & (pos < seq_len), inner, NEG)
+        mask[kind] = jnp.concatenate([one] * groups, axis=1)
+    copies.wait(0, n_kv)
     for i in range(kvbuf.shape[0] // block):
         here = pl.ds(i * block, block)
         vbuf[0:kv_cols, here] = kvbuf[here, kv_cols:].T
+    copies.wait(n_kv)
     lane = lax.broadcasted_iota(jnp.int32, (block, kv_cols), 1)
-    n_steps = total // block
-
-    def step(i, carry):
-        first = pl.multiple_of(i * block, block)
+    for i in range(n_steps):
+        first = i * block
         q = qbuf[pl.ds(first, block)]
         k = kvbuf[pl.ds(first, span), :kv_cols]
-        kind = jnp.where(i == 0, 0, jnp.where(i == n_steps - 1, 2, 1))
-        bias = mask[kind]
+        bias = mask[edges.index(i) + 1 if i in edges else 0]
         scores = []
         for g in range(kv_local):
             mine = (lane >= g * HD) & (lane < (g + 1) * HD)
@@ -350,32 +345,29 @@
             o = o[:HD] / (o[HD : HD + 1] + rests[g])
             outs += [o[:, j * block : (j + 1) * block] for j in range(groups)]
         out_ref[pl.ds(first, block)] = jnp.concatenate(outs, axis=0).T.astype(BF16)
-        return carry
-
-    lax.fori_loop(0, n_steps, step, 0, unroll=n_steps)
-
-
-def attend(sink, proj, low, high, kv_local, groups, seq_len):
+
+
+def attend(sink, proj, low, high, kv_local, groups, seq_len, start, rows):
     n = len(proj)
     width = proj[0].shape[2]
     total = sum(p.shape[1] for p in proj)
     kv_cols = kv_local * HD
     return pl.pallas_call(
-        functools.partial(attend_kernel, n, kv_local, groups, seq_len),
-        out_shape=jax.ShapeDtypeStruct((total, width), BF16),
-        in_specs=[SMEM] + [HBM] * (n + 2),
+        functools.partial(attend_kernel, n, kv_local, groups, seq_len, total, start),
+        out_shape=jax.ShapeDtypeStruct((rows, width), BF16),
+        in_specs=[SMEM] + [HBM] * n + [VMEM, VMEM],
         out_specs=VMEM,
         scratch_shapes=[
-            pltpu.VMEM((total, width), BF16),
-            pltpu.VMEM((total + 2 * WINDOW, 2 * kv_cols), BF16),
-            pltpu.VMEM((kv_cols + 16, total + 2 * WINDOW), BF16),
+            pltpu.VMEM((rows, width), BF16),
+            pltpu.VMEM((rows + 2 * WINDOW, 2 * kv_cols), BF16),
+            pltpu.VMEM((kv_cols + 16, rows + 2 * WINDOW), BF16),
             pltpu.VMEM((3, 3 * WINDOW, groups * WINDOW), F32),
             pltpu.SemaphoreType.DMA((2 * n + 2,)),
         ],
-        cost_estimate=cost(1.5e9, 3 << 20),
+        cost_estimate=cost(0.8e9, 3 << 20),
         compiler_params=PARAMS,
         name="attend",
-    )(sink, *in_hbm([*proj, low, high]))
+    )(sink, *in_hbm(proj), low, high)
 
 
 def totals_kernel(n_chunks, ret_local, n_sp, *refs):
@@ -413,67 +405,21 @@
     )(ccol, *sums)
 
 
-def local_kernel(n_chunks, ret_local, *refs):
-    ccol_ref, crow_ref = refs[:2]
-    proj = refs[2 : 2 + n_chunks]
-    out_ref = refs[2 + n_chunks]
-    rbuf, vbuf, sems = refs[-3:]
-    total = crow_ref.shape[1]
+def retain_kernel(n_chunks, ret_local, n_sp, *refs):
+    ccol_hbm, crow_hbm, got_hbm, init_hbm = refs[:4]
+    proj = refs[4 : 4 + n_chunks]
+    outs = refs[4 + n_chunks : 4 + n_chunks + HALVES]
+    states, got_ref, init_ref, ccol_ref, crow_ref, rbuf, vbuf, gbuf, sems = refs[-9:]
+    me = lax.axis_index("sp")
+    total = ccol_ref.shape[0]
+    last = total - 1
     cols = ret_local * RK
-    copies = Copies(sems)
-    for group, buf in ((2, rbuf), (3, vbuf)):
-        at = 0
-        for ref in proj:
-            copies.start(ref.at[group], buf.at[pl.ds(at, ref.shape[1])])
-            at += ref.shape[1]
-    copies.wait()
-    block = min(256, total)
-    lane = lax.broadcasted_iota(jnp.int32, (block, cols), 1)
-
-    def step(i, carry):
-        here = pl.ds(pl.multiple_of(i * block, block), block)
-        q = rbuf[here, :cols]
-        for h in range(ret_local):
-            mine = (lane >= h * RK) & (lane < (h + 1) * RK)
-            qh = jnp.where(mine, q, jnp.zeros_like(q))
-            gap = ccol_ref[here, h : h + 1] - crow_ref[h : h + 1, :]
-            w = (dot_t(qh, rbuf[:, cols:]) * jnp.exp(-jnp.abs(gap))).astype(BF16)
-            out_ref[here, h * RV : (h + 1) * RV] = dot(w, vbuf[:, h * RV : (h + 1) * RV])
-        return carry
-
-    lax.fori_loop(0, total // block, step, 0)
-
-
-def local(ccol, crow, proj, ret_local):
-    n = len(proj)
-    width = proj[0].shape[2]
-    total = crow.shape[1]
-    return pl.pallas_call(
-        functools.partial(local_kernel, n, ret_local),
-        out_shape=pltpu.VMEM((total, width), F32),
-        in_specs=[VMEM, VMEM] + [HBM] * n,
-        out_specs=VMEM,
-        scratch_shapes=[
-            pltpu.VMEM((total, width), BF16),
-            pltpu.VMEM((total, width), BF16),
-            pltpu.SemaphoreType.DMA((2 * n,)),
-        ],
-        cost_estimate=cost(1e9, 3 << 20),
-        compiler_params=PARAMS,
-        name="local",
-    )(*in_vmem([ccol, crow]), *in_hbm(proj))
-
-
-def cross_kernel(n_chunks, ret_local, n_sp, *refs):
-    ccol_ref, loc_ref, got_hbm, init_hbm = refs[:4]
-    proj = refs[4 : 4 + n_chunks]
-    out_ref, states, got_ref, init_ref, qbuf, gbuf, sems = refs[-7:]
-    me = lax.axis_index("sp")
-    last = ccol_ref.shape[0] - 1
     copies = Copies(sems)
     copies.start(got_hbm, got_ref)
     copies.start(init_hbm, init_ref)
-    for group, buf in ((2, qbuf), (4, gbuf)):
+    copies.start(ccol_hbm, ccol_ref)
+    copies.start(crow_hbm, crow_ref)
+    for group, buf in ((2, rbuf), (3, vbuf), (4, gbuf)):
         at = 0
         for ref in proj:
             copies.start(ref.at[group], buf.at[pl.ds(at, ref.shape[1])])
@@ -497,15 +443,23 @@
             col = (2 * h + side) * RV
             states[h * RK : (h + 1) * RK, col : col + RV] = state.astype(BF16)
     copies.wait(2)
-    block = min(256, last + 1)
-    for i in range((last + 1) // block):
+    block = min(256, total // HALVES)
+    lane = lax.broadcasted_iota(jnp.int32, (block, cols), 1)
+    for i in range(total // block):
         here = pl.ds(i * block, block)
-        both = dot(qbuf[here, : ret_local * RK], states[...])
+        out_ref = outs[i * block * HALVES // total]
+        there = pl.ds(i * block % (total // HALVES), block)
+        q = rbuf[here, :cols]
+        both = dot(q, states[...])
         for h in range(ret_local):
+            mine = (lane >= h * RK) & (lane < (h + 1) * RK)
+            qh = jnp.where(mine, q, jnp.zeros_like(q))
             col = ccol_ref[here, h : h + 1]
             end = ccol_ref[last : last + 1, h : h + 1]
+            gap = col - crow_ref[h : h + 1, :]
+            w = (dot_t(qh, rbuf[:, cols:]) * jnp.exp(-jnp.abs(gap))).astype(BF16)
             ret = (
-                loc_ref[here, h * RV : (h + 1) * RV]
+                dot(w, vbuf[:, h * RV : (h + 1) * RV])
                 + jnp.exp(col) * both[:, 2 * h * RV : (2 * h + 1) * RV]
                 + jnp.exp(end - col) * both[:, (2 * h + 1) * RV : (2 * h + 2) * RV]
             )
@@ -513,36 +467,40 @@
             scale = lax.rsqrt(jnp.mean(centered * centered, axis=1, keepdims=True) + NORM_EPS)
             gate = gbuf[here, h * RV : (h + 1) * RV].astype(F32)
             gated = gate / (1.0 + jnp.exp(-gate))
-            out_ref[here, h * RV : (h + 1) * RV] = (gated * (centered * scale)).astype(BF16)
-
-
-def cross(ccol, got, init, loc, proj, ret_local, n_sp):
+            out_ref[there, h * RV : (h + 1) * RV] = (gated * (centered * scale)).astype(BF16)
+
+
+def retain(ccol, crow, got, init, proj, ret_local, n_sp):
     n = len(proj)
     width = proj[0].shape[2]
     total = ccol.shape[0]
     return pl.pallas_call(
-        functools.partial(cross_kernel, n, ret_local, n_sp),
-        out_shape=jax.ShapeDtypeStruct((total, width), BF16),
-        in_specs=[VMEM, VMEM] + [HBM] * (n + 2),
-        out_specs=VMEM,
+        functools.partial(retain_kernel, n, ret_local, n_sp),
+        out_shape=(jax.ShapeDtypeStruct((total // HALVES, width), BF16),) * HALVES,
+        in_specs=[HBM] * (n + 4),
+        out_specs=(VMEM,) * HALVES,
         scratch_shapes=[
             pltpu.VMEM((ret_local * RK, 2 * ret_local * RV), BF16),
             pltpu.VMEM(got.shape, BF16),
             pltpu.VMEM(init.shape, F32),
+            pltpu.VMEM(ccol.shape, F32),
+            pltpu.VMEM(crow.shape, F32),
             pltpu.VMEM((total, width), BF16),
             pltpu.VMEM((total, width), BF16),
-            pltpu.SemaphoreType.DMA((2 * n + 2,)),
+            pltpu.VMEM((total, width), BF16),
+            pltpu.SemaphoreType.DMA((3 * n + 4,)),
         ],
-        cost_estimate=cost(0.5e9, 4 << 20),
-        compiler_params=PARAMS,
-        name="cross",
-    )(*in_vmem([ccol, loc]), *in_hbm([got, init]), *in_vmem(proj))
-
-
-def most_kernel(n_data, *refs):
-    near_att, near_ret, peer_att, peer_ret, spread, peer_spread = refs[:6]
-    data = refs[6 : 6 + n_data]
-    out_ref, rest_ref = refs[6 + n_data : 8 + n_data]
+        cost_estimate=cost(1.5e9, 4 << 20),
+        compiler_params=PARAMS,
+        name="retain",
+    )(*in_hbm([ccol, crow, got, init, *proj]))
+
+
+def most_kernel(n_far, n_data, *refs):
+    near_att, near_ret, peer_att, peer_ret = refs[:4]
+    far_att, far_ret = refs[4 : 4 + n_far], refs[4 + n_far : 4 + 2 * n_far]
+    data = refs[4 + 2 * n_far : 4 + 2 * n_far + n_data]
+    out_ref, rest_ref = refs[4 + 2 * n_far + n_data : 6 + 2 * n_far + n_data]
     left, right, sems = refs[-3:]
     copies = Copies(sems)
     cols = out_ref.shape[1]
@@ -550,26 +508,15 @@
     mine = pl.ds(pl.multiple_of(tp * cols, cols), cols)
     half = pl.ds(pl.multiple_of(lax.rem(tp, 2) * cols, cols), cols)
     depth = near_att.shape[0]
-    share = spread.shape[2] // 2
-    at = 0
-    for ref in (near_att, peer_att):
-        copies.start(ref.at[:, mine], right.at[pl.ds(at, depth)])
-        at += depth
-    below = 0
-    for far in range(spread.shape[1]):
-        for ref in (spread, peer_spread):
-            for s in range(spread.shape[0]):
-                from_att = ref.at[s, far, pl.ds(0, share), half]
-                from_ret = ref.at[s, far, pl.ds(share, share), half]
-                copies.start(from_att, right.at[pl.ds(at + s * share, share)])
-                copies.start(from_ret, rest_ref.at[pl.ds(below + s * share, share)])
-            at += depth
-            below += depth
-    for ref in (near_ret, peer_ret):
-        copies.start(ref.at[:, mine], right.at[pl.ds(at, depth)])
-        at += depth
+    rows = [(ref, mine) for ref in (near_att, peer_att)] + [(ref, half) for ref in far_att]
+    rows += [(ref, mine) for ref in (near_ret, peer_ret)]
+    for i, (ref, at) in enumerate(rows):
+        copies.start(ref.at[:, at], right.at[pl.ds(i * depth, depth)])
     for i, ref in enumerate(data):
-        copies.start(ref, left.at[:, pl.ds(i * depth, depth)])
+        half_rows = pl.ds(i % HALVES * ref.shape[0], ref.shape[0])
+        copies.start(ref, left.at[half_rows, pl.ds(i // HALVES * depth, depth)])
+    for i, ref in enumerate(far_ret):
+        copies.start(ref.at[:, half], rest_ref.at[pl.ds(i * depth, depth)])
     copies.wait()
     rows = min(256, out_ref.shape[0])
     for i in range(out_ref.shape[0] // rows):
@@ -578,23 +525,21 @@
 
 
 def most(weights, data, cols):
-    total, depth = data[0].shape
+    total, depth = data[0].shape[0] * HALVES, data[0].shape[1]
     n = len(data)
-    spread = weights[4]
-    count = 4 + 4 * spread.shape[0] * spread.shape[1] + n
-    rest = 2 * spread.shape[1] * depth
-    return pl.pallas_call(
-        functools.partial(most_kernel, n),
+    n_far = (len(weights) - 4) // 2
+    return pl.pallas_call(
+        functools.partial(most_kernel, n_far, n),
         out_shape=(
             pltpu.VMEM((total, cols), F32),
-            pltpu.VMEM((rest, cols), BF16),
+            pltpu.VMEM((n_far * depth, cols), BF16),
         ),
-        in_specs=[HBM] * (6 + n),
+        in_specs=[HBM] * (len(weights) + n),
         out_specs=(VMEM, VMEM),
         scratch_shapes=[
-            pltpu.VMEM((total, n * depth), BF16),
-            pltpu.VMEM((n * depth, cols), BF16),
-            pltpu.SemaphoreType.DMA((count,)),
+            pltpu.VMEM((total, n // HALVES * depth), BF16),
+            pltpu.VMEM((n // HALVES * depth, cols), BF16),
+            pltpu.SemaphoreType.DMA((len(weights) + n,)),
         ],
         cost_estimate=cost(1e9, 8 << 20),
         compiler_params=PARAMS,
@@ -602,7 +547,7 @@
     )(*in_hbm(weights), *in_hbm(data))
 
 
-def last_kernel(n_data, *refs):
+def last_kernel(n_data, start, *refs):
     base, right = refs[:2]
     data = refs[2 : 2 + n_data]
     out_ref, held, sems = refs[-3:]
@@ -610,28 +555,33 @@
     rows = held.shape[1]
     for i in range(held.shape[0]):
         here = pl.ds(i * rows, rows)
+        there = pl.ds(start + i * rows, rows)
         part = dot(jnp.concatenate([ref[here] for ref in data], axis=1), right[...])
-        held[i] = (part + base[here]).astype(BF16)
-        copies.start(held.at[i], out_ref.at[here])
+        held[i] = (part + base[there]).astype(BF16)
+        copies.start(held.at[i], out_ref.at[there])
     copies.wait()
 
 
-def last(base, right, data):
+def last(base, right, data, start, done):
     total, cols = base.shape
-    rows = min(256, total)
-    return pl.pallas_call(
-        functools.partial(last_kernel, len(data)),
+    part = data[0].shape[0]
+    rows = min(256, part)
+    n = len(data)
+    extra = [] if done is None else [done]
+    return pl.pallas_call(
+        functools.partial(last_kernel, n, start),
         out_shape=jax.ShapeDtypeStruct((total, cols), BF16),
-        in_specs=[VMEM] * (2 + len(data)),
+        in_specs=[VMEM] * (2 + n) + [HBM] * len(extra),
         out_specs=HBM,
         scratch_shapes=[
-            pltpu.VMEM((total // rows, rows, cols), BF16),
-            pltpu.SemaphoreType.DMA((total // rows,)),
+            pltpu.VMEM((part // rows, rows, cols), BF16),
+            pltpu.SemaphoreType.DMA((part // rows,)),
         ],
-        cost_estimate=cost(1e9, 8 << 20),
+        input_output_aliases={} if done is None else {2 + n: 0},
+        cost_estimate=cost(0.5e9, 4 << 20),
         compiler_params=PARAMS,
         name="last",
-    )(*in_vmem([base, right]), *data)
+    )(*in_vmem([base, right]), *data, *extra)
 
 
 def core_swap(value):
@@ -663,20 +613,13 @@
 
 
 def output_weights(out_att, out_ret, slabs):
-    n_sp = lax.axis_size("sp")
-    moved = []
-    for by, slab in enumerate(slabs, 1):
-        moved.append(chip_turn(slab, by))
-    spread = repeat(moved, n_sp)
-    spread = lax.all_to_all(spread, "sp", 0, 0, tiled=True)
-    share, cols = slabs[0].shape[0] // 2, slabs[0].shape[1]
-    if share % 16:
-        shape = (n_sp, len(slabs), 2, share, cols)
-        spread = jnp.transpose(spread.reshape(shape), (1, 2, 0, 3, 4))
-        spread = spread.reshape(1, len(slabs), -1, cols)
     peers = [core_swap(w) for w in (out_att, out_ret)]
-    peer_spread = core_swap(spread)
-    return [out_att, out_ret] + peers + [spread, peer_spread]
+    att, ret = [], []
+    for i, piece in enumerate(slabs):
+        by = i // 2 + 1
+        moved = chip_turn(piece, by)
+        (att if i % 2 == 0 else ret).extend([moved, core_swap(moved)])
+    return [out_att, out_ret] + peers + att + ret
 
 
 def body(
@@ -706,7 +649,7 @@
     cols = tokens.shape[1]
 
     slabs = slab(out_att, out_ret, cols)
-    pieces = split(tokens)
+    pieces = split(tokens, CHUNKS)
     near = core_swap(tokens)
     far = {}
     for c in ORDER:
@@ -746,26 +689,31 @@
     sums = [None] * len(CHUNKS)
     edges = [None] * len(CHUNKS)
     for c in ORDER:
-        first, rows = CHUNKS[c][0] * total // 4, CHUNKS[c][1] * total // 4
+        first, rows = CHUNKS[c][0] * total // 8, CHUNKS[c][1] * total // 8
         proj[c], sums[c], *edges[c] = project(
             gain, ccol, swap, mix, cos, sin, [tokens, near] + far[c], weights, parts,
-            first, rows, ret_local,
+            first, rows, ret_local, [edges[-1][0]] if c == 0 else [],
         )
 
-    forward = [(i, (i + 1) % n_sp) for i in range(n_sp)]
-    backward = [(target, source) for source, target in forward]
-    low = lax.ppermute(edges[-1][0], "sp", forward)
-    high = lax.ppermute(edges[0][1], "sp", backward)
-
+    edge0 = lax.ppermute(edges[0][0], "sp", [(i, i ^ 1) for i in range(n_sp)])
+    turn = [(i, (((i + 1) ^ 1) + n_sp - 1) % n_sp) for i in range(n_sp)]
+    edge1 = lax.ppermute(edges[0][1], "sp", turn)
     sent = totals(ccol, sums, n_sp)
     got = lax.all_to_all(sent, "sp", 0, 0, tiled=True)
-    attended = attend(att_sink, proj, low, high, kv_local, groups, seq_len)
-    att_blocks = gather_tp(attended)
-    loc = local(ccol, crow, proj, ret_local)
-    kept = cross(ccol, got, init_state, loc, proj, ret_local, n_sp)
-    ret_blocks = gather_tp(kept)
-    base, right = most(out_w, att_blocks + ret_blocks[:2], cols)
-    return last(base, right, ret_blocks[2:])
+    part = total // HALVES
+    att_blocks = []
+    for i in range(HALVES):
+        attended = attend(att_sink, proj, edge0, edge1, kv_local, groups, seq_len, i * part, part)
+        att_blocks.append(gather_tp(attended))
+    kept = retain(ccol, crow, got, init_state, proj, ret_local, n_sp)
+    ret_blocks = [gather_tp(kept[i]) for i in range(HALVES)]
+    att_pieces = [block for pair in zip(*att_blocks) for block in pair]
+    ret_pieces = [block for pair in zip(*ret_blocks) for block in pair]
+    base, right = most(out_w, att_pieces + ret_pieces[: 2 * HALVES], cols)
+    done = None
+    for i in range(HALVES):
+        done = last(base, right, ret_blocks[i][2:], i * part, done)
+    return done
 
 
 def solution(mesh):

time: 115 us -> 119 us (1.035)
  the two profiles are of different devices: /device:TPU:1 before, /device:TPU:0 now
where the time goes in v4:
time: 119 us
  waiting for transfers between devices  51 us (43%)
  Pallas kernels  38.7 us (33%)
  starting transfers between devices  26.9 us (23%)
  local copies, waits for them, and re-layouts  1.61 us (1%)
    ppermute x9, waiting for transfers between devices, chip_turn(): return lax.ppermute(value, 'tp', [(i, (i + 2 * by) % n) for i in range(n)])  42.7 us
    pallas_call x3, Pallas kernels, project(): pl.pallas_call(functools.partial(project_kernel, n, len(weights), len(oth...  14.5 us
    ppermute x9, starting transfers between devices, chip_turn(): return lax.ppermute(value, 'tp', [(i, (i + 2 * by) % n) for i in range(n)])  12.8 us
    pallas_call x2, Pallas kernels, attend(): pl.pallas_call(functools.partial(attend_kernel, n, kv_local, groups, seq_...  7.17 us
    pallas_call x1, Pallas kernels, retain(): pl.pallas_call(functools.partial(retain_kernel, n, ret_local, n_sp), out_...  6.16 us
    all_to_all x1, starting transfers between devices, body(): got = lax.all_to_all(sent, 'sp', 0, 0, tiled=True)  5.8 us
    ppermute x1, waiting for transfers between devices, body(): edge0 = lax.ppermute(edges[0][0], 'sp', [(i, i ^ 1) for i in range(n_sp)])  4.73 us
    pallas_call x1, Pallas kernels, most(): pl.pallas_call(functools.partial(most_kernel, n_far, n), out_shape=(pltpu...  4.47 us
  transfers between devices with their start and end apart: 28, of which 7 were waited for; matrix products, arithmetic and copies ran while one was open for 0% of the time, Pallas kernels for 32%

profile of v4, /device:TPU:0, one launch (start us, length us, event | category | flops | bytes accessed | tf_op | source)
XLA Modules:
  0.0 118.9 jit_solution(1661696222293189121)
XLA Ops:
  0.6 1.3 %split.1 = (bf16[256,512]{1,0:T(8,128)(2,1)S(1)}, bf16[384,512]{1,0:T(8,128)(2,1)S(1)}, bf16[384,512]{1,0:T(8,128)(2,1)S(1)}) custom-call(bf16[1024,512]{1,0:T(8,128)(2,1)} %refs_6_.5), custom_call_target="tpu_custom_call" | custom-call | flops 100000000 | bytes 3145728 | tf_op jit(solution)/shard_map/split/pallas_call | solution.py:113
  1.9 2.6 %collective-permute-start.9 = (bf16[384,512]{1,0:T(8,128)(2,1)S(1)}, bf16[384,512]{1,0:T(8,128)(2,1)S(1)}, u32[]{:S(2)}, u32[]{:S(2)}) collective-permute-start(bf16[384,512]{1,0:T(8,128)(2,1)S(1)} %get-tuple-element.33), channel_id=1, source_target_pairs={{0,2},{1,3},{2,0},{3,1},{4,6},{5,7},{6,4},{7,5},{8,10},{9,11},{10,... | collective-permute-start | bytes 1179656 | tf_op jit(solution)/shard_map/ppermute | solution.py:594
  4.5 1.2 %slab.1 = (bf16[256,1024]{1,0:T(8,128)(2,1)S(1)}, bf16[256,1024]{1,0:T(8,128)(2,1)S(1)}) custom-call(bf16[256,2048]{1,0:T(8,128)(2,1)} %refs_0_.9, bf16[256,2048]{1,0:T(8,128)(2,1)} %refs_1_.3), custom_call_target="tpu_custom_call" | custom-call | flops 100000000 | bytes 3145728 | tf_op jit(solution)/shard_map/slab/pallas_call | solution.py:89
  5.8 2.0 %collective-permute-start.11 = (bf16[384,512]{1,0:T(8,128)(2,1)S(1)}, bf16[384,512]{1,0:T(8,128)(2,1)S(1)}, u32[]{:S(2)}, u32[]{:S(2)}) collective-permute-start(bf16[384,512]{1,0:T(8,128)(2,1)S(1)} %get-tuple-element.36), channel_id=1, source_target_pairs={{0,2},{1,3},{2,0},{3,1},{4,6},{5,7},{6,4},{7,5},{8,10},{9,11},{10,... | collective-permute-start | bytes 1179656 | tf_op jit(solution)/shard_map/ppermute | solution.py:594
  7.8 6.6 %collective-permute-done.9.refs_8_ = bf16[384,512]{1,0:T(8,128)(2,1)S(1)} collective-permute-done((bf16[384,512]{1,0:T(8,128)(2,1)S(1)}, bf16[384,512]{1,0:T(8,128)(2,1)S(1)}, u32[]{:S(2)}, u32[]{:S(2)}) %collective-permute-start.9) | collective-permute-done | bytes 393248 | tf_op jit(solution)/shard_map/ppermute | solution.py:594
  14.5 2.0 %collective-permute-start.7 = (bf16[256,512]{1,0:T(8,128)(2,1)S(1)}, bf16[256,512]{1,0:T(8,128)(2,1)S(1)}, u32[]{:S(2)}, u32[]{:S(2)}) collective-permute-start(bf16[256,512]{1,0:T(8,128)(2,1)S(1)} %get-tuple-element.32), channel_id=1, source_target_pairs={{0,2},{1,3},{2,0},{3,1},{4,6},{5,7},{6,4},{7,5},{8,10},{9,11},{10,... | collective-permute-start | bytes 786440 | tf_op jit(solution)/shard_map/ppermute | solution.py:594
  16.5 22.9 %collective-permute-done.7.refs_8_ = bf16[256,512]{1,0:T(8,128)(2,1)S(1)} collective-permute-done((bf16[256,512]{1,0:T(8,128)(2,1)S(1)}, bf16[256,512]{1,0:T(8,128)(2,1)S(1)}, u32[]{:S(2)}, u32[]{:S(2)}) %collective-permute-start.7) | collective-permute-done | bytes 262176 | tf_op jit(solution)/shard_map/ppermute | solution.py:594
  40.1 1.8 %collective-permute-start.4 = (bf16[256,1024]{1,0:T(8,128)(2,1)S(1)}, bf16[256,1024]{1,0:T(8,128)(2,1)}, u32[]{:S(2)}, u32[]{:S(2)}) collective-permute-start(bf16[256,1024]{1,0:T(8,128)(2,1)S(1)} %get-tuple-element.28), channel_id=1, source_target_pairs={{0,2},{1,3},{2,0},{3,1},{4,6},{5,7},{6,4},{7,5},{8,10},{9,11},{10,... | collective-permute-start | bytes 1572872 | tf_op jit(solution)/shard_map/ppermute | solution.py:594
  42.4 0.8 prepare.1
  43.3 5.4 %project.3 = (bf16[5,384,256]{2,1,0:T(8,128)(2,1)}, f32[2,64,256]{2,1,0:T(8,128)S(1)}, bf16[128,256]{1,0:T(8,128)(2,1)S(1)}, bf16[128,256]{1,0:T(8,128)(2,1)}) custom-call(f32[1,2048]{1,0:T(1,128)S(1)} %bitcast.1, f32[1024,8]{1,0:T(8,128)S(1)} %get-tuple-element.29.refs_1_.refs_0_, bf16[128,128]{1,0:T(8,128)(2,1)S(1)} %copy-done.12, ...), custom_call_target="tpu_custom_call" | custom-call | flops 503316480 | bytes 7340032 | tf_op jit(solution)/shard_map/project/pallas_call | solution.py:243
  48.9 5.5 %project.5 = (bf16[5,384,256]{2,1,0:T(8,128)(2,1)}, f32[2,64,256]{2,1,0:T(8,128)S(1)}, bf16[128,256]{1,0:T(8,128)(2,1)}, bf16[128,256]{1,0:T(8,128)(2,1)}) custom-call(f32[1,2048]{1,0:T(1,128)S(1)} %bitcast.2, f32[1024,8]{1,0:T(8,128)S(1)} %get-tuple-element.29.refs_1_.refs_0_, bf16[128,128]{1,0:T(8,128)(2,1)S(1)} %copy-done.12, ...), custom_call_target="tpu_custom_call" | custom-call | flops 503316480 | bytes 7340032 | tf_op jit(solution)/shard_map/project/pallas_call | solution.py:243
  54.4 3.6 %project.4 = (bf16[5,256,256]{2,1,0:T(8,128)(2,1)}, f32[2,64,256]{2,1,0:T(8,128)S(1)}, bf16[128,256]{1,0:T(8,128)(2,1)S(1)}, bf16[128,256]{1,0:T(8,128)(2,1)S(1)}) custom-call(f32[1,2048]{1,0:T(1,128)S(1)} %bitcast.3, f32[1024,8]{1,0:T(8,128)S(1)} %get-tuple-element.29.refs_1_.refs_0_, bf16[128,128]{1,0:T(8,128)(2,1)S(1)} %copy-done.12, ...), custom_call_target="tpu_custom_call" | custom-call | flops 335544320 | bytes 7340032 | tf_op jit(solution)/shard_map/project/pallas_call | solution.py:243
  58.0 0.8 totals.1
  58.9 5.8 %all-to-all-start = ((bf16[8,2,80,128]{3,2,1,0:T(8,128)(2,1)}), bf16[8,2,80,128]{3,2,1,0:T(8,128)(2,1)}, u32[]{:S(2)}, u32[]{:S(2)}) async-start(bf16[8,2,80,128]{3,2,1,0:T(8,128)(2,1)} %totals.1), calls=%async_computation | async-start | bytes 655360 | tf_op jit(solution)/shard_map/all_to_all | solution.py:702
  64.9 1.9 %collective-permute-start.13 = (bf16[128,256]{1,0:T(8,128)(2,1)S(1)}, bf16[128,256]{1,0:T(8,128)(2,1)S(1)}, u32[]{:S(2)}, u32[]{:S(2)}) collective-permute-start(bf16[128,256]{1,0:T(8,128)(2,1)S(1)} %get-tuple-element.39), channel_id=1, source_target_pairs={{0,4},{4,0},{8,12},{12,8},{16,20},{20,16},{24,28},{28,24},{1,5},{5... | collective-permute-start | bytes 196616 | tf_op jit(solution)/shard_map/ppermute | solution.py:698
  66.8 4.7 %collective-permute-done.13.refs_4_ = bf16[128,256]{1,0:T(8,128)(2,1)S(1)} collective-permute-done((bf16[128,256]{1,0:T(8,128)(2,1)S(1)}, bf16[128,256]{1,0:T(8,128)(2,1)S(1)}, u32[]{:S(2)}, u32[]{:S(2)}) %collective-permute-start.13) | collective-permute-done | bytes 65568 | tf_op jit(solution)/shard_map/ppermute | solution.py:698
  71.5 3.4 %collective-permute-start.14 = (bf16[128,256]{1,0:T(8,128)(2,1)S(1)}, bf16[128,256]{1,0:T(8,128)(2,1)S(1)}, u32[]{:S(2)}, u32[]{:S(2)}) collective-permute-start(bf16[128,256]{1,0:T(8,128)(2,1)S(1)} %get-tuple-element.40), channel_id=1, source_target_pairs={{0,28},{4,8},{8,4},{12,16},{16,12},{20,24},{24,20},{28,0},{1,29},{... | collective-permute-start | bytes 196616 | tf_op jit(solution)/shard_map/ppermute | solution.py:700
  74.9 3.5 %collective-permute-done.14.refs_5_ = bf16[128,256]{1,0:T(8,128)(2,1)S(1)} collective-permute-done((bf16[128,256]{1,0:T(8,128)(2,1)S(1)}, bf16[128,256]{1,0:T(8,128)(2,1)S(1)}, u32[]{:S(2)}, u32[]{:S(2)}) %collective-permute-start.14) | collective-permute-done | bytes 65568 | tf_op jit(solution)/shard_map/ppermute | solution.py:700
  78.4 3.6 %attend.3.refs_9_ = bf16[512,256]{1,0:T(8,128)(2,1)S(1)} custom-call(f32[4]{0:T(128)S(1)} %copy-done.16, bf16[5,256,256]{2,1,0:T(8,128)(2,1)} %get-tuple-element.35.refs_1_.refs_4_, bf16[5,384,256]{2,1,0:T(8,128)(2,1)} %get-tuple-element.37.refs_2_.refs_5_, bf16[5,384,256]{2,1,0:T(8,128)(2,1)} %get-tuple-element.38.refs_3_.refs_6_, ...), custom_call_target="tpu_custom_call" | custom-call | flops 800000000 | bytes 3145728 | tf_op jit(solution)/shard_map/attend/pallas_call | solution.py:355
  82.0 1.2 %collective-permute-start.18 = (bf16[512,256]{1,0:T(8,128)(2,1)S(1)}, bf16[512,256]{1,0:T(8,128)(2,1)S(1)}, u32[]{:S(2)}, u32[]{:S(2)}) collective-permute-start(bf16[512,256]{1,0:T(8,128)(2,1)S(1)} %attend.3.refs_9_), channel_id=1, source_target_pairs={{0,2},{1,3},{2,0},{3,1},{4,6},{5,7},{6,4},{7,5},{8,10},{9,11},{10,... | collective-permute-start | bytes 786440 | tf_op jit(solution)/shard_map/ppermute | solution.py:594
  83.3 3.6 %attend.2.refs_8_ = bf16[512,256]{1,0:T(8,128)(2,1)S(1)} custom-call(f32[4]{0:T(128)S(1)} %copy-done.16, bf16[5,256,256]{2,1,0:T(8,128)(2,1)} %get-tuple-element.35.refs_1_.refs_4_, bf16[5,384,256]{2,1,0:T(8,128)(2,1)} %get-tuple-element.37.refs_2_.refs_5_, bf16[5,384,256]{2,1,0:T(8,128)(2,1)} %get-tuple-element.38.refs_3_.refs_6_, ...), custom_call_target="tpu_custom_call" | custom-call | flops 800000000 | bytes 3145728 | tf_op jit(solution)/shard_map/attend/pallas_call | solution.py:355
  86.9 0.9 collective-permute-start.17
  88.3 1.5 %collective-permute-done.18.refs_13_ = bf16[512,256]{1,0:T(8,128)(2,1)S(1)} collective-permute-done((bf16[512,256]{1,0:T(8,128)(2,1)S(1)}, bf16[512,256]{1,0:T(8,128)(2,1)S(1)}, u32[]{:S(2)}, u32[]{:S(2)}) %collective-permute-start.18) | collective-permute-done | bytes 262176 | tf_op jit(solution)/shard_map/ppermute | solution.py:594
  89.8 6.2 %retain.1 = (bf16[512,256]{1,0:T(8,128)(2,1)S(1)}, bf16[512,256]{1,0:T(8,128)(2,1)S(1)}) custom-call(f32[1024,8]{1,0:T(8,128)} %copy-done.4, f32[8,1024]{1,0:T(8,128)} %copy-done.18, bf16[8,2,80,128]{3,2,1,0:T(8,128)(2,1)} %all-to-all-done.refs_2_, f32[2,2,64,128]{3,2,1,0:T(8,128)} %refs_3_.4, bf16[5,256,256]{2,1,0:T(8,128)(2,1)} %get-tuple-element.35.refs_1_.refs_4_, ...), custom_call_target="tpu_custom_call" | custom-call | flops 1500000000 | bytes 4194304 | tf_op jit(solution)/shard_map/retain/pallas_call | solution.py:477
  96.1 1.6 %collective-permute-start.25 = (bf16[512,256]{1,0:T(8,128)(2,1)S(1)}, bf16[512,256]{1,0:T(8,128)(2,1)S(1)}, u32[]{:S(2)}, u32[]{:S(2)}) collective-permute-start(bf16[512,256]{1,0:T(8,128)(2,1)S(1)} %get-tuple-element.45.refs_16_), channel_id=1, source_target_pairs={{0,2},{1,3},{2,0},{3,1},{4,6},{5,7},{6,4},{7,5},{8,10},{9,11},{10,... | collective-permute-start | bytes 786440 | tf_op jit(solution)/shard_map/ppermute | solution.py:594
  98.8 6.5 %collective-permute-done.25.refs_2_ = bf16[512,256]{1,0:T(8,128)(2,1)S(1)} collective-permute-done((bf16[512,256]{1,0:T(8,128)(2,1)S(1)}, bf16[512,256]{1,0:T(8,128)(2,1)S(1)}, u32[]{:S(2)}, u32[]{:S(2)}) %collective-permute-start.25) | collective-permute-done | bytes 262176 | tf_op jit(solution)/shard_map/ppermute | solution.py:594
  105.3 5.1 %collective-permute-done.23.refs_2_ = bf16[512,256]{1,0:T(8,128)(2,1)S(1)} collective-permute-done((bf16[512,256]{1,0:T(8,128)(2,1)S(1)}, bf16[512,256]{1,0:T(8,128)(2,1)S(1)}, u32[]{:S(2)}, u32[]{:S(2)}) %collective-permute-start.23) | collective-permute-done | bytes 262176 | tf_op jit(solution)/shard_map/ppermute | solution.py:594
  110.5 0.6 copy-done.25
  111.2 0.7 copy-done.27
  111.9 4.5 %most.1 = (f32[1024,512]{1,0:T(8,128)S(1)}, bf16[512,512]{1,0:T(8,128)(2,1)S(1)}) custom-call(bf16[256,2048]{1,0:T(8,128)(2,1)} %refs_0_.9, bf16[256,2048]{1,0:T(8,128)(2,1)} %refs_1_.3, bf16[256,2048]{1,0:T(8,128)(2,1)} %collective-permute-done.refs_2_, bf16[256,2048]{1,0:T(8,128)(2,1)} %collective-permute-done.1.refs_3_, ...), custom_call_target="tpu_custom_call" | custom-call | flops 1000000000 | bytes 8388608 | tf_op jit(solution)/shard_map/most/pallas_call | solution.py:531
  116.4 1.2 last.2.refs_4_
  117.6 1.2 last.3
  (93 shorter events, 4.0 us)
Async XLA Ops:
  0.0 39.4 %copy-start.19 = (bf16[256,2048]{1,0:T(8,128)(2,1)S(1)}, bf16[256,2048]{1,0:T(8,128)(2,1)}, u32[]{:S(2)}) copy-start(bf16[256,2048]{1,0:T(8,128)(2,1)} %refs_0_.9) | copy-start | bytes 3145732
  0.0 39.4 %copy-start.20 = (bf16[256,2048]{1,0:T(8,128)(2,1)S(1)}, bf16[256,2048]{1,0:T(8,128)(2,1)}, u32[]{:S(2)}) copy-start(bf16[256,2048]{1,0:T(8,128)(2,1)} %refs_1_.3) | copy-start | bytes 3145732
  0.0 42.4 %copy-start.17 = (f32[2,1024]{1,0:T(2,128)S(1)}, f32[2,1024]{1,0:T(2,128)}, u32[]{:S(2)}) copy-start(f32[2,1024]{1,0:T(2,128)} %log_ref.1) | copy-start | bytes 24580
  0.0 41.9 %collective-permute-start.6 = (bf16[1024,512]{1,0:T(8,128)(2,1)}, bf16[1024,512]{1,0:T(8,128)(2,1)S(1)}, u32[]{:S(2)}, u32[]{:S(2)}) collective-permute-start(bf16[1024,512]{1,0:T(8,128)(2,1)} %refs_6_.5), channel_id=1, source_target_pairs={{0,1},{1,0},{2,3},{3,2},{4,5},{5,4},{6,7},{7,6},{8,9},{9,8},{10,11... | collective-permute-start | bytes 3145736 | tf_op jit(solution)/shard_map/ppermute | solution.py:589
  1.9 12.6 %collective-permute-start.9 = (bf16[384,512]{1,0:T(8,128)(2,1)S(1)}, bf16[384,512]{1,0:T(8,128)(2,1)S(1)}, u32[]{:S(2)}, u32[]{:S(2)}) collective-permute-start(bf16[384,512]{1,0:T(8,128)(2,1)S(1)} %get-tuple-element.33), channel_id=1, source_target_pairs={{0,2},{1,3},{2,0},{3,1},{4,6},{5,7},{6,4},{7,5},{8,10},{9,11},{10,... | collective-permute-start | bytes 1179656 | tf_op jit(solution)/shard_map/ppermute | solution.py:594
  5.7 34.2 %collective-permute-start.2 = (bf16[256,1024]{1,0:T(8,128)(2,1)S(1)}, bf16[256,1024]{1,0:T(8,128)(2,1)}, u32[]{:S(2)}, u32[]{:S(2)}) collective-permute-start(bf16[256,1024]{1,0:T(8,128)(2,1)S(1)} %get-tuple-element.27), channel_id=1, source_target_pairs={{0,2},{1,3},{2,0},{3,1},{4,6},{5,7},{6,4},{7,5},{8,10},{9,11},{10,... | collective-permute-start | bytes 1572872 | tf_op jit(solution)/shard_map/ppermute | solution.py:594
  5.8 33.6 %collective-permute-start.11 = (bf16[384,512]{1,0:T(8,128)(2,1)S(1)}, bf16[384,512]{1,0:T(8,128)(2,1)S(1)}, u32[]{:S(2)}, u32[]{:S(2)}) collective-permute-start(bf16[384,512]{1,0:T(8,128)(2,1)S(1)} %get-tuple-element.36), channel_id=1, source_target_pairs={{0,2},{1,3},{2,0},{3,1},{4,6},{5,7},{6,4},{7,5},{8,10},{9,11},{10,... | collective-permute-start | bytes 1179656 | tf_op jit(solution)/shard_map/ppermute | solution.py:594
  14.5 27.4 %collective-permute-start.10 = (bf16[384,512]{1,0:T(8,128)(2,1)S(1)}, bf16[384,512]{1,0:T(8,128)(2,1)S(1)}, u32[]{:S(2)}, u32[]{:S(2)}) collective-permute-start(bf16[384,512]{1,0:T(8,128)(2,1)S(1)} %collective-permute-done.9.refs_8_), channel_id=1, source_target_pairs={{0,1},{1,0},{2,3},{3,2},{4,5},{5,4},{6,7},{7,6},{8,9},{9,8},{10,11... | collective-permute-start | bytes 1179656 | tf_op jit(solution)/shard_map/ppermute | solution.py:589
  14.5 25.0 %collective-permute-start.7 = (bf16[256,512]{1,0:T(8,128)(2,1)S(1)}, bf16[256,512]{1,0:T(8,128)(2,1)S(1)}, u32[]{:S(2)}, u32[]{:S(2)}) collective-permute-start(bf16[256,512]{1,0:T(8,128)(2,1)S(1)} %get-tuple-element.32), channel_id=1, source_target_pairs={{0,2},{1,3},{2,0},{3,1},{4,6},{5,7},{6,4},{7,5},{8,10},{9,11},{10,... | collective-permute-start | bytes 786440 | tf_op jit(solution)/shard_map/ppermute | solution.py:594
  39.4 48.4 %collective-permute-start = (bf16[256,2048]{1,0:T(8,128)(2,1)S(1)}, bf16[256,2048]{1,0:T(8,128)(2,1)}, u32[]{:S(2)}, u32[]{:S(2)}) collective-permute-start(bf16[256,2048]{1,0:T(8,128)(2,1)S(1)} %copy-done.19), channel_id=1, source_target_pairs={{0,1},{1,0},{2,3},{3,2},{4,5},{5,4},{6,7},{7,6},{8,9},{9,8},{10,11... | collective-permute-start | bytes 3145736 | tf_op jit(solution)/shard_map/ppermute | solution.py:589
  39.5 56.6 %collective-permute-start.1 = (bf16[256,2048]{1,0:T(8,128)(2,1)S(1)}, bf16[256,2048]{1,0:T(8,128)(2,1)}, u32[]{:S(2)}, u32[]{:S(2)}) collective-permute-start(bf16[256,2048]{1,0:T(8,128)(2,1)S(1)} %copy-done.20), channel_id=1, source_target_pairs={{0,1},{1,0},{2,3},{3,2},{4,5},{5,4},{6,7},{7,6},{8,9},{9,8},{10,11... | collective-permute-start | bytes 3145736 | tf_op jit(solution)/shard_map/ppermute | solution.py:589
  40.1 24.6 %collective-permute-start.4 = (bf16[256,1024]{1,0:T(8,128)(2,1)S(1)}, bf16[256,1024]{1,0:T(8,128)(2,1)}, u32[]{:S(2)}, u32[]{:S(2)}) collective-permute-start(bf16[256,1024]{1,0:T(8,128)(2,1)S(1)} %get-tuple-element.28), channel_id=1, source_target_pairs={{0,2},{1,3},{2,0},{3,1},{4,6},{5,7},{6,4},{7,5},{8,10},{9,11},{10,... | collective-permute-start | bytes 1572872 | tf_op jit(solution)/shard_map/ppermute | solution.py:594
  41.9 12.5 %collective-permute-start.8 = (bf16[256,512]{1,0:T(8,128)(2,1)S(1)}, bf16[256,512]{1,0:T(8,128)(2,1)S(1)}, u32[]{:S(2)}, u32[]{:S(2)}) collective-permute-start(bf16[256,512]{1,0:T(8,128)(2,1)S(1)} %collective-permute-done.7.refs_8_), channel_id=1, source_target_pairs={{0,1},{1,0},{2,3},{3,2},{4,5},{5,4},{6,7},{7,6},{8,9},{9,8},{10,11... | collective-permute-start | bytes 786440 | tf_op jit(solution)/shard_map/ppermute | solution.py:589
  41.9 6.9 %collective-permute-start.12 = (bf16[384,512]{1,0:T(8,128)(2,1)S(1)}, bf16[384,512]{1,0:T(8,128)(2,1)S(1)}, u32[]{:S(2)}, u32[]{:S(2)}) collective-permute-start(bf16[384,512]{1,0:T(8,128)(2,1)S(1)} %collective-permute-done.11.refs_8_), channel_id=1, source_target_pairs={{0,1},{1,0},{2,3},{3,2},{4,5},{5,4},{6,7},{7,6},{8,9},{9,8},{10,11... | collective-permute-start | bytes 1179656 | tf_op jit(solution)/shard_map/ppermute | solution.py:589
  48.8 38.2 %collective-permute-start.3 = (bf16[256,1024]{1,0:T(8,128)(2,1)}, bf16[256,1024]{1,0:T(8,128)(2,1)}, u32[]{:S(2)}, u32[]{:S(2)}) collective-permute-start(bf16[256,1024]{1,0:T(8,128)(2,1)} %collective-permute-done.2.refs_4_), channel_id=1, source_target_pairs={{0,1},{1,0},{2,3},{3,2},{4,5},{5,4},{6,7},{7,6},{8,9},{9,8},{10,11... | collective-permute-start | bytes 1572872 | tf_op jit(solution)/shard_map/ppermute | solution.py:589
  54.4 24.1 %copy-start.16 = (f32[4]{0:T(128)S(1)}, f32[4]{0:T(128)}, u32[]{:S(2)}) copy-start(f32[4]{0:T(128)} %refs_0_.8) | copy-start | bytes 52
  58.9 31.0 %all-to-all-start = ((bf16[8,2,80,128]{3,2,1,0:T(8,128)(2,1)}), bf16[8,2,80,128]{3,2,1,0:T(8,128)(2,1)}, u32[]{:S(2)}, u32[]{:S(2)}) async-start(bf16[8,2,80,128]{3,2,1,0:T(8,128)(2,1)} %totals.1), calls=%async_computation | async-start | bytes 655360 | tf_op jit(solution)/shard_map/all_to_all | solution.py:702
  64.7 23.2 %collective-permute-start.5 = (bf16[256,1024]{1,0:T(8,128)(2,1)}, bf16[256,1024]{1,0:T(8,128)(2,1)S(1)}, u32[]{:S(2)}, u32[]{:S(2)}) collective-permute-start(bf16[256,1024]{1,0:T(8,128)(2,1)} %collective-permute-done.4.refs_6_), channel_id=1, source_target_pairs={{0,1},{1,0},{2,3},{3,2},{4,5},{5,4},{6,7},{7,6},{8,9},{9,8},{10,11... | collective-permute-start | bytes 1572872 | tf_op jit(solution)/shard_map/ppermute | solution.py:589
  64.9 6.6 %collective-permute-start.13 = (bf16[128,256]{1,0:T(8,128)(2,1)S(1)}, bf16[128,256]{1,0:T(8,128)(2,1)S(1)}, u32[]{:S(2)}, u32[]{:S(2)}) collective-permute-start(bf16[128,256]{1,0:T(8,128)(2,1)S(1)} %get-tuple-element.39), channel_id=1, source_target_pairs={{0,4},{4,0},{8,12},{12,8},{16,20},{20,16},{24,28},{28,24},{1,5},{5... | collective-permute-start | bytes 196616 | tf_op jit(solution)/shard_map/ppermute | solution.py:698
  71.5 7.0 %collective-permute-start.14 = (bf16[128,256]{1,0:T(8,128)(2,1)S(1)}, bf16[128,256]{1,0:T(8,128)(2,1)S(1)}, u32[]{:S(2)}, u32[]{:S(2)}) collective-permute-start(bf16[128,256]{1,0:T(8,128)(2,1)S(1)} %get-tuple-element.40), channel_id=1, source_target_pairs={{0,28},{4,8},{8,4},{12,16},{16,12},{20,24},{24,20},{28,0},{1,29},{... | collective-permute-start | bytes 196616 | tf_op jit(solution)/shard_map/ppermute | solution.py:700
  82.0 7.8 %collective-permute-start.18 = (bf16[512,256]{1,0:T(8,128)(2,1)S(1)}, bf16[512,256]{1,0:T(8,128)(2,1)S(1)}, u32[]{:S(2)}, u32[]{:S(2)}) collective-permute-start(bf16[512,256]{1,0:T(8,128)(2,1)S(1)} %attend.3.refs_9_), channel_id=1, source_target_pairs={{0,2},{1,3},{2,0},{3,1},{4,6},{5,7},{6,4},{7,5},{8,10},{9,11},{10,... | collective-permute-start | bytes 786440 | tf_op jit(solution)/shard_map/ppermute | solution.py:594
  86.9 10.8 %collective-permute-start.17 = (bf16[512,256]{1,0:T(8,128)(2,1)S(1)}, bf16[512,256]{1,0:T(8,128)(2,1)}, u32[]{:S(2)}, u32[]{:S(2)}) collective-permute-start(bf16[512,256]{1,0:T(8,128)(2,1)S(1)} %attend.2.refs_8_), channel_id=1, source_target_pairs={{0,2},{1,3},{2,0},{3,1},{4,6},{5,7},{6,4},{7,5},{8,10},{9,11},{10,... | collective-permute-start | bytes 786440 | tf_op jit(solution)/shard_map/ppermute | solution.py:594
  87.8 10.3 %collective-permute-start.16 = (bf16[512,256]{1,0:T(8,128)(2,1)S(1)}, bf16[512,256]{1,0:T(8,128)(2,1)}, u32[]{:S(2)}, u32[]{:S(2)}) collective-permute-start(bf16[512,256]{1,0:T(8,128)(2,1)S(1)} %attend.3.refs_9_), channel_id=1, source_target_pairs={{0,1},{1,0},{2,3},{3,2},{4,5},{5,4},{6,7},{7,6},{8,9},{9,8},{10,11... | collective-permute-start | bytes 786440 | tf_op jit(solution)/shard_map/ppermute | solution.py:589
  87.8 10.3 %collective-permute-start.15 = (bf16[512,256]{1,0:T(8,128)(2,1)S(1)}, bf16[512,256]{1,0:T(8,128)(2,1)S(1)}, u32[]{:S(2)}, u32[]{:S(2)}) collective-permute-start(bf16[512,256]{1,0:T(8,128)(2,1)S(1)} %attend.2.refs_8_), channel_id=1, source_target_pairs={{0,1},{1,0},{2,3},{3,2},{4,5},{5,4},{6,7},{7,6},{8,9},{9,8},{10,11... | collective-permute-start | bytes 786440 | tf_op jit(solution)/shard_map/ppermute | solution.py:589
  89.8 8.9 %collective-permute-start.20 = (bf16[512,256]{1,0:T(8,128)(2,1)S(1)}, bf16[512,256]{1,0:T(8,128)(2,1)S(1)}, u32[]{:S(2)}, u32[]{:S(2)}) collective-permute-start(bf16[512,256]{1,0:T(8,128)(2,1)S(1)} %collective-permute-done.18.refs_13_), channel_id=1, source_target_pairs={{0,1},{1,0},{2,3},{3,2},{4,5},{5,4},{6,7},{7,6},{8,9},{9,8},{10,11... | collective-permute-start | bytes 786440 | tf_op jit(solution)/shard_map/ppermute | solution.py:589
  96.1 9.2 %collective-permute-start.25 = (bf16[512,256]{1,0:T(8,128)(2,1)S(1)}, bf16[512,256]{1,0:T(8,128)(2,1)S(1)}, u32[]{:S(2)}, u32[]{:S(2)}) collective-permute-start(bf16[512,256]{1,0:T(8,128)(2,1)S(1)} %get-tuple-element.45.refs_16_), channel_id=1, source_target_pairs={{0,2},{1,3},{2,0},{3,1},{4,6},{5,7},{6,4},{7,5},{8,10},{9,11},{10,... | collective-permute-start | bytes 786440 | tf_op jit(solution)/shard_map/ppermute | solution.py:594
  97.7 12.7 %collective-permute-start.23 = (bf16[512,256]{1,0:T(8,128)(2,1)S(1)}, bf16[512,256]{1,0:T(8,128)(2,1)S(1)}, u32[]{:S(2)}, u32[]{:S(2)}) collective-permute-start(bf16[512,256]{1,0:T(8,128)(2,1)S(1)} %get-tuple-element.46.refs_17_), channel_id=1, source_target_pairs={{0,2},{1,3},{2,0},{3,1},{4,6},{5,7},{6,4},{7,5},{8,10},{9,11},{10,... | collective-permute-start | bytes 786440 | tf_op jit(solution)/shard_map/ppermute | solution.py:594
  98.2 12.2 %collective-permute-start.19 = (bf16[512,256]{1,0:T(8,128)(2,1)}, bf16[512,256]{1,0:T(8,128)(2,1)S(1)}, u32[]{:S(2)}, u32[]{:S(2)}) collective-permute-start(bf16[512,256]{1,0:T(8,128)(2,1)} %collective-permute-done.17.refs_12_), channel_id=1, source_target_pairs={{0,1},{1,0},{2,3},{3,2},{4,5},{5,4},{6,7},{7,6},{8,9},{9,8},{10,11... | collective-permute-start | bytes 786440 | tf_op jit(solution)/shard_map/ppermute | solution.py:589
  98.2 12.2 %collective-permute-start.21 = (bf16[512,256]{1,0:T(8,128)(2,1)S(1)}, bf16[512,256]{1,0:T(8,128)(2,1)S(1)}, u32[]{:S(2)}, u32[]{:S(2)}) collective-permute-start(bf16[512,256]{1,0:T(8,128)(2,1)S(1)} %get-tuple-element.45.refs_16_), channel_id=1, source_target_pairs={{0,1},{1,0},{2,3},{3,2},{4,5},{5,4},{6,7},{7,6},{8,9},{9,8},{10,11... | collective-permute-start | bytes 786440 | tf_op jit(solution)/shard_map/ppermute | solution.py:589
  98.7 11.7 %collective-permute-start.22 = (bf16[512,256]{1,0:T(8,128)(2,1)S(1)}, bf16[512,256]{1,0:T(8,128)(2,1)S(1)}, u32[]{:S(2)}, u32[]{:S(2)}) collective-permute-start(bf16[512,256]{1,0:T(8,128)(2,1)S(1)} %get-tuple-element.46.refs_17_), channel_id=1, source_target_pairs={{0,1},{1,0},{2,3},{3,2},{4,5},{5,4},{6,7},{7,6},{8,9},{9,8},{10,11... | collective-permute-start | bytes 786440 | tf_op jit(solution)/shard_map/ppermute | solution.py:589
  105.3 11.1 %collective-permute-start.26 = (bf16[512,256]{1,0:T(8,128)(2,1)S(1)}, bf16[512,256]{1,0:T(8,128)(2,1)S(1)}, u32[]{:S(2)}, u32[]{:S(2)}) collective-permute-start(bf16[512,256]{1,0:T(8,128)(2,1)S(1)} %collective-permute-done.25.refs_2_), channel_id=1, source_target_pairs={{0,1},{1,0},{2,3},{3,2},{4,5},{5,4},{6,7},{7,6},{8,9},{9,8},{10,11... | collective-permute-start | bytes 786440 | tf_op jit(solution)/shard_map/ppermute | solution.py:589
  110.4 7.2 %collective-permute-start.24 = (bf16[512,256]{1,0:T(8,128)(2,1)S(1)}, bf16[512,256]{1,0:T(8,128)(2,1)S(1)}, u32[]{:S(2)}, u32[]{:S(2)}) collective-permute-start(bf16[512,256]{1,0:T(8,128)(2,1)S(1)} %collective-permute-done.23.refs_2_), channel_id=1, source_target_pairs={{0,1},{1,0},{2,3},{3,2},{4,5},{5,4},{6,7},{7,6},{8,9},{9,8},{10,11... | collective-permute-start | bytes 786440 | tf_op jit(solution)/shard_map/ppermute | solution.py:589
  (24 other events, 148.6 us)

commit v5 on v4

--- a/solution.py
+++ b/solution.py
@@ -18,8 +18,7 @@
 ROPE_BASE = 10000.0
 NEG = -1e30
 EXTRA = 16
-CHUNKS = ((0, 2), (2, 3), (5, 3))
-ORDER = (2, 0, 1)
+CHUNKS = ((0, 7), (1, 2, 3), (4, 5, 6))
 TABLE = 32
 HALVES = 2
 F32 = jnp.float32
@@ -53,6 +52,17 @@
 
 def in_hbm(values):
     return [pltpu.with_memory_space_constraint(v, pltpu.HBM) for v in values]
+
+
+def runs():
+    out = []
+    for c, eighths in enumerate(CHUNKS):
+        for i, e in enumerate(eighths):
+            if out and out[-1][0] == c and out[-1][2] + out[-1][3] == e:
+                out[-1][3] += 1
+            else:
+                out.append([c, i, e, 1])
+    return sorted(out, key=lambda run: run[2])
 
 
 class Copies:
@@ -98,24 +108,24 @@
     )(*in_hbm([att, ret]))
 
 
-def split_kernel(chunks, *refs):
-    tokens = refs[0]
-    pieces = refs[1 : 1 + len(chunks)]
-    copies = Copies(refs[-1])
-    for (first, _), piece in zip(chunks, pieces):
-        rows = pl.ds(first * tokens.shape[0] // 8, piece.shape[0])
-        copies.start(tokens.at[rows], piece)
+def split_kernel(*refs):
+    tokens, sems = refs[0], refs[-1]
+    copies = Copies(sems)
+    size = tokens.shape[0] // 8
+    for c, inner, first, count in runs():
+        dst = refs[1 + c].at[pl.ds(inner * size, count * size)]
+        copies.start(tokens.at[pl.ds(first * size, count * size)], dst)
     copies.wait()
 
 
-def split(tokens, chunks):
+def split(tokens):
     total, cols = tokens.shape
     return pl.pallas_call(
-        functools.partial(split_kernel, chunks),
-        out_shape=tuple(jax.ShapeDtypeStruct((n * total // 8, cols), BF16) for _, n in chunks),
+        split_kernel,
+        out_shape=tuple(jax.ShapeDtypeStruct((len(e) * total // 8, cols), BF16) for e in CHUNKS),
         in_specs=[HBM],
-        out_specs=(VMEM,) * len(chunks),
-        scratch_shapes=[pltpu.SemaphoreType.DMA((len(chunks),))],
+        out_specs=(VMEM,) * len(CHUNKS),
+        scratch_shapes=[pltpu.SemaphoreType.DMA((len(runs()),))],
         cost_estimate=cost(0.1e9, 3 << 20),
         compiler_params=PARAMS,
         name="split",
@@ -164,13 +174,12 @@
     )(log, *weights)
 
 
-def project_kernel(n_blocks, n_w, n_other, parts, first, ret_local, *refs):
+def project_kernel(n_blocks, n_w, parts, eighths, ret_local, *refs):
     gain_ref, ccol_ref, swap_ref, mix_ref, cos_ref, sin_ref = refs[:6]
     blocks = refs[6 : 6 + n_blocks]
     w_refs = refs[6 + n_blocks : 6 + n_blocks + n_w]
-    other_refs = refs[6 + n_blocks + n_w : 6 + n_blocks + n_w + n_other]
-    at_out = 6 + n_blocks + n_w + n_other
-    out_ref, sum_ref, low_ref, high_ref = refs[at_out : at_out + 4]
+    out_ref, sum_ref = refs[6 + n_blocks + n_w : 8 + n_blocks + n_w]
+    edge_refs = refs[8 + n_blocks + n_w : -4]
     xn, inv, held, sems = refs[-4:]
     copies = Copies(sems)
     width = blocks[0].shape[1]
@@ -178,15 +187,14 @@
     group_width = inv.shape[1]
     half = group_width // 2
     total = ccol_ref.shape[0]
-    mine = pl.ds(first, rows)
     starts = [pl.multiple_of(i * width, width) for i in sources()]
-    tile = min(128, rows)
+    tile = total // 8
     lanes = min(128, width)
-    for r in range(rows // tile):
+    for r, eighth in enumerate(eighths):
         here = pl.ds(r * tile, tile)
         squares = jnp.zeros((tile, lanes), F32)
         for start, block in zip(starts, blocks):
-            at = here if block.shape[0] == rows else pl.ds(first + r * tile, tile)
+            at = here if block.shape[0] == rows else pl.ds(eighth * tile, tile)
             for low in range(0, width, lanes):
                 part = block[at, low : low + lanes].astype(F32)
                 squares = squares + part * part
@@ -197,7 +205,7 @@
     count = total // TABLE
     cos_b, sin_b = cos_ref[count:], sin_ref[count:]
     cosines, sines = [], []
-    for k in range(first // TABLE, (first + rows) // TABLE):
+    for k in [e * tile // TABLE + i for e in eighths for i in range(tile // TABLE)]:
         cos_k, sin_k = cos_ref[k : k + 1], sin_ref[k : k + 1]
         cosines.append(cos_k * cos_b - sin_k * sin_b)
         sines.append(sin_k * cos_b + cos_k * sin_b)
@@ -219,37 +227,36 @@
             raw = jnp.concatenate(sides, axis=1)
         if group == 3:
             for h in range(ret_local):
-                col = ccol_ref[mine, h : h + 1]
+                col = [ccol_ref[e * tile : (e + 1) * tile, h : h + 1] for e in eighths]
+                col = jnp.concatenate(col, axis=0)
                 end = ccol_ref[total - 1 : total, h : h + 1]
                 v = raw[:, h * RV : (h + 1) * RV].astype(F32)
                 both = jnp.concatenate([v * jnp.exp(end - col), v * jnp.exp(col)], axis=1)
                 sum_ref[h] = t_dot(keys, both.astype(BF16))[h * RK : (h + 1) * RK]
-        if group == 1:
-            low_ref[...] = raw[rows - WINDOW :]
-            high_ref[...] = raw[:WINDOW]
-            for other in other_refs:
-                even = lax.rem(lax.axis_index("sp"), 2) == 0
-                low_ref[...] = jnp.where(even, other[...], raw[:WINDOW])
-                high_ref[...] = jnp.where(even, raw[:WINDOW], other[...])
+        if group == 1 and edge_refs:
+            even = lax.rem(lax.axis_index("sp"), 2) == 0
+            edge_refs[0][...] = jnp.where(even, raw[rows - WINDOW :], raw[:WINDOW])
+            edge_refs[1][...] = jnp.where(even, raw[:WINDOW], raw[rows - WINDOW :])
         held[group] = raw
         copies.start(held.at[group], out_ref.at[group])
     copies.wait()
 
 
-def project(gain, ccol, swap, mix, cos, sin, blocks, weights, parts, first, rows, ret_local, other):
+def project(gain, ccol, swap, mix, cos, sin, blocks, weights, parts, eighths, ret_local):
     width = mix.shape[0]
     depth = gain.shape[1]
     n = len(blocks)
-    return pl.pallas_call(
-        functools.partial(project_kernel, n, len(weights), len(other), parts, first, ret_local),
+    rows = len(eighths) * ccol.shape[0] // 8
+    n_edges = 2 if eighths[0] == 0 and eighths[-1] == 7 else 0
+    return pl.pallas_call(
+        functools.partial(project_kernel, n, len(weights), parts, eighths, ret_local),
         out_shape=(
             pltpu.HBM((5, rows, width), BF16),
             pltpu.VMEM((ret_local, RK, 2 * RV), F32),
-            jax.ShapeDtypeStruct((WINDOW, width), BF16),
-            jax.ShapeDtypeStruct((WINDOW, width), BF16),
+            *[jax.ShapeDtypeStruct((WINDOW, width), BF16)] * n_edges,
         ),
-        in_specs=[VMEM] * (n + 6 + len(weights) + len(other)),
-        out_specs=(HBM, VMEM, VMEM, VMEM),
+        in_specs=[VMEM] * (n + 6 + len(weights)),
+        out_specs=(HBM, VMEM) + (VMEM,) * n_edges,
         scratch_shapes=[
             pltpu.VMEM((rows, depth), BF16),
             pltpu.VMEM((rows, width), F32),
@@ -259,7 +266,7 @@
         cost_estimate=cost(2 * rows * depth * 5 * width // 4, 7 << 20),
         compiler_params=PARAMS,
         name="project",
-    )(gain, ccol, swap, mix, cos, sin, *blocks, *weights, *other)
+    )(gain, ccol, swap, mix, cos, sin, *blocks, *weights)
 
 
 def overlaps(sizes, first, rows):
@@ -284,18 +291,24 @@
     kv_cols = kv_local * HD
     block = WINDOW
     span = block + 2 * WINDOW
-    sizes = [WINDOW] + [ref.shape[1] for ref in proj] + [WINDOW]
+    size = total // 8
+    order = runs()
+    sizes = [WINDOW] + [run[3] * size for run in order] + [WINDOW]
     for i, low, count, to in overlaps(sizes, start, rows + 2 * WINDOW):
-        if i in (0, n_chunks + 1):
+        if i in (0, len(order) + 1):
             even = lax.rem(lax.axis_index("sp"), 2) == 0
             here = pl.ds(low, count)
             near, far = (high_ref, low_ref) if i == 0 else (low_ref, high_ref)
             kvbuf[pl.ds(to, count)] = jnp.where(even, near[here], far[here])
         else:
-            copies.start(proj[i - 1].at[1, pl.ds(low, count)], kvbuf.at[pl.ds(to, count)])
+            c, inner = order[i - 1][:2]
+            src = proj[c].at[1, pl.ds(inner * size + low, count)]
+            copies.start(src, kvbuf.at[pl.ds(to, count)])
     n_kv = len(copies.copies)
     for i, low, count, to in overlaps(sizes[1:-1], start, rows):
-        copies.start(proj[i].at[0, pl.ds(low, count)], qbuf.at[pl.ds(to, count)])
+        c, inner = order[i][:2]
+        src = proj[c].at[0, pl.ds(inner * size + low, count)]
+        copies.start(src, qbuf.at[pl.ds(to, count)])
     vbuf[kv_cols:] = jnp.ones((vbuf.shape[0] - kv_cols, vbuf.shape[1]), BF16)
     row = lax.broadcasted_iota(jnp.int32, (span, block), 1)
     col = lax.broadcasted_iota(jnp.int32, (span, block), 0)
@@ -362,7 +375,7 @@
             pltpu.VMEM((rows + 2 * WINDOW, 2 * kv_cols), BF16),
             pltpu.VMEM((kv_cols + 16, rows + 2 * WINDOW), BF16),
             pltpu.VMEM((3, 3 * WINDOW, groups * WINDOW), F32),
-            pltpu.SemaphoreType.DMA((2 * n + 2,)),
+            pltpu.SemaphoreType.DMA((2 * len(runs()),)),
         ],
         cost_estimate=cost(0.8e9, 3 << 20),
         compiler_params=PARAMS,
@@ -419,11 +432,11 @@
     copies.start(init_hbm, init_ref)
     copies.start(ccol_hbm, ccol_ref)
     copies.start(crow_hbm, crow_ref)
+    size = total // 8
     for group, buf in ((2, rbuf), (3, vbuf), (4, gbuf)):
-        at = 0
-        for ref in proj:
-            copies.start(ref.at[group], buf.at[pl.ds(at, ref.shape[1])])
-            at += ref.shape[1]
+        for c, inner, first, count in runs():
+            src = proj[c].at[group, pl.ds(inner * size, count * size)]
+            copies.start(src, buf.at[pl.ds(first * size, count * size)])
     copies.wait(0, 2)
     states[...] = jnp.zeros(states.shape, BF16)
     for h in range(ret_local):
@@ -488,7 +501,7 @@
             pltpu.VMEM((total, width), BF16),
             pltpu.VMEM((total, width), BF16),
             pltpu.VMEM((total, width), BF16),
-            pltpu.SemaphoreType.DMA((3 * n + 4,)),
+            pltpu.SemaphoreType.DMA((3 * len(runs()) + 4,)),
         ],
         cost_estimate=cost(1.5e9, 4 << 20),
         compiler_params=PARAMS,
@@ -649,10 +662,10 @@
     cols = tokens.shape[1]
 
     slabs = slab(out_att, out_ret, cols)
-    pieces = split(tokens, CHUNKS)
+    pieces = split(tokens)
     near = core_swap(tokens)
     far = {}
-    for c in ORDER:
+    for c in range(len(CHUNKS)):
         far[c] = []
         for by in range(1, lax.axis_size("tp") // 2):
             block = chip_turn(pieces[c], by)
@@ -687,17 +700,17 @@
     out_w = output_weights(out_att, out_ret, slabs)
     proj = [None] * len(CHUNKS)
     sums = [None] * len(CHUNKS)
-    edges = [None] * len(CHUNKS)
-    for c in ORDER:
-        first, rows = CHUNKS[c][0] * total // 8, CHUNKS[c][1] * total // 8
-        proj[c], sums[c], *edges[c] = project(
+    edges = []
+    for c, eighths in enumerate(CHUNKS):
+        proj[c], sums[c], *found = project(
             gain, ccol, swap, mix, cos, sin, [tokens, near] + far[c], weights, parts,
-            first, rows, ret_local, [edges[-1][0]] if c == 0 else [],
+            eighths, ret_local,
         )
-
-    edge0 = lax.ppermute(edges[0][0], "sp", [(i, i ^ 1) for i in range(n_sp)])
+        edges += found
+
+    edge0 = lax.ppermute(edges[0], "sp", [(i, i ^ 1) for i in range(n_sp)])
     turn = [(i, (((i + 1) ^ 1) + n_sp - 1) % n_sp) for i in range(n_sp)]
-    edge1 = lax.ppermute(edges[0][1], "sp", turn)
+    edge1 = lax.ppermute(edges[1], "sp", turn)
     sent = totals(ccol, sums, n_sp)
     got = lax.all_to_all(sent, "sp", 0, 0, tiled=True)
     part = total // HALVES

time: 119 us -> 118 us (level)
  Pallas kernels: 38.7 us -> 37.4 us
    pallas_call x4, Pallas kernels: 15.8 us -> 14.5 us  [the longest x3 13.2 us: project(): pl.pallas_call(functools.partial(project_kernel, n, len(weights), parts,...]
  transfers between devices with their start and end apart: 28 -> 28, of which waited for: 7 -> 7; matrix products, arithmetic and copies ran while one was open for 0% -> 0% of each run, Pallas kernels for 32% -> 31%
where the time goes in v5:
time: 118 us
  waiting for transfers between devices  51 us (43%)
  Pallas kernels  37.4 us (32%)
  starting transfers between devices  26.9 us (23%)
  local copies, waits for them, and re-layouts  1.61 us (1%)
    ppermute x9, waiting for transfers between devices, chip_turn(): return lax.ppermute(value, 'tp', [(i, (i + 2 * by) % n) for i in range(n)])  42.7 us
    pallas_call x3, Pallas kernels, project(): pl.pallas_call(functools.partial(project_kernel, n, len(weights), parts,...  13.2 us
    ppermute x9, starting transfers between devices, chip_turn(): return lax.ppermute(value, 'tp', [(i, (i + 2 * by) % n) for i in range(n)])  12.8 us
    pallas_call x2, Pallas kernels, attend(): pl.pallas_call(functools.partial(attend_kernel, n, kv_local, groups, seq_...  7.14 us
    pallas_call x1, Pallas kernels, retain(): pl.pallas_call(functools.partial(retain_kernel, n, ret_local, n_sp), out_...  6.18 us
    all_to_all x1, starting transfers between devices, body(): got = lax.all_to_all(sent, 'sp', 0, 0, tiled=True)  5.81 us
    ppermute x1, waiting for transfers between devices, body(): edge0 = lax.ppermute(edges[0], 'sp', [(i, i ^ 1) for i in range(n_sp)])  4.73 us
    pallas_call x1, Pallas kernels, most(): pl.pallas_call(functools.partial(most_kernel, n_far, n), out_shape=(pltpu...  4.47 us
  transfers between devices with their start and end apart: 28, of which 7 were waited for; matrix products, arithmetic and copies ran while one was open for 0% of the time, Pallas kernels for 31%

profile of v5, /device:TPU:0, one launch (start us, length us, event | category | flops | bytes accessed | tf_op | source)
XLA Modules:
  0.0 117.6 jit_solution(5055155469553230676)
XLA Ops:
  0.6 1.3 %split.1 = (bf16[256,512]{1,0:T(8,128)(2,1)S(1)}, bf16[384,512]{1,0:T(8,128)(2,1)S(1)}, bf16[384,512]{1,0:T(8,128)(2,1)S(1)}) custom-call(bf16[1024,512]{1,0:T(8,128)(2,1)} %refs_6_.5), custom_call_target="tpu_custom_call" | custom-call | flops 100000000 | bytes 3145728 | tf_op jit(solution)/shard_map/split/pallas_call | solution.py:123
  1.9 2.6 %collective-permute-start.9 = (bf16[384,512]{1,0:T(8,128)(2,1)S(1)}, bf16[384,512]{1,0:T(8,128)(2,1)S(1)}, u32[]{:S(2)}, u32[]{:S(2)}) collective-permute-start(bf16[384,512]{1,0:T(8,128)(2,1)S(1)} %get-tuple-element.33), channel_id=1, source_target_pairs={{0,2},{1,3},{2,0},{3,1},{4,6},{5,7},{6,4},{7,5},{8,10},{9,11},{10,... | collective-permute-start | bytes 1179656 | tf_op jit(solution)/shard_map/ppermute | solution.py:607
  4.5 1.2 %slab.1 = (bf16[256,1024]{1,0:T(8,128)(2,1)S(1)}, bf16[256,1024]{1,0:T(8,128)(2,1)S(1)}) custom-call(bf16[256,2048]{1,0:T(8,128)(2,1)} %refs_0_.9, bf16[256,2048]{1,0:T(8,128)(2,1)} %refs_1_.3), custom_call_target="tpu_custom_call" | custom-call | flops 100000000 | bytes 3145728 | tf_op jit(solution)/shard_map/slab/pallas_call | solution.py:99
  5.9 2.0 %collective-permute-start.11 = (bf16[384,512]{1,0:T(8,128)(2,1)S(1)}, bf16[384,512]{1,0:T(8,128)(2,1)S(1)}, u32[]{:S(2)}, u32[]{:S(2)}) collective-permute-start(bf16[384,512]{1,0:T(8,128)(2,1)S(1)} %get-tuple-element.35), channel_id=1, source_target_pairs={{0,2},{1,3},{2,0},{3,1},{4,6},{5,7},{6,4},{7,5},{8,10},{9,11},{10,... | collective-permute-start | bytes 1179656 | tf_op jit(solution)/shard_map/ppermute | solution.py:607
  7.8 6.7 %collective-permute-done.9.refs_8_ = bf16[384,512]{1,0:T(8,128)(2,1)S(1)} collective-permute-done((bf16[384,512]{1,0:T(8,128)(2,1)S(1)}, bf16[384,512]{1,0:T(8,128)(2,1)S(1)}, u32[]{:S(2)}, u32[]{:S(2)}) %collective-permute-start.9) | collective-permute-done | bytes 393248 | tf_op jit(solution)/shard_map/ppermute | solution.py:607
  14.5 2.0 %collective-permute-start.7 = (bf16[256,512]{1,0:T(8,128)(2,1)S(1)}, bf16[256,512]{1,0:T(8,128)(2,1)S(1)}, u32[]{:S(2)}, u32[]{:S(2)}) collective-permute-start(bf16[256,512]{1,0:T(8,128)(2,1)S(1)} %get-tuple-element.31), channel_id=1, source_target_pairs={{0,2},{1,3},{2,0},{3,1},{4,6},{5,7},{6,4},{7,5},{8,10},{9,11},{10,... | collective-permute-start | bytes 786440 | tf_op jit(solution)/shard_map/ppermute | solution.py:607
  16.5 22.9 %collective-permute-done.7.refs_8_ = bf16[256,512]{1,0:T(8,128)(2,1)S(1)} collective-permute-done((bf16[256,512]{1,0:T(8,128)(2,1)S(1)}, bf16[256,512]{1,0:T(8,128)(2,1)S(1)}, u32[]{:S(2)}, u32[]{:S(2)}) %collective-permute-start.7) | collective-permute-done | bytes 262176 | tf_op jit(solution)/shard_map/ppermute | solution.py:607
  40.1 1.8 %collective-permute-start.4 = (bf16[256,1024]{1,0:T(8,128)(2,1)S(1)}, bf16[256,1024]{1,0:T(8,128)(2,1)}, u32[]{:S(2)}, u32[]{:S(2)}) collective-permute-start(bf16[256,1024]{1,0:T(8,128)(2,1)S(1)} %get-tuple-element.27), channel_id=1, source_target_pairs={{0,2},{1,3},{2,0},{3,1},{4,6},{5,7},{6,4},{7,5},{8,10},{9,11},{10,... | collective-permute-start | bytes 1572872 | tf_op jit(solution)/shard_map/ppermute | solution.py:607
  42.4 0.8 prepare.1
  43.3 4.8 %project.4 = (bf16[5,384,256]{2,1,0:T(8,128)(2,1)}, f32[2,64,256]{2,1,0:T(8,128)S(1)}) custom-call(f32[1,2048]{1,0:T(1,128)S(1)} %bitcast.1, f32[1024,8]{1,0:T(8,128)S(1)} %get-tuple-element.28.refs_1_.refs_0_, bf16[128,128]{1,0:T(8,128)(2,1)S(1)} %copy-done.12, bf16[256,256]{1,0:T(8,128)(2,1)S(1)} %copy-done.9, f32[64,128]{1,0:T(8,128)S(1)} %get-tuple-element.29.refs_4_, ...), custom_call_target="tpu_custom_call" | custom-call | flops 503316480 | bytes 7340032 | tf_op jit(solution)/shard_map/project/pallas_call | solution.py:251
  48.3 4.8 %project.5 = (bf16[5,384,256]{2,1,0:T(8,128)(2,1)}, f32[2,64,256]{2,1,0:T(8,128)S(1)}) custom-call(f32[1,2048]{1,0:T(1,128)S(1)} %bitcast.2, f32[1024,8]{1,0:T(8,128)S(1)} %get-tuple-element.28.refs_1_.refs_0_, bf16[128,128]{1,0:T(8,128)(2,1)S(1)} %copy-done.12, bf16[256,256]{1,0:T(8,128)(2,1)S(1)} %copy-done.9, f32[64,128]{1,0:T(8,128)S(1)} %get-tuple-element.29.refs_4_, ...), custom_call_target="tpu_custom_call" | custom-call | flops 503316480 | bytes 7340032 | tf_op jit(solution)/shard_map/project/pallas_call | solution.py:251
  53.1 3.6 %project.3 = (bf16[5,256,256]{2,1,0:T(8,128)(2,1)}, f32[2,64,256]{2,1,0:T(8,128)S(1)}, bf16[128,256]{1,0:T(8,128)(2,1)S(1)}, bf16[128,256]{1,0:T(8,128)(2,1)S(1)}) custom-call(f32[1,2048]{1,0:T(1,128)S(1)} %bitcast.3, f32[1024,8]{1,0:T(8,128)S(1)} %get-tuple-element.28.refs_1_.refs_0_, bf16[128,128]{1,0:T(8,128)(2,1)S(1)} %copy-done.12, ...), custom_call_target="tpu_custom_call" | custom-call | flops 335544320 | bytes 7340032 | tf_op jit(solution)/shard_map/project/pallas_call | solution.py:251
  56.7 0.8 totals.1
  57.6 5.8 %all-to-all-start = ((bf16[8,2,80,128]{3,2,1,0:T(8,128)(2,1)}), bf16[8,2,80,128]{3,2,1,0:T(8,128)(2,1)}, u32[]{:S(2)}, u32[]{:S(2)}) async-start(bf16[8,2,80,128]{3,2,1,0:T(8,128)(2,1)} %totals.1), calls=%async_computation | async-start | bytes 655360 | tf_op jit(solution)/shard_map/all_to_all | solution.py:715
  63.6 1.9 %collective-permute-start.13 = (bf16[128,256]{1,0:T(8,128)(2,1)S(1)}, bf16[128,256]{1,0:T(8,128)(2,1)S(1)}, u32[]{:S(2)}, u32[]{:S(2)}) collective-permute-start(bf16[128,256]{1,0:T(8,128)(2,1)S(1)} %get-tuple-element.37), channel_id=1, source_target_pairs={{0,4},{4,0},{8,12},{12,8},{16,20},{20,16},{24,28},{28,24},{1,5},{5... | collective-permute-start | bytes 196616 | tf_op jit(solution)/shard_map/ppermute | solution.py:711
  65.5 4.7 %collective-permute-done.13.refs_4_ = bf16[128,256]{1,0:T(8,128)(2,1)S(1)} collective-permute-done((bf16[128,256]{1,0:T(8,128)(2,1)S(1)}, bf16[128,256]{1,0:T(8,128)(2,1)S(1)}, u32[]{:S(2)}, u32[]{:S(2)}) %collective-permute-start.13) | collective-permute-done | bytes 65568 | tf_op jit(solution)/shard_map/ppermute | solution.py:711
  70.2 3.4 %collective-permute-start.14 = (bf16[128,256]{1,0:T(8,128)(2,1)S(1)}, bf16[128,256]{1,0:T(8,128)(2,1)S(1)}, u32[]{:S(2)}, u32[]{:S(2)}) collective-permute-start(bf16[128,256]{1,0:T(8,128)(2,1)S(1)} %get-tuple-element.38), channel_id=1, source_target_pairs={{0,28},{4,8},{8,4},{12,16},{16,12},{20,24},{24,20},{28,0},{1,29},{... | collective-permute-start | bytes 196616 | tf_op jit(solution)/shard_map/ppermute | solution.py:713
  73.6 3.5 %collective-permute-done.14.refs_5_ = bf16[128,256]{1,0:T(8,128)(2,1)S(1)} collective-permute-done((bf16[128,256]{1,0:T(8,128)(2,1)S(1)}, bf16[128,256]{1,0:T(8,128)(2,1)S(1)}, u32[]{:S(2)}, u32[]{:S(2)}) %collective-permute-start.14) | collective-permute-done | bytes 65568 | tf_op jit(solution)/shard_map/ppermute | solution.py:713
  77.2 3.5 %attend.3.refs_9_ = bf16[512,256]{1,0:T(8,128)(2,1)S(1)} custom-call(f32[4]{0:T(128)S(1)} %copy-done.16, bf16[5,256,256]{2,1,0:T(8,128)(2,1)} %get-tuple-element.32.refs_1_.refs_4_, bf16[5,384,256]{2,1,0:T(8,128)(2,1)} %get-tuple-element.34.refs_2_.refs_5_, bf16[5,384,256]{2,1,0:T(8,128)(2,1)} %get-tuple-element.36.refs_3_.refs_6_, ...), custom_call_target="tpu_custom_call" | custom-call | flops 800000000 | bytes 3145728 | tf_op jit(solution)/shard_map/attend/pallas_call | solution.py:368
  80.7 1.3 %collective-permute-start.18 = (bf16[512,256]{1,0:T(8,128)(2,1)S(1)}, bf16[512,256]{1,0:T(8,128)(2,1)S(1)}, u32[]{:S(2)}, u32[]{:S(2)}) collective-permute-start(bf16[512,256]{1,0:T(8,128)(2,1)S(1)} %attend.3.refs_9_), channel_id=1, source_target_pairs={{0,2},{1,3},{2,0},{3,1},{4,6},{5,7},{6,4},{7,5},{8,10},{9,11},{10,... | collective-permute-start | bytes 786440 | tf_op jit(solution)/shard_map/ppermute | solution.py:607
  82.0 3.6 %attend.2.refs_8_ = bf16[512,256]{1,0:T(8,128)(2,1)S(1)} custom-call(f32[4]{0:T(128)S(1)} %copy-done.16, bf16[5,256,256]{2,1,0:T(8,128)(2,1)} %get-tuple-element.32.refs_1_.refs_4_, bf16[5,384,256]{2,1,0:T(8,128)(2,1)} %get-tuple-element.34.refs_2_.refs_5_, bf16[5,384,256]{2,1,0:T(8,128)(2,1)} %get-tuple-element.36.refs_3_.refs_6_, ...), custom_call_target="tpu_custom_call" | custom-call | flops 800000000 | bytes 3145728 | tf_op jit(solution)/shard_map/attend/pallas_call | solution.py:368
  85.6 0.9 collective-permute-start.17
  87.0 1.5 %collective-permute-done.18.refs_13_ = bf16[512,256]{1,0:T(8,128)(2,1)S(1)} collective-permute-done((bf16[512,256]{1,0:T(8,128)(2,1)S(1)}, bf16[512,256]{1,0:T(8,128)(2,1)S(1)}, u32[]{:S(2)}, u32[]{:S(2)}) %collective-permute-start.18) | collective-permute-done | bytes 262176 | tf_op jit(solution)/shard_map/ppermute | solution.py:607
  88.5 6.2 %retain.1 = (bf16[512,256]{1,0:T(8,128)(2,1)S(1)}, bf16[512,256]{1,0:T(8,128)(2,1)S(1)}) custom-call(f32[1024,8]{1,0:T(8,128)} %copy-done.4, f32[8,1024]{1,0:T(8,128)} %copy-done.18, bf16[8,2,80,128]{3,2,1,0:T(8,128)(2,1)} %all-to-all-done.refs_2_, f32[2,2,64,128]{3,2,1,0:T(8,128)} %refs_3_.4, bf16[5,256,256]{2,1,0:T(8,128)(2,1)} %get-tuple-element.32.refs_1_.refs_4_, ...), custom_call_target="tpu_custom_call" | custom-call | flops 1500000000 | bytes 4194304 | tf_op jit(solution)/shard_map/retain/pallas_call | solution.py:490
  94.8 1.6 %collective-permute-start.25 = (bf16[512,256]{1,0:T(8,128)(2,1)S(1)}, bf16[512,256]{1,0:T(8,128)(2,1)S(1)}, u32[]{:S(2)}, u32[]{:S(2)}) collective-permute-start(bf16[512,256]{1,0:T(8,128)(2,1)S(1)} %get-tuple-element.43.refs_16_), channel_id=1, source_target_pairs={{0,2},{1,3},{2,0},{3,1},{4,6},{5,7},{6,4},{7,5},{8,10},{9,11},{10,... | collective-permute-start | bytes 786440 | tf_op jit(solution)/shard_map/ppermute | solution.py:607
  97.5 6.5 %collective-permute-done.25.refs_2_ = bf16[512,256]{1,0:T(8,128)(2,1)S(1)} collective-permute-done((bf16[512,256]{1,0:T(8,128)(2,1)S(1)}, bf16[512,256]{1,0:T(8,128)(2,1)S(1)}, u32[]{:S(2)}, u32[]{:S(2)}) %collective-permute-start.25) | collective-permute-done | bytes 262176 | tf_op jit(solution)/shard_map/ppermute | solution.py:607
  104.0 5.0 %collective-permute-done.23.refs_2_ = bf16[512,256]{1,0:T(8,128)(2,1)S(1)} collective-permute-done((bf16[512,256]{1,0:T(8,128)(2,1)S(1)}, bf16[512,256]{1,0:T(8,128)(2,1)S(1)}, u32[]{:S(2)}, u32[]{:S(2)}) %collective-permute-start.23) | collective-permute-done | bytes 262176 | tf_op jit(solution)/shard_map/ppermute | solution.py:607
  109.2 0.6 copy-done.25
  109.9 0.7 copy-done.27
  110.6 4.5 %most.1 = (f32[1024,512]{1,0:T(8,128)S(1)}, bf16[512,512]{1,0:T(8,128)(2,1)S(1)}) custom-call(bf16[256,2048]{1,0:T(8,128)(2,1)} %refs_0_.9, bf16[256,2048]{1,0:T(8,128)(2,1)} %refs_1_.3, bf16[256,2048]{1,0:T(8,128)(2,1)} %collective-permute-done.refs_2_, bf16[256,2048]{1,0:T(8,128)(2,1)} %collective-permute-done.1.refs_3_, ...), custom_call_target="tpu_custom_call" | custom-call | flops 1000000000 | bytes 8388608 | tf_op jit(solution)/shard_map/most/pallas_call | solution.py:544
  115.1 1.2 last.2.refs_4_
  116.3 1.2 last.3
  (93 shorter events, 3.9 us)
Async XLA Ops:
  0.0 39.5 %copy-start.19 = (bf16[256,2048]{1,0:T(8,128)(2,1)S(1)}, bf16[256,2048]{1,0:T(8,128)(2,1)}, u32[]{:S(2)}) copy-start(bf16[256,2048]{1,0:T(8,128)(2,1)} %refs_0_.9) | copy-start | bytes 3145732
  0.0 39.5 %copy-start.20 = (bf16[256,2048]{1,0:T(8,128)(2,1)S(1)}, bf16[256,2048]{1,0:T(8,128)(2,1)}, u32[]{:S(2)}) copy-start(bf16[256,2048]{1,0:T(8,128)(2,1)} %refs_1_.3) | copy-start | bytes 3145732
  0.0 42.4 %copy-start.17 = (f32[2,1024]{1,0:T(2,128)S(1)}, f32[2,1024]{1,0:T(2,128)}, u32[]{:S(2)}) copy-start(f32[2,1024]{1,0:T(2,128)} %log_ref.1) | copy-start | bytes 24580
  0.0 41.9 %collective-permute-start.6 = (bf16[1024,512]{1,0:T(8,128)(2,1)}, bf16[1024,512]{1,0:T(8,128)(2,1)S(1)}, u32[]{:S(2)}, u32[]{:S(2)}) collective-permute-start(bf16[1024,512]{1,0:T(8,128)(2,1)} %refs_6_.5), channel_id=1, source_target_pairs={{0,1},{1,0},{2,3},{3,2},{4,5},{5,4},{6,7},{7,6},{8,9},{9,8},{10,11... | collective-permute-start | bytes 3145736 | tf_op jit(solution)/shard_map/ppermute | solution.py:602
  1.9 12.6 %collective-permute-start.9 = (bf16[384,512]{1,0:T(8,128)(2,1)S(1)}, bf16[384,512]{1,0:T(8,128)(2,1)S(1)}, u32[]{:S(2)}, u32[]{:S(2)}) collective-permute-start(bf16[384,512]{1,0:T(8,128)(2,1)S(1)} %get-tuple-element.33), channel_id=1, source_target_pairs={{0,2},{1,3},{2,0},{3,1},{4,6},{5,7},{6,4},{7,5},{8,10},{9,11},{10,... | collective-permute-start | bytes 1179656 | tf_op jit(solution)/shard_map/ppermute | solution.py:607
  5.8 34.2 %collective-permute-start.2 = (bf16[256,1024]{1,0:T(8,128)(2,1)S(1)}, bf16[256,1024]{1,0:T(8,128)(2,1)}, u32[]{:S(2)}, u32[]{:S(2)}) collective-permute-start(bf16[256,1024]{1,0:T(8,128)(2,1)S(1)} %get-tuple-element.26), channel_id=1, source_target_pairs={{0,2},{1,3},{2,0},{3,1},{4,6},{5,7},{6,4},{7,5},{8,10},{9,11},{10,... | collective-permute-start | bytes 1572872 | tf_op jit(solution)/shard_map/ppermute | solution.py:607
  5.9 33.6 %collective-permute-start.11 = (bf16[384,512]{1,0:T(8,128)(2,1)S(1)}, bf16[384,512]{1,0:T(8,128)(2,1)S(1)}, u32[]{:S(2)}, u32[]{:S(2)}) collective-permute-start(bf16[384,512]{1,0:T(8,128)(2,1)S(1)} %get-tuple-element.35), channel_id=1, source_target_pairs={{0,2},{1,3},{2,0},{3,1},{4,6},{5,7},{6,4},{7,5},{8,10},{9,11},{10,... | collective-permute-start | bytes 1179656 | tf_op jit(solution)/shard_map/ppermute | solution.py:607
  14.5 27.4 %collective-permute-start.10 = (bf16[384,512]{1,0:T(8,128)(2,1)S(1)}, bf16[384,512]{1,0:T(8,128)(2,1)S(1)}, u32[]{:S(2)}, u32[]{:S(2)}) collective-permute-start(bf16[384,512]{1,0:T(8,128)(2,1)S(1)} %collective-permute-done.9.refs_8_), channel_id=1, source_target_pairs={{0,1},{1,0},{2,3},{3,2},{4,5},{5,4},{6,7},{7,6},{8,9},{9,8},{10,11... | collective-permute-start | bytes 1179656 | tf_op jit(solution)/shard_map/ppermute | solution.py:602
  14.5 25.0 %collective-permute-start.7 = (bf16[256,512]{1,0:T(8,128)(2,1)S(1)}, bf16[256,512]{1,0:T(8,128)(2,1)S(1)}, u32[]{:S(2)}, u32[]{:S(2)}) collective-permute-start(bf16[256,512]{1,0:T(8,128)(2,1)S(1)} %get-tuple-element.31), channel_id=1, source_target_pairs={{0,2},{1,3},{2,0},{3,1},{4,6},{5,7},{6,4},{7,5},{8,10},{9,11},{10,... | collective-permute-start | bytes 786440 | tf_op jit(solution)/shard_map/ppermute | solution.py:607
  39.5 47.1 %collective-permute-start = (bf16[256,2048]{1,0:T(8,128)(2,1)S(1)}, bf16[256,2048]{1,0:T(8,128)(2,1)}, u32[]{:S(2)}, u32[]{:S(2)}) collective-permute-start(bf16[256,2048]{1,0:T(8,128)(2,1)S(1)} %copy-done.19), channel_id=1, source_target_pairs={{0,1},{1,0},{2,3},{3,2},{4,5},{5,4},{6,7},{7,6},{8,9},{9,8},{10,11... | collective-permute-start | bytes 3145736 | tf_op jit(solution)/shard_map/ppermute | solution.py:602
  39.5 55.3 %collective-permute-start.1 = (bf16[256,2048]{1,0:T(8,128)(2,1)S(1)}, bf16[256,2048]{1,0:T(8,128)(2,1)}, u32[]{:S(2)}, u32[]{:S(2)}) collective-permute-start(bf16[256,2048]{1,0:T(8,128)(2,1)S(1)} %copy-done.20), channel_id=1, source_target_pairs={{0,1},{1,0},{2,3},{3,2},{4,5},{5,4},{6,7},{7,6},{8,9},{9,8},{10,11... | collective-permute-start | bytes 3145736 | tf_op jit(solution)/shard_map/ppermute | solution.py:602
  40.1 23.3 %collective-permute-start.4 = (bf16[256,1024]{1,0:T(8,128)(2,1)S(1)}, bf16[256,1024]{1,0:T(8,128)(2,1)}, u32[]{:S(2)}, u32[]{:S(2)}) collective-permute-start(bf16[256,1024]{1,0:T(8,128)(2,1)S(1)} %get-tuple-element.27), channel_id=1, source_target_pairs={{0,2},{1,3},{2,0},{3,1},{4,6},{5,7},{6,4},{7,5},{8,10},{9,11},{10,... | collective-permute-start | bytes 1572872 | tf_op jit(solution)/shard_map/ppermute | solution.py:607
  41.9 11.2 %collective-permute-start.8 = (bf16[256,512]{1,0:T(8,128)(2,1)S(1)}, bf16[256,512]{1,0:T(8,128)(2,1)S(1)}, u32[]{:S(2)}, u32[]{:S(2)}) collective-permute-start(bf16[256,512]{1,0:T(8,128)(2,1)S(1)} %collective-permute-done.7.refs_8_), channel_id=1, source_target_pairs={{0,1},{1,0},{2,3},{3,2},{4,5},{5,4},{6,7},{7,6},{8,9},{9,8},{10,11... | collective-permute-start | bytes 786440 | tf_op jit(solution)/shard_map/ppermute | solution.py:602
  41.9 6.2 %collective-permute-start.12 = (bf16[384,512]{1,0:T(8,128)(2,1)S(1)}, bf16[384,512]{1,0:T(8,128)(2,1)S(1)}, u32[]{:S(2)}, u32[]{:S(2)}) collective-permute-start(bf16[384,512]{1,0:T(8,128)(2,1)S(1)} %collective-permute-done.11.refs_8_), channel_id=1, source_target_pairs={{0,1},{1,0},{2,3},{3,2},{4,5},{5,4},{6,7},{7,6},{8,9},{9,8},{10,11... | collective-permute-start | bytes 1179656 | tf_op jit(solution)/shard_map/ppermute | solution.py:602
  48.1 37.5 %collective-permute-start.3 = (bf16[256,1024]{1,0:T(8,128)(2,1)}, bf16[256,1024]{1,0:T(8,128)(2,1)}, u32[]{:S(2)}, u32[]{:S(2)}) collective-permute-start(bf16[256,1024]{1,0:T(8,128)(2,1)} %collective-permute-done.2.refs_4_), channel_id=1, source_target_pairs={{0,1},{1,0},{2,3},{3,2},{4,5},{5,4},{6,7},{7,6},{8,9},{9,8},{10,11... | collective-permute-start | bytes 1572872 | tf_op jit(solution)/shard_map/ppermute | solution.py:602
  53.1 24.1 %copy-start.16 = (f32[4]{0:T(128)S(1)}, f32[4]{0:T(128)}, u32[]{:S(2)}) copy-start(f32[4]{0:T(128)} %refs_0_.8) | copy-start | bytes 52
  57.6 31.0 %all-to-all-start = ((bf16[8,2,80,128]{3,2,1,0:T(8,128)(2,1)}), bf16[8,2,80,128]{3,2,1,0:T(8,128)(2,1)}, u32[]{:S(2)}, u32[]{:S(2)}) async-start(bf16[8,2,80,128]{3,2,1,0:T(8,128)(2,1)} %totals.1), calls=%async_computation | async-start | bytes 655360 | tf_op jit(solution)/shard_map/all_to_all | solution.py:715
  63.4 23.1 %collective-permute-start.5 = (bf16[256,1024]{1,0:T(8,128)(2,1)}, bf16[256,1024]{1,0:T(8,128)(2,1)S(1)}, u32[]{:S(2)}, u32[]{:S(2)}) collective-permute-start(bf16[256,1024]{1,0:T(8,128)(2,1)} %collective-permute-done.4.refs_6_), channel_id=1, source_target_pairs={{0,1},{1,0},{2,3},{3,2},{4,5},{5,4},{6,7},{7,6},{8,9},{9,8},{10,11... | collective-permute-start | bytes 1572872 | tf_op jit(solution)/shard_map/ppermute | solution.py:602
  63.6 6.6 %collective-permute-start.13 = (bf16[128,256]{1,0:T(8,128)(2,1)S(1)}, bf16[128,256]{1,0:T(8,128)(2,1)S(1)}, u32[]{:S(2)}, u32[]{:S(2)}) collective-permute-start(bf16[128,256]{1,0:T(8,128)(2,1)S(1)} %get-tuple-element.37), channel_id=1, source_target_pairs={{0,4},{4,0},{8,12},{12,8},{16,20},{20,16},{24,28},{28,24},{1,5},{5... | collective-permute-start | bytes 196616 | tf_op jit(solution)/shard_map/ppermute | solution.py:711
  70.2 7.0 %collective-permute-start.14 = (bf16[128,256]{1,0:T(8,128)(2,1)S(1)}, bf16[128,256]{1,0:T(8,128)(2,1)S(1)}, u32[]{:S(2)}, u32[]{:S(2)}) collective-permute-start(bf16[128,256]{1,0:T(8,128)(2,1)S(1)} %get-tuple-element.38), channel_id=1, source_target_pairs={{0,28},{4,8},{8,4},{12,16},{16,12},{20,24},{24,20},{28,0},{1,29},{... | collective-permute-start | bytes 196616 | tf_op jit(solution)/shard_map/ppermute | solution.py:713
  80.7 7.8 %collective-permute-start.18 = (bf16[512,256]{1,0:T(8,128)(2,1)S(1)}, bf16[512,256]{1,0:T(8,128)(2,1)S(1)}, u32[]{:S(2)}, u32[]{:S(2)}) collective-permute-start(bf16[512,256]{1,0:T(8,128)(2,1)S(1)} %attend.3.refs_9_), channel_id=1, source_target_pairs={{0,2},{1,3},{2,0},{3,1},{4,6},{5,7},{6,4},{7,5},{8,10},{9,11},{10,... | collective-permute-start | bytes 786440 | tf_op jit(solution)/shard_map/ppermute | solution.py:607
  85.6 10.8 %collective-permute-start.17 = (bf16[512,256]{1,0:T(8,128)(2,1)S(1)}, bf16[512,256]{1,0:T(8,128)(2,1)}, u32[]{:S(2)}, u32[]{:S(2)}) collective-permute-start(bf16[512,256]{1,0:T(8,128)(2,1)S(1)} %attend.2.refs_8_), channel_id=1, source_target_pairs={{0,2},{1,3},{2,0},{3,1},{4,6},{5,7},{6,4},{7,5},{8,10},{9,11},{10,... | collective-permute-start | bytes 786440 | tf_op jit(solution)/shard_map/ppermute | solution.py:607
  86.5 10.4 %collective-permute-start.16 = (bf16[512,256]{1,0:T(8,128)(2,1)S(1)}, bf16[512,256]{1,0:T(8,128)(2,1)}, u32[]{:S(2)}, u32[]{:S(2)}) collective-permute-start(bf16[512,256]{1,0:T(8,128)(2,1)S(1)} %attend.3.refs_9_), channel_id=1, source_target_pairs={{0,1},{1,0},{2,3},{3,2},{4,5},{5,4},{6,7},{7,6},{8,9},{9,8},{10,11... | collective-permute-start | bytes 786440 | tf_op jit(solution)/shard_map/ppermute | solution.py:602
  86.5 10.4 %collective-permute-start.15 = (bf16[512,256]{1,0:T(8,128)(2,1)S(1)}, bf16[512,256]{1,0:T(8,128)(2,1)S(1)}, u32[]{:S(2)}, u32[]{:S(2)}) collective-permute-start(bf16[512,256]{1,0:T(8,128)(2,1)S(1)} %attend.2.refs_8_), channel_id=1, source_target_pairs={{0,1},{1,0},{2,3},{3,2},{4,5},{5,4},{6,7},{7,6},{8,9},{9,8},{10,11... | collective-permute-start | bytes 786440 | tf_op jit(solution)/shard_map/ppermute | solution.py:602
  88.5 8.9 %collective-permute-start.20 = (bf16[512,256]{1,0:T(8,128)(2,1)S(1)}, bf16[512,256]{1,0:T(8,128)(2,1)S(1)}, u32[]{:S(2)}, u32[]{:S(2)}) collective-permute-start(bf16[512,256]{1,0:T(8,128)(2,1)S(1)} %collective-permute-done.18.refs_13_), channel_id=1, source_target_pairs={{0,1},{1,0},{2,3},{3,2},{4,5},{5,4},{6,7},{7,6},{8,9},{9,8},{10,11... | collective-permute-start | bytes 786440 | tf_op jit(solution)/shard_map/ppermute | solution.py:602
  94.8 9.2 %collective-permute-start.25 = (bf16[512,256]{1,0:T(8,128)(2,1)S(1)}, bf16[512,256]{1,0:T(8,128)(2,1)S(1)}, u32[]{:S(2)}, u32[]{:S(2)}) collective-permute-start(bf16[512,256]{1,0:T(8,128)(2,1)S(1)} %get-tuple-element.43.refs_16_), channel_id=1, source_target_pairs={{0,2},{1,3},{2,0},{3,1},{4,6},{5,7},{6,4},{7,5},{8,10},{9,11},{10,... | collective-permute-start | bytes 786440 | tf_op jit(solution)/shard_map/ppermute | solution.py:607
  96.4 12.7 %collective-permute-start.23 = (bf16[512,256]{1,0:T(8,128)(2,1)S(1)}, bf16[512,256]{1,0:T(8,128)(2,1)S(1)}, u32[]{:S(2)}, u32[]{:S(2)}) collective-permute-start(bf16[512,256]{1,0:T(8,128)(2,1)S(1)} %get-tuple-element.44.refs_17_), channel_id=1, source_target_pairs={{0,2},{1,3},{2,0},{3,1},{4,6},{5,7},{6,4},{7,5},{8,10},{9,11},{10,... | collective-permute-start | bytes 786440 | tf_op jit(solution)/shard_map/ppermute | solution.py:607
  96.9 12.2 %collective-permute-start.19 = (bf16[512,256]{1,0:T(8,128)(2,1)}, bf16[512,256]{1,0:T(8,128)(2,1)S(1)}, u32[]{:S(2)}, u32[]{:S(2)}) collective-permute-start(bf16[512,256]{1,0:T(8,128)(2,1)} %collective-permute-done.17.refs_12_), channel_id=1, source_target_pairs={{0,1},{1,0},{2,3},{3,2},{4,5},{5,4},{6,7},{7,6},{8,9},{9,8},{10,11... | collective-permute-start | bytes 786440 | tf_op jit(solution)/shard_map/ppermute | solution.py:602
  96.9 12.2 %collective-permute-start.21 = (bf16[512,256]{1,0:T(8,128)(2,1)S(1)}, bf16[512,256]{1,0:T(8,128)(2,1)S(1)}, u32[]{:S(2)}, u32[]{:S(2)}) collective-permute-start(bf16[512,256]{1,0:T(8,128)(2,1)S(1)} %get-tuple-element.43.refs_16_), channel_id=1, source_target_pairs={{0,1},{1,0},{2,3},{3,2},{4,5},{5,4},{6,7},{7,6},{8,9},{9,8},{10,11... | collective-permute-start | bytes 786440 | tf_op jit(solution)/shard_map/ppermute | solution.py:602
  97.4 11.7 %collective-permute-start.22 = (bf16[512,256]{1,0:T(8,128)(2,1)S(1)}, bf16[512,256]{1,0:T(8,128)(2,1)S(1)}, u32[]{:S(2)}, u32[]{:S(2)}) collective-permute-start(bf16[512,256]{1,0:T(8,128)(2,1)S(1)} %get-tuple-element.44.refs_17_), channel_id=1, source_target_pairs={{0,1},{1,0},{2,3},{3,2},{4,5},{5,4},{6,7},{7,6},{8,9},{9,8},{10,11... | collective-permute-start | bytes 786440 | tf_op jit(solution)/shard_map/ppermute | solution.py:602
  104.0 11.1 %collective-permute-start.26 = (bf16[512,256]{1,0:T(8,128)(2,1)S(1)}, bf16[512,256]{1,0:T(8,128)(2,1)S(1)}, u32[]{:S(2)}, u32[]{:S(2)}) collective-permute-start(bf16[512,256]{1,0:T(8,128)(2,1)S(1)} %collective-permute-done.25.refs_2_), channel_id=1, source_target_pairs={{0,1},{1,0},{2,3},{3,2},{4,5},{5,4},{6,7},{7,6},{8,9},{9,8},{10,11... | collective-permute-start | bytes 786440 | tf_op jit(solution)/shard_map/ppermute | solution.py:602
  109.1 7.2 %collective-permute-start.24 = (bf16[512,256]{1,0:T(8,128)(2,1)S(1)}, bf16[512,256]{1,0:T(8,128)(2,1)S(1)}, u32[]{:S(2)}, u32[]{:S(2)}) collective-permute-start(bf16[512,256]{1,0:T(8,128)(2,1)S(1)} %collective-permute-done.23.refs_2_), channel_id=1, source_target_pairs={{0,1},{1,0},{2,3},{3,2},{4,5},{5,4},{6,7},{7,6},{8,9},{9,8},{10,11... | collective-permute-start | bytes 786440 | tf_op jit(solution)/shard_map/ppermute | solution.py:602
  (24 other events, 146.6 us)

commit v6 on v5

--- a/solution.py
+++ b/solution.py
@@ -108,23 +108,26 @@
     )(*in_hbm([att, ret]))
 
 
-def split_kernel(*refs):
+def split_kernel(low, high, *refs):
     tokens, sems = refs[0], refs[-1]
     copies = Copies(sems)
     size = tokens.shape[0] // 8
     for c, inner, first, count in runs():
-        dst = refs[1 + c].at[pl.ds(inner * size, count * size)]
+        if not low <= c < high:
+            continue
+        dst = refs[1 + c - low].at[pl.ds(inner * size, count * size)]
         copies.start(tokens.at[pl.ds(first * size, count * size)], dst)
     copies.wait()
 
 
-def split(tokens):
+def split(tokens, low, high):
     total, cols = tokens.shape
-    return pl.pallas_call(
-        split_kernel,
-        out_shape=tuple(jax.ShapeDtypeStruct((len(e) * total // 8, cols), BF16) for e in CHUNKS),
+    sizes = [len(e) * total // 8 for e in CHUNKS[low:high]]
+    return pl.pallas_call(
+        functools.partial(split_kernel, low, high),
+        out_shape=tuple(jax.ShapeDtypeStruct((size, cols), BF16) for size in sizes),
         in_specs=[HBM],
-        out_specs=(VMEM,) * len(CHUNKS),
+        out_specs=(VMEM,) * len(sizes),
         scratch_shapes=[pltpu.SemaphoreType.DMA((len(runs()),))],
         cost_estimate=cost(0.1e9, 3 << 20),
         compiler_params=PARAMS,
@@ -662,7 +665,8 @@
     cols = tokens.shape[1]
 
     slabs = slab(out_att, out_ret, cols)
-    pieces = split(tokens)
+    pieces = list(split(tokens, 0, 1))
+    pieces += split(tokens, 1, len(CHUNKS))
     near = core_swap(tokens)
     far = {}
     for c in range(len(CHUNKS)):

time: 118 us -> 118 us (level)
  transfers between devices with their start and end apart: 28 -> 28, of which waited for: 7 -> 7; matrix products, arithmetic and copies ran while one was open for 0% -> 0% of each run, Pallas kernels for 31% -> 32%
where the time goes in v6:
time: 118 us
  waiting for transfers between devices  49.9 us (42%)
  Pallas kernels  38.3 us (32%)
  starting transfers between devices  27 us (23%)
  local copies, waits for them, and re-layouts  1.61 us (1%)
    ppermute x9, waiting for transfers between devices, chip_turn(): return lax.ppermute(value, 'tp', [(i, (i + 2 * by) % n) for i in range(n)])  41.6 us
    pallas_call x3, Pallas kernels, project(): pl.pallas_call(functools.partial(project_kernel, n, len(weights), parts,...  13.2 us
    ppermute x9, starting transfers between devices, chip_turn(): return lax.ppermute(value, 'tp', [(i, (i + 2 * by) % n) for i in range(n)])  12.9 us
    pallas_call x2, Pallas kernels, attend(): pl.pallas_call(functools.partial(attend_kernel, n, kv_local, groups, seq_...  7.14 us
    pallas_call x1, Pallas kernels, retain(): pl.pallas_call(functools.partial(retain_kernel, n, ret_local, n_sp), out_...  6.17 us
    all_to_all x1, starting transfers between devices, body(): got = lax.all_to_all(sent, 'sp', 0, 0, tiled=True)  5.81 us
    ppermute x1, waiting for transfers between devices, body(): edge0 = lax.ppermute(edges[0], 'sp', [(i, i ^ 1) for i in range(n_sp)])  4.73 us
    pallas_call x1, Pallas kernels, most(): pl.pallas_call(functools.partial(most_kernel, n_far, n), out_shape=(pltpu...  4.47 us
  transfers between devices with their start and end apart: 28, of which 7 were waited for; matrix products, arithmetic and copies ran while one was open for 0% of the time, Pallas kernels for 32%

profile of v6, /device:TPU:0, one launch (start us, length us, event | category | flops | bytes accessed | tf_op | source)
XLA Modules:
  0.0 117.5 jit_solution(16172929697661586411)
XLA Ops:
  0.6 1.2 %split.3 = (bf16[384,512]{1,0:T(8,128)(2,1)S(1)}, bf16[384,512]{1,0:T(8,128)(2,1)S(1)}) custom-call(bf16[1024,512]{1,0:T(8,128)(2,1)} %refs_6_.5), custom_call_target="tpu_custom_call" | custom-call | flops 100000000 | bytes 3145728 | tf_op jit(solution)/shard_map/split/pallas_call | solution.py:126
  1.8 2.6 %collective-permute-start.9 = (bf16[384,512]{1,0:T(8,128)(2,1)S(1)}, bf16[384,512]{1,0:T(8,128)(2,1)S(1)}, u32[]{:S(2)}, u32[]{:S(2)}) collective-permute-start(bf16[384,512]{1,0:T(8,128)(2,1)S(1)} %get-tuple-element.31), channel_id=1, source_target_pairs={{0,2},{1,3},{2,0},{3,1},{4,6},{5,7},{6,4},{7,5},{8,10},{9,11},{10,... | collective-permute-start | bytes 1179656 | tf_op jit(solution)/shard_map/ppermute | solution.py:610
  4.4 1.2 %slab.1 = (bf16[256,1024]{1,0:T(8,128)(2,1)S(1)}, bf16[256,1024]{1,0:T(8,128)(2,1)S(1)}) custom-call(bf16[256,2048]{1,0:T(8,128)(2,1)} %refs_0_.11, bf16[256,2048]{1,0:T(8,128)(2,1)} %refs_1_.3), custom_call_target="tpu_custom_call" | custom-call | flops 100000000 | bytes 3145728 | tf_op jit(solution)/shard_map/slab/pallas_call | solution.py:99
  5.8 2.0 %collective-permute-start.11 = (bf16[384,512]{1,0:T(8,128)(2,1)S(1)}, bf16[384,512]{1,0:T(8,128)(2,1)S(1)}, u32[]{:S(2)}, u32[]{:S(2)}) collective-permute-start(bf16[384,512]{1,0:T(8,128)(2,1)S(1)} %get-tuple-element.33), channel_id=1, source_target_pairs={{0,2},{1,3},{2,0},{3,1},{4,6},{5,7},{6,4},{7,5},{8,10},{9,11},{10,... | collective-permute-start | bytes 1179656 | tf_op jit(solution)/shard_map/ppermute | solution.py:610
  7.8 6.7 %collective-permute-done.9.refs_8_ = bf16[384,512]{1,0:T(8,128)(2,1)S(1)} collective-permute-done((bf16[384,512]{1,0:T(8,128)(2,1)S(1)}, bf16[384,512]{1,0:T(8,128)(2,1)S(1)}, u32[]{:S(2)}, u32[]{:S(2)}) %collective-permute-start.9) | collective-permute-done | bytes 393248 | tf_op jit(solution)/shard_map/ppermute | solution.py:610
  14.4 1.0 split.2
  15.4 2.1 %collective-permute-start.7 = (bf16[256,512]{1,0:T(8,128)(2,1)S(1)}, bf16[256,512]{1,0:T(8,128)(2,1)S(1)}, u32[]{:S(2)}, u32[]{:S(2)}) collective-permute-start(bf16[256,512]{1,0:T(8,128)(2,1)S(1)} %split.2), channel_id=1, source_target_pairs={{0,2},{1,3},{2,0},{3,1},{4,6},{5,7},{6,4},{7,5},{8,10},{9,11},{10,... | collective-permute-start | bytes 786440 | tf_op jit(solution)/shard_map/ppermute | solution.py:610
  17.5 21.9 %collective-permute-done.7.refs_8_ = bf16[256,512]{1,0:T(8,128)(2,1)S(1)} collective-permute-done((bf16[256,512]{1,0:T(8,128)(2,1)S(1)}, bf16[256,512]{1,0:T(8,128)(2,1)S(1)}, u32[]{:S(2)}, u32[]{:S(2)}) %collective-permute-start.7) | collective-permute-done | bytes 262176 | tf_op jit(solution)/shard_map/ppermute | solution.py:610
  40.0 1.8 %collective-permute-start.4 = (bf16[256,1024]{1,0:T(8,128)(2,1)S(1)}, bf16[256,1024]{1,0:T(8,128)(2,1)}, u32[]{:S(2)}, u32[]{:S(2)}) collective-permute-start(bf16[256,1024]{1,0:T(8,128)(2,1)S(1)} %get-tuple-element.26), channel_id=1, source_target_pairs={{0,2},{1,3},{2,0},{3,1},{4,6},{5,7},{6,4},{7,5},{8,10},{9,11},{10,... | collective-permute-start | bytes 1572872 | tf_op jit(solution)/shard_map/ppermute | solution.py:610
  42.3 0.8 prepare.1
  43.2 4.8 %project.4 = (bf16[5,384,256]{2,1,0:T(8,128)(2,1)}, f32[2,64,256]{2,1,0:T(8,128)S(1)}) custom-call(f32[1,2048]{1,0:T(1,128)S(1)} %bitcast.1, f32[1024,8]{1,0:T(8,128)S(1)} %get-tuple-element.27.refs_1_.refs_0_, bf16[128,128]{1,0:T(8,128)(2,1)S(1)} %copy-done.12, bf16[256,256]{1,0:T(8,128)(2,1)S(1)} %copy-done.9, f32[64,128]{1,0:T(8,128)S(1)} %get-tuple-element.28.refs_4_, ...), custom_call_target="tpu_custom_call" | custom-call | flops 503316480 | bytes 7340032 | tf_op jit(solution)/shard_map/project/pallas_call | solution.py:254
  48.2 4.8 %project.5 = (bf16[5,384,256]{2,1,0:T(8,128)(2,1)}, f32[2,64,256]{2,1,0:T(8,128)S(1)}) custom-call(f32[1,2048]{1,0:T(1,128)S(1)} %bitcast.2, f32[1024,8]{1,0:T(8,128)S(1)} %get-tuple-element.27.refs_1_.refs_0_, bf16[128,128]{1,0:T(8,128)(2,1)S(1)} %copy-done.12, bf16[256,256]{1,0:T(8,128)(2,1)S(1)} %copy-done.9, f32[64,128]{1,0:T(8,128)S(1)} %get-tuple-element.28.refs_4_, ...), custom_call_target="tpu_custom_call" | custom-call | flops 503316480 | bytes 7340032 | tf_op jit(solution)/shard_map/project/pallas_call | solution.py:254
  53.0 3.6 %project.3 = (bf16[5,256,256]{2,1,0:T(8,128)(2,1)}, f32[2,64,256]{2,1,0:T(8,128)S(1)}, bf16[128,256]{1,0:T(8,128)(2,1)S(1)}, bf16[128,256]{1,0:T(8,128)(2,1)S(1)}) custom-call(f32[1,2048]{1,0:T(1,128)S(1)} %bitcast.3, f32[1024,8]{1,0:T(8,128)S(1)} %get-tuple-element.27.refs_1_.refs_0_, bf16[128,128]{1,0:T(8,128)(2,1)S(1)} %copy-done.12, ...), custom_call_target="tpu_custom_call" | custom-call | flops 335544320 | bytes 7340032 | tf_op jit(solution)/shard_map/project/pallas_call | solution.py:254
  56.6 0.8 totals.1
  57.5 5.8 %all-to-all-start = ((bf16[8,2,80,128]{3,2,1,0:T(8,128)(2,1)}), bf16[8,2,80,128]{3,2,1,0:T(8,128)(2,1)}, u32[]{:S(2)}, u32[]{:S(2)}) async-start(bf16[8,2,80,128]{3,2,1,0:T(8,128)(2,1)} %totals.1), calls=%async_computation | async-start | bytes 655360 | tf_op jit(solution)/shard_map/all_to_all | solution.py:719
  63.5 1.9 %collective-permute-start.13 = (bf16[128,256]{1,0:T(8,128)(2,1)S(1)}, bf16[128,256]{1,0:T(8,128)(2,1)S(1)}, u32[]{:S(2)}, u32[]{:S(2)}) collective-permute-start(bf16[128,256]{1,0:T(8,128)(2,1)S(1)} %get-tuple-element.35), channel_id=1, source_target_pairs={{0,4},{4,0},{8,12},{12,8},{16,20},{20,16},{24,28},{28,24},{1,5},{5... | collective-permute-start | bytes 196616 | tf_op jit(solution)/shard_map/ppermute | solution.py:715
  65.4 4.7 %collective-permute-done.13.refs_4_ = bf16[128,256]{1,0:T(8,128)(2,1)S(1)} collective-permute-done((bf16[128,256]{1,0:T(8,128)(2,1)S(1)}, bf16[128,256]{1,0:T(8,128)(2,1)S(1)}, u32[]{:S(2)}, u32[]{:S(2)}) %collective-permute-start.13) | collective-permute-done | bytes 65568 | tf_op jit(solution)/shard_map/ppermute | solution.py:715
  70.1 3.4 %collective-permute-start.14 = (bf16[128,256]{1,0:T(8,128)(2,1)S(1)}, bf16[128,256]{1,0:T(8,128)(2,1)S(1)}, u32[]{:S(2)}, u32[]{:S(2)}) collective-permute-start(bf16[128,256]{1,0:T(8,128)(2,1)S(1)} %get-tuple-element.36), channel_id=1, source_target_pairs={{0,28},{4,8},{8,4},{12,16},{16,12},{20,24},{24,20},{28,0},{1,29},{... | collective-permute-start | bytes 196616 | tf_op jit(solution)/shard_map/ppermute | solution.py:717
  73.6 3.5 %collective-permute-done.14.refs_5_ = bf16[128,256]{1,0:T(8,128)(2,1)S(1)} collective-permute-done((bf16[128,256]{1,0:T(8,128)(2,1)S(1)}, bf16[128,256]{1,0:T(8,128)(2,1)S(1)}, u32[]{:S(2)}, u32[]{:S(2)}) %collective-permute-start.14) | collective-permute-done | bytes 65568 | tf_op jit(solution)/shard_map/ppermute | solution.py:717
  77.1 3.5 %attend.3.refs_9_ = bf16[512,256]{1,0:T(8,128)(2,1)S(1)} custom-call(f32[4]{0:T(128)S(1)} %copy-done.16, bf16[5,256,256]{2,1,0:T(8,128)(2,1)} %get-tuple-element.30.refs_1_.refs_4_, bf16[5,384,256]{2,1,0:T(8,128)(2,1)} %get-tuple-element.32.refs_2_.refs_5_, bf16[5,384,256]{2,1,0:T(8,128)(2,1)} %get-tuple-element.34.refs_3_.refs_6_, ...), custom_call_target="tpu_custom_call" | custom-call | flops 800000000 | bytes 3145728 | tf_op jit(solution)/shard_map/attend/pallas_call | solution.py:371
  80.6 1.2 %collective-permute-start.18 = (bf16[512,256]{1,0:T(8,128)(2,1)S(1)}, bf16[512,256]{1,0:T(8,128)(2,1)S(1)}, u32[]{:S(2)}, u32[]{:S(2)}) collective-permute-start(bf16[512,256]{1,0:T(8,128)(2,1)S(1)} %attend.3.refs_9_), channel_id=1, source_target_pairs={{0,2},{1,3},{2,0},{3,1},{4,6},{5,7},{6,4},{7,5},{8,10},{9,11},{10,... | collective-permute-start | bytes 786440 | tf_op jit(solution)/shard_map/ppermute | solution.py:610
  81.9 3.6 %attend.2.refs_8_ = bf16[512,256]{1,0:T(8,128)(2,1)S(1)} custom-call(f32[4]{0:T(128)S(1)} %copy-done.16, bf16[5,256,256]{2,1,0:T(8,128)(2,1)} %get-tuple-element.30.refs_1_.refs_4_, bf16[5,384,256]{2,1,0:T(8,128)(2,1)} %get-tuple-element.32.refs_2_.refs_5_, bf16[5,384,256]{2,1,0:T(8,128)(2,1)} %get-tuple-element.34.refs_3_.refs_6_, ...), custom_call_target="tpu_custom_call" | custom-call | flops 800000000 | bytes 3145728 | tf_op jit(solution)/shard_map/attend/pallas_call | solution.py:371
  85.5 0.9 collective-permute-start.17
  86.9 1.5 %collective-permute-done.18.refs_13_ = bf16[512,256]{1,0:T(8,128)(2,1)S(1)} collective-permute-done((bf16[512,256]{1,0:T(8,128)(2,1)S(1)}, bf16[512,256]{1,0:T(8,128)(2,1)S(1)}, u32[]{:S(2)}, u32[]{:S(2)}) %collective-permute-start.18) | collective-permute-done | bytes 262176 | tf_op jit(solution)/shard_map/ppermute | solution.py:610
  88.4 6.2 %retain.1 = (bf16[512,256]{1,0:T(8,128)(2,1)S(1)}, bf16[512,256]{1,0:T(8,128)(2,1)S(1)}) custom-call(f32[1024,8]{1,0:T(8,128)} %copy-done.4, f32[8,1024]{1,0:T(8,128)} %copy-done.18, bf16[8,2,80,128]{3,2,1,0:T(8,128)(2,1)} %all-to-all-done.refs_2_, f32[2,2,64,128]{3,2,1,0:T(8,128)} %refs_3_.4, bf16[5,256,256]{2,1,0:T(8,128)(2,1)} %get-tuple-element.30.refs_1_.refs_4_, ...), custom_call_target="tpu_custom_call" | custom-call | flops 1500000000 | bytes 4194304 | tf_op jit(solution)/shard_map/retain/pallas_call | solution.py:493
  94.7 1.6 %collective-permute-start.25 = (bf16[512,256]{1,0:T(8,128)(2,1)S(1)}, bf16[512,256]{1,0:T(8,128)(2,1)S(1)}, u32[]{:S(2)}, u32[]{:S(2)}) collective-permute-start(bf16[512,256]{1,0:T(8,128)(2,1)S(1)} %get-tuple-element.41.refs_16_), channel_id=1, source_target_pairs={{0,2},{1,3},{2,0},{3,1},{4,6},{5,7},{6,4},{7,5},{8,10},{9,11},{10,... | collective-permute-start | bytes 786440 | tf_op jit(solution)/shard_map/ppermute | solution.py:610
  97.4 6.5 %collective-permute-done.25.refs_2_ = bf16[512,256]{1,0:T(8,128)(2,1)S(1)} collective-permute-done((bf16[512,256]{1,0:T(8,128)(2,1)S(1)}, bf16[512,256]{1,0:T(8,128)(2,1)S(1)}, u32[]{:S(2)}, u32[]{:S(2)}) %collective-permute-start.25) | collective-permute-done | bytes 262176 | tf_op jit(solution)/shard_map/ppermute | solution.py:610
  103.9 5.0 %collective-permute-done.23.refs_2_ = bf16[512,256]{1,0:T(8,128)(2,1)S(1)} collective-permute-done((bf16[512,256]{1,0:T(8,128)(2,1)S(1)}, bf16[512,256]{1,0:T(8,128)(2,1)S(1)}, u32[]{:S(2)}, u32[]{:S(2)}) %collective-permute-start.23) | collective-permute-done | bytes 262176 | tf_op jit(solution)/shard_map/ppermute | solution.py:610
  109.8 0.7 copy-done.27
  110.5 4.5 %most.1 = (f32[1024,512]{1,0:T(8,128)S(1)}, bf16[512,512]{1,0:T(8,128)(2,1)S(1)}) custom-call(bf16[256,2048]{1,0:T(8,128)(2,1)} %refs_0_.11, bf16[256,2048]{1,0:T(8,128)(2,1)} %refs_1_.3, bf16[256,2048]{1,0:T(8,128)(2,1)} %collective-permute-done.refs_2_, bf16[256,2048]{1,0:T(8,128)(2,1)} %collective-permute-done.1.refs_3_, ...), custom_call_target="tpu_custom_call" | custom-call | flops 1000000000 | bytes 8388608 | tf_op jit(solution)/shard_map/most/pallas_call | solution.py:547
  115.0 1.2 last.2.refs_4_
  116.2 1.2 last.3
  (94 shorter events, 4.6 us)
Async XLA Ops:
  0.0 39.4 %copy-start.19 = (bf16[256,2048]{1,0:T(8,128)(2,1)S(1)}, bf16[256,2048]{1,0:T(8,128)(2,1)}, u32[]{:S(2)}) copy-start(bf16[256,2048]{1,0:T(8,128)(2,1)} %refs_0_.11) | copy-start | bytes 3145732
  0.0 39.4 %copy-start.20 = (bf16[256,2048]{1,0:T(8,128)(2,1)S(1)}, bf16[256,2048]{1,0:T(8,128)(2,1)}, u32[]{:S(2)}) copy-start(bf16[256,2048]{1,0:T(8,128)(2,1)} %refs_1_.3) | copy-start | bytes 3145732
  0.0 42.3 %copy-start.17 = (f32[2,1024]{1,0:T(2,128)S(1)}, f32[2,1024]{1,0:T(2,128)}, u32[]{:S(2)}) copy-start(f32[2,1024]{1,0:T(2,128)} %log_ref.1) | copy-start | bytes 24580
  0.0 41.8 %collective-permute-start.6 = (bf16[1024,512]{1,0:T(8,128)(2,1)}, bf16[1024,512]{1,0:T(8,128)(2,1)S(1)}, u32[]{:S(2)}, u32[]{:S(2)}) collective-permute-start(bf16[1024,512]{1,0:T(8,128)(2,1)} %refs_6_.5), channel_id=1, source_target_pairs={{0,1},{1,0},{2,3},{3,2},{4,5},{5,4},{6,7},{7,6},{8,9},{9,8},{10,11... | collective-permute-start | bytes 3145736 | tf_op jit(solution)/shard_map/ppermute | solution.py:605
  1.8 12.6 %collective-permute-start.9 = (bf16[384,512]{1,0:T(8,128)(2,1)S(1)}, bf16[384,512]{1,0:T(8,128)(2,1)S(1)}, u32[]{:S(2)}, u32[]{:S(2)}) collective-permute-start(bf16[384,512]{1,0:T(8,128)(2,1)S(1)} %get-tuple-element.31), channel_id=1, source_target_pairs={{0,2},{1,3},{2,0},{3,1},{4,6},{5,7},{6,4},{7,5},{8,10},{9,11},{10,... | collective-permute-start | bytes 1179656 | tf_op jit(solution)/shard_map/ppermute | solution.py:610
  5.7 34.2 %collective-permute-start.2 = (bf16[256,1024]{1,0:T(8,128)(2,1)S(1)}, bf16[256,1024]{1,0:T(8,128)(2,1)}, u32[]{:S(2)}, u32[]{:S(2)}) collective-permute-start(bf16[256,1024]{1,0:T(8,128)(2,1)S(1)} %get-tuple-element.25), channel_id=1, source_target_pairs={{0,2},{1,3},{2,0},{3,1},{4,6},{5,7},{6,4},{7,5},{8,10},{9,11},{10,... | collective-permute-start | bytes 1572872 | tf_op jit(solution)/shard_map/ppermute | solution.py:610
  5.8 33.6 %collective-permute-start.11 = (bf16[384,512]{1,0:T(8,128)(2,1)S(1)}, bf16[384,512]{1,0:T(8,128)(2,1)S(1)}, u32[]{:S(2)}, u32[]{:S(2)}) collective-permute-start(bf16[384,512]{1,0:T(8,128)(2,1)S(1)} %get-tuple-element.33), channel_id=1, source_target_pairs={{0,2},{1,3},{2,0},{3,1},{4,6},{5,7},{6,4},{7,5},{8,10},{9,11},{10,... | collective-permute-start | bytes 1179656 | tf_op jit(solution)/shard_map/ppermute | solution.py:610
  14.4 27.4 %collective-permute-start.10 = (bf16[384,512]{1,0:T(8,128)(2,1)S(1)}, bf16[384,512]{1,0:T(8,128)(2,1)S(1)}, u32[]{:S(2)}, u32[]{:S(2)}) collective-permute-start(bf16[384,512]{1,0:T(8,128)(2,1)S(1)} %collective-permute-done.9.refs_8_), channel_id=1, source_target_pairs={{0,1},{1,0},{2,3},{3,2},{4,5},{5,4},{6,7},{7,6},{8,9},{9,8},{10,11... | collective-permute-start | bytes 1179656 | tf_op jit(solution)/shard_map/ppermute | solution.py:605
  15.4 23.9 %collective-permute-start.7 = (bf16[256,512]{1,0:T(8,128)(2,1)S(1)}, bf16[256,512]{1,0:T(8,128)(2,1)S(1)}, u32[]{:S(2)}, u32[]{:S(2)}) collective-permute-start(bf16[256,512]{1,0:T(8,128)(2,1)S(1)} %split.2), channel_id=1, source_target_pairs={{0,2},{1,3},{2,0},{3,1},{4,6},{5,7},{6,4},{7,5},{8,10},{9,11},{10,... | collective-permute-start | bytes 786440 | tf_op jit(solution)/shard_map/ppermute | solution.py:610
  39.4 47.1 %collective-permute-start = (bf16[256,2048]{1,0:T(8,128)(2,1)S(1)}, bf16[256,2048]{1,0:T(8,128)(2,1)}, u32[]{:S(2)}, u32[]{:S(2)}) collective-permute-start(bf16[256,2048]{1,0:T(8,128)(2,1)S(1)} %copy-done.19), channel_id=1, source_target_pairs={{0,1},{1,0},{2,3},{3,2},{4,5},{5,4},{6,7},{7,6},{8,9},{9,8},{10,11... | collective-permute-start | bytes 3145736 | tf_op jit(solution)/shard_map/ppermute | solution.py:605
  39.4 55.3 %collective-permute-start.1 = (bf16[256,2048]{1,0:T(8,128)(2,1)S(1)}, bf16[256,2048]{1,0:T(8,128)(2,1)}, u32[]{:S(2)}, u32[]{:S(2)}) collective-permute-start(bf16[256,2048]{1,0:T(8,128)(2,1)S(1)} %copy-done.20), channel_id=1, source_target_pairs={{0,1},{1,0},{2,3},{3,2},{4,5},{5,4},{6,7},{7,6},{8,9},{9,8},{10,11... | collective-permute-start | bytes 3145736 | tf_op jit(solution)/shard_map/ppermute | solution.py:605
  40.0 23.3 %collective-permute-start.4 = (bf16[256,1024]{1,0:T(8,128)(2,1)S(1)}, bf16[256,1024]{1,0:T(8,128)(2,1)}, u32[]{:S(2)}, u32[]{:S(2)}) collective-permute-start(bf16[256,1024]{1,0:T(8,128)(2,1)S(1)} %get-tuple-element.26), channel_id=1, source_target_pairs={{0,2},{1,3},{2,0},{3,1},{4,6},{5,7},{6,4},{7,5},{8,10},{9,11},{10,... | collective-permute-start | bytes 1572872 | tf_op jit(solution)/shard_map/ppermute | solution.py:610
  41.8 11.2 %collective-permute-start.8 = (bf16[256,512]{1,0:T(8,128)(2,1)S(1)}, bf16[256,512]{1,0:T(8,128)(2,1)S(1)}, u32[]{:S(2)}, u32[]{:S(2)}) collective-permute-start(bf16[256,512]{1,0:T(8,128)(2,1)S(1)} %collective-permute-done.7.refs_8_), channel_id=1, source_target_pairs={{0,1},{1,0},{2,3},{3,2},{4,5},{5,4},{6,7},{7,6},{8,9},{9,8},{10,11... | collective-permute-start | bytes 786440 | tf_op jit(solution)/shard_map/ppermute | solution.py:605
  41.8 6.2 %collective-permute-start.12 = (bf16[384,512]{1,0:T(8,128)(2,1)S(1)}, bf16[384,512]{1,0:T(8,128)(2,1)S(1)}, u32[]{:S(2)}, u32[]{:S(2)}) collective-permute-start(bf16[384,512]{1,0:T(8,128)(2,1)S(1)} %collective-permute-done.11.refs_8_), channel_id=1, source_target_pairs={{0,1},{1,0},{2,3},{3,2},{4,5},{5,4},{6,7},{7,6},{8,9},{9,8},{10,11... | collective-permute-start | bytes 1179656 | tf_op jit(solution)/shard_map/ppermute | solution.py:605
  48.0 37.5 %collective-permute-start.3 = (bf16[256,1024]{1,0:T(8,128)(2,1)}, bf16[256,1024]{1,0:T(8,128)(2,1)}, u32[]{:S(2)}, u32[]{:S(2)}) collective-permute-start(bf16[256,1024]{1,0:T(8,128)(2,1)} %collective-permute-done.2.refs_4_), channel_id=1, source_target_pairs={{0,1},{1,0},{2,3},{3,2},{4,5},{5,4},{6,7},{7,6},{8,9},{9,8},{10,11... | collective-permute-start | bytes 1572872 | tf_op jit(solution)/shard_map/ppermute | solution.py:605
  53.0 24.1 %copy-start.16 = (f32[4]{0:T(128)S(1)}, f32[4]{0:T(128)}, u32[]{:S(2)}) copy-start(f32[4]{0:T(128)} %refs_0_.10) | copy-start | bytes 52
  57.5 30.9 %all-to-all-start = ((bf16[8,2,80,128]{3,2,1,0:T(8,128)(2,1)}), bf16[8,2,80,128]{3,2,1,0:T(8,128)(2,1)}, u32[]{:S(2)}, u32[]{:S(2)}) async-start(bf16[8,2,80,128]{3,2,1,0:T(8,128)(2,1)} %totals.1), calls=%async_computation | async-start | bytes 655360 | tf_op jit(solution)/shard_map/all_to_all | solution.py:719
  63.3 23.1 %collective-permute-start.5 = (bf16[256,1024]{1,0:T(8,128)(2,1)}, bf16[256,1024]{1,0:T(8,128)(2,1)S(1)}, u32[]{:S(2)}, u32[]{:S(2)}) collective-permute-start(bf16[256,1024]{1,0:T(8,128)(2,1)} %collective-permute-done.4.refs_6_), channel_id=1, source_target_pairs={{0,1},{1,0},{2,3},{3,2},{4,5},{5,4},{6,7},{7,6},{8,9},{9,8},{10,11... | collective-permute-start | bytes 1572872 | tf_op jit(solution)/shard_map/ppermute | solution.py:605
  63.5 6.6 %collective-permute-start.13 = (bf16[128,256]{1,0:T(8,128)(2,1)S(1)}, bf16[128,256]{1,0:T(8,128)(2,1)S(1)}, u32[]{:S(2)}, u32[]{:S(2)}) collective-permute-start(bf16[128,256]{1,0:T(8,128)(2,1)S(1)} %get-tuple-element.35), channel_id=1, source_target_pairs={{0,4},{4,0},{8,12},{12,8},{16,20},{20,16},{24,28},{28,24},{1,5},{5... | collective-permute-start | bytes 196616 | tf_op jit(solution)/shard_map/ppermute | solution.py:715
  70.1 7.0 %collective-permute-start.14 = (bf16[128,256]{1,0:T(8,128)(2,1)S(1)}, bf16[128,256]{1,0:T(8,128)(2,1)S(1)}, u32[]{:S(2)}, u32[]{:S(2)}) collective-permute-start(bf16[128,256]{1,0:T(8,128)(2,1)S(1)} %get-tuple-element.36), channel_id=1, source_target_pairs={{0,28},{4,8},{8,4},{12,16},{16,12},{20,24},{24,20},{28,0},{1,29},{... | collective-permute-start | bytes 196616 | tf_op jit(solution)/shard_map/ppermute | solution.py:717
  80.6 7.8 %collective-permute-start.18 = (bf16[512,256]{1,0:T(8,128)(2,1)S(1)}, bf16[512,256]{1,0:T(8,128)(2,1)S(1)}, u32[]{:S(2)}, u32[]{:S(2)}) collective-permute-start(bf16[512,256]{1,0:T(8,128)(2,1)S(1)} %attend.3.refs_9_), channel_id=1, source_target_pairs={{0,2},{1,3},{2,0},{3,1},{4,6},{5,7},{6,4},{7,5},{8,10},{9,11},{10,... | collective-permute-start | bytes 786440 | tf_op jit(solution)/shard_map/ppermute | solution.py:610
  85.5 10.8 %collective-permute-start.17 = (bf16[512,256]{1,0:T(8,128)(2,1)S(1)}, bf16[512,256]{1,0:T(8,128)(2,1)}, u32[]{:S(2)}, u32[]{:S(2)}) collective-permute-start(bf16[512,256]{1,0:T(8,128)(2,1)S(1)} %attend.2.refs_8_), channel_id=1, source_target_pairs={{0,2},{1,3},{2,0},{3,1},{4,6},{5,7},{6,4},{7,5},{8,10},{9,11},{10,... | collective-permute-start | bytes 786440 | tf_op jit(solution)/shard_map/ppermute | solution.py:610
  86.4 10.4 %collective-permute-start.16 = (bf16[512,256]{1,0:T(8,128)(2,1)S(1)}, bf16[512,256]{1,0:T(8,128)(2,1)}, u32[]{:S(2)}, u32[]{:S(2)}) collective-permute-start(bf16[512,256]{1,0:T(8,128)(2,1)S(1)} %attend.3.refs_9_), channel_id=1, source_target_pairs={{0,1},{1,0},{2,3},{3,2},{4,5},{5,4},{6,7},{7,6},{8,9},{9,8},{10,11... | collective-permute-start | bytes 786440 | tf_op jit(solution)/shard_map/ppermute | solution.py:605
  86.4 10.3 %collective-permute-start.15 = (bf16[512,256]{1,0:T(8,128)(2,1)S(1)}, bf16[512,256]{1,0:T(8,128)(2,1)S(1)}, u32[]{:S(2)}, u32[]{:S(2)}) collective-permute-start(bf16[512,256]{1,0:T(8,128)(2,1)S(1)} %attend.2.refs_8_), channel_id=1, source_target_pairs={{0,1},{1,0},{2,3},{3,2},{4,5},{5,4},{6,7},{7,6},{8,9},{9,8},{10,11... | collective-permute-start | bytes 786440 | tf_op jit(solution)/shard_map/ppermute | solution.py:605
  88.4 8.9 %collective-permute-start.20 = (bf16[512,256]{1,0:T(8,128)(2,1)S(1)}, bf16[512,256]{1,0:T(8,128)(2,1)S(1)}, u32[]{:S(2)}, u32[]{:S(2)}) collective-permute-start(bf16[512,256]{1,0:T(8,128)(2,1)S(1)} %collective-permute-done.18.refs_13_), channel_id=1, source_target_pairs={{0,1},{1,0},{2,3},{3,2},{4,5},{5,4},{6,7},{7,6},{8,9},{9,8},{10,11... | collective-permute-start | bytes 786440 | tf_op jit(solution)/shard_map/ppermute | solution.py:605
  94.7 9.2 %collective-permute-start.25 = (bf16[512,256]{1,0:T(8,128)(2,1)S(1)}, bf16[512,256]{1,0:T(8,128)(2,1)S(1)}, u32[]{:S(2)}, u32[]{:S(2)}) collective-permute-start(bf16[512,256]{1,0:T(8,128)(2,1)S(1)} %get-tuple-element.41.refs_16_), channel_id=1, source_target_pairs={{0,2},{1,3},{2,0},{3,1},{4,6},{5,7},{6,4},{7,5},{8,10},{9,11},{10,... | collective-permute-start | bytes 786440 | tf_op jit(solution)/shard_map/ppermute | solution.py:610
  96.3 12.7 %collective-permute-start.23 = (bf16[512,256]{1,0:T(8,128)(2,1)S(1)}, bf16[512,256]{1,0:T(8,128)(2,1)S(1)}, u32[]{:S(2)}, u32[]{:S(2)}) collective-permute-start(bf16[512,256]{1,0:T(8,128)(2,1)S(1)} %get-tuple-element.42.refs_17_), channel_id=1, source_target_pairs={{0,2},{1,3},{2,0},{3,1},{4,6},{5,7},{6,4},{7,5},{8,10},{9,11},{10,... | collective-permute-start | bytes 786440 | tf_op jit(solution)/shard_map/ppermute | solution.py:610
  96.8 12.2 %collective-permute-start.19 = (bf16[512,256]{1,0:T(8,128)(2,1)}, bf16[512,256]{1,0:T(8,128)(2,1)S(1)}, u32[]{:S(2)}, u32[]{:S(2)}) collective-permute-start(bf16[512,256]{1,0:T(8,128)(2,1)} %collective-permute-done.17.refs_12_), channel_id=1, source_target_pairs={{0,1},{1,0},{2,3},{3,2},{4,5},{5,4},{6,7},{7,6},{8,9},{9,8},{10,11... | collective-permute-start | bytes 786440 | tf_op jit(solution)/shard_map/ppermute | solution.py:605
  96.8 12.2 %collective-permute-start.21 = (bf16[512,256]{1,0:T(8,128)(2,1)S(1)}, bf16[512,256]{1,0:T(8,128)(2,1)S(1)}, u32[]{:S(2)}, u32[]{:S(2)}) collective-permute-start(bf16[512,256]{1,0:T(8,128)(2,1)S(1)} %get-tuple-element.41.refs_16_), channel_id=1, source_target_pairs={{0,1},{1,0},{2,3},{3,2},{4,5},{5,4},{6,7},{7,6},{8,9},{9,8},{10,11... | collective-permute-start | bytes 786440 | tf_op jit(solution)/shard_map/ppermute | solution.py:605
  97.3 11.7 %collective-permute-start.22 = (bf16[512,256]{1,0:T(8,128)(2,1)S(1)}, bf16[512,256]{1,0:T(8,128)(2,1)S(1)}, u32[]{:S(2)}, u32[]{:S(2)}) collective-permute-start(bf16[512,256]{1,0:T(8,128)(2,1)S(1)} %get-tuple-element.42.refs_17_), channel_id=1, source_target_pairs={{0,1},{1,0},{2,3},{3,2},{4,5},{5,4},{6,7},{7,6},{8,9},{9,8},{10,11... | collective-permute-start | bytes 786440 | tf_op jit(solution)/shard_map/ppermute | solution.py:605
  103.9 11.1 %collective-permute-start.26 = (bf16[512,256]{1,0:T(8,128)(2,1)S(1)}, bf16[512,256]{1,0:T(8,128)(2,1)S(1)}, u32[]{:S(2)}, u32[]{:S(2)}) collective-permute-start(bf16[512,256]{1,0:T(8,128)(2,1)S(1)} %collective-permute-done.25.refs_2_), channel_id=1, source_target_pairs={{0,1},{1,0},{2,3},{3,2},{4,5},{5,4},{6,7},{7,6},{8,9},{9,8},{10,11... | collective-permute-start | bytes 786440 | tf_op jit(solution)/shard_map/ppermute | solution.py:605
  109.0 7.2 %collective-permute-start.24 = (bf16[512,256]{1,0:T(8,128)(2,1)S(1)}, bf16[512,256]{1,0:T(8,128)(2,1)S(1)}, u32[]{:S(2)}, u32[]{:S(2)}) collective-permute-start(bf16[512,256]{1,0:T(8,128)(2,1)S(1)} %collective-permute-done.23.refs_2_), channel_id=1, source_target_pairs={{0,1},{1,0},{2,3},{3,2},{4,5},{5,4},{6,7},{7,6},{8,9},{9,8},{10,11... | collective-permute-start | bytes 786440 | tf_op jit(solution)/shard_map/ppermute | solution.py:605
  (24 other events, 146.6 us)
